TPU v7x, 512 devices: a whole 4x8x8 slice. The times are simulated.
512 devices in a mesh: ep: 32 (over z, x), tp: 16 (over y, core).
Axes of the slice: x: 4, y: 8, z: 8, core: 2. Of those that a mesh axis runs over, the one named last changes fastest.
Arguments:
- mixer_rows: bfloat16 [4096, 2048], P('ep'), may hold values from -40 to 40
- mixer_gain: float32 [2048], replicated, may hold values from 0.1 to 1.9
- inner_weight: bfloat16 [2048, 1024], P(None, 'tp'), may hold values from -0.125 to 0.125
- gate_in_weight: bfloat16 [2048, 1024], P(None, 'tp'), may hold values from -0.125 to 0.125
- gate_out_weight: bfloat16 [2048, 1024], P(None, 'tp'), may hold values from -0.125 to 0.125
- conv_taps: float32 [3, 1024], P(None, 'tp'), may hold values from -3.5 to 3.5
- mixer_out_weight: bfloat16 [1024, 2048], P('tp'), may hold values from -0.1875 to 0.1875
- routed_rows: bfloat16 [8192, 2048], P('ep'), may hold values from -40 to 40
- routed_gain: float32 [2048], replicated, may hold values from 0.1 to 1.9
- route_ids: int32 [8192, 2], P('ep'), may hold values from 0 to 31, all different within a row; in each aligned block of 256 rows (0 to 255, 256 to 511, ...) at most 32 rows name the same one
- route_weights: float32 [8192, 2], P('ep'), may hold values from 0.25 to 1
- expert_gate: bfloat16 [32, 2048, 2048], P('ep', None, 'tp'), may hold values from -0.125 to 0.125
- expert_up: bfloat16 [32, 2048, 2048], P('ep', None, 'tp'), may hold values from -0.125 to 0.125
- expert_down: bfloat16 [32, 2048, 2048], P('ep', 'tp'), may hold values from -0.125 to 0.125
Outputs:
- mixer_output: bfloat16 [4096, 2048], P('ep')
- routed_output: bfloat16 [8192, 2048], P('ep')
Inputs may be any that keep to these rules, and one draw needn't show every extreme that they name: `route_ids`: within each aligned block of 256 tokens, no expert is named by more than 32 choices, a bound that some block reaches; a token's 2 experts differ.
All inputs are finite; a program needn't handle non-finite values.
Results may differ from a plain program's by a relative error of at most 0.019.
Values may be sent and summed in bfloat16 or wider, within the bound.
No kernel may reach another device: no remote copies, remote signals or barrier semaphores. Data moves between devices by JAX's collectives and lax.ppermute only.
A program may use at most 64 MiB of HBM per device.

v0:
```python
import jax
import jax.numpy as jnp
from jax import lax
from jax.sharding import PartitionSpec as P


def shifted(value, axis, steps):
    count = lax.axis_size(axis)
    initial, last = (max(0, -steps), min(count, count - steps))
    return lax.ppermute(value, axis, [(source, source + steps) for source in range(initial, last)])


def packed_total(arrays, axis):
    ends = [0]
    for a in arrays:
        ends.append(ends[-1] + a.size)
    so_far = lax.psum(jnp.concatenate([a.ravel() for a in arrays]), axis)
    return tuple((so_far[b:e].reshape(a.shape) for a, b, e in zip(arrays, ends, ends[1:])))


def rms_scale(row_block, gain_row):
    values = row_block.astype(jnp.float32)
    scaled = values * lax.rsqrt(jnp.mean(values * values, axis=-1, keepdims=True) + 1e-06)
    return (scaled * gain_row).astype(jnp.bfloat16)


def on_device(
    mixer_rows,
    mixer_gain,
    inner_weight,
    gate_in_weight,
    gate_out_weight,
    conv_taps,
    mixer_out_weight,
    routed_rows,
    routed_gain,
    route_ids,
    route_weights,
    expert_gate,
    expert_up,
    expert_down,
):
    normed = rms_scale(mixer_rows, mixer_gain)
    inner_proj = jnp.dot(normed, inner_weight, preferred_element_type=jnp.float32)
    gate_in = jnp.dot(normed, gate_in_weight, preferred_element_type=jnp.float32)
    conv_input = (gate_in * inner_proj).astype(jnp.bfloat16)
    gate_out = jnp.dot(normed, gate_out_weight, preferred_element_type=jnp.float32)
    tap_total = conv_taps.shape[0]
    rim_rows = tap_total - 1
    earlier_rows = shifted(conv_input[conv_input.shape[0] - rim_rows :], "ep", 1)
    extended = jnp.concatenate([earlier_rows, conv_input], axis=0).astype(jnp.float32)
    length = conv_input.shape[0]
    conv_out = jnp.zeros(conv_input.shape, jnp.float32)
    for tap_index in range(tap_total):
        conv_out = conv_out + conv_taps[tap_index] * extended[tap_index : tap_index + length]
    gated_conv = (gate_out * conv_out).astype(jnp.bfloat16)
    mixer_terms = jnp.dot(gated_conv, mixer_out_weight, preferred_element_type=jnp.float32)
    routed_normed = rms_scale(routed_rows, routed_gain)
    experts = lax.axis_size("ep")
    groups = lax.axis_size("tp")
    column = lax.axis_index("tp")
    tok_count, pick_count = route_ids.shape
    model_width = routed_rows.shape[1]
    capacity = 2 * tok_count * pick_count // experts
    share_rows = capacity // groups
    flat_ids = route_ids.reshape(-1)
    onehot = (flat_ids[:, None] == jnp.arange(experts, dtype=jnp.int32)[None, :]).astype(jnp.int32)
    slot_rank = jnp.sum((jnp.cumsum(onehot, axis=0) - onehot) * onehot, axis=1)
    slot_number = slot_rank * experts + flat_ids
    owners = jnp.arange(tok_count * pick_count, dtype=jnp.int32) // pick_count
    matches = slot_number[None, :] == jnp.arange(capacity * experts, dtype=jnp.int32)[:, None]
    token_table = jnp.where(
        jnp.any(matches, axis=1), jnp.sum(jnp.where(matches, owners[None, :], 0), axis=1), tok_count
    )
    padded_rows = jnp.concatenate(
        [routed_normed, jnp.zeros((1, model_width), jnp.bfloat16)], axis=0
    )
    table_share = lax.dynamic_slice_in_dim(
        token_table.reshape(capacity, experts), column * share_rows, share_rows, 0
    )
    outgoing = jnp.take(padded_rows, table_share.reshape(-1), axis=0).reshape(
        share_rows, experts, model_width
    )
    arrived = lax.all_to_all(outgoing, "ep", split_axis=1, concat_axis=1, tiled=True)
    incoming = lax.all_gather(arrived, "tp", axis=0, tiled=True)
    slot_rows = incoming.reshape(capacity * experts, model_width)
    gate_act = jnp.dot(slot_rows, expert_gate[0], preferred_element_type=jnp.float32)
    up_act = jnp.dot(slot_rows, expert_up[0], preferred_element_type=jnp.float32)
    hidden = (jax.nn.silu(gate_act) * up_act).astype(jnp.bfloat16)
    summed = lax.psum_scatter(
        jnp.dot(hidden, expert_down[0], preferred_element_type=jnp.float32).astype(jnp.bfloat16),
        "tp",
        scatter_dimension=0,
        tiled=True,
    )
    returned = lax.all_to_all(
        summed.reshape(share_rows, experts, model_width),
        "ep",
        split_axis=1,
        concat_axis=1,
        tiled=True,
    )
    flat_back = jnp.concatenate(
        [
            returned.reshape(share_rows * experts, model_width),
            jnp.zeros((1, model_width), jnp.bfloat16),
        ],
        axis=0,
    )
    local_slot = jnp.where(
        slot_rank // share_rows == column,
        (slot_rank - column * share_rows) * experts + flat_ids,
        share_rows * experts,
    )
    contrib = (
        jnp.take(flat_back, local_slot, axis=0).astype(jnp.float32)
        * route_weights.reshape(-1)[:, None]
    )
    routed_terms = jnp.sum(contrib.reshape(tok_count, pick_count, model_width), axis=1)
    mixer_total, routed_total = tuple(
        (
            part.astype(jnp.float32)
            for part in packed_total(
                (mixer_terms.astype(jnp.bfloat16), routed_terms.astype(jnp.bfloat16)), "tp"
            )
        )
    )
    return (mixer_total.astype(jnp.bfloat16), routed_total.astype(jnp.bfloat16))


def solution(mesh):
    return jax.shard_map(
        on_device,
        mesh=mesh,
        in_specs=(
            P("ep", None),
            P(),
            P(None, "tp"),
            P(None, "tp"),
            P(None, "tp"),
            P(None, "tp"),
            P("tp", None),
            P("ep", None),
            P(),
            P("ep", None),
            P("ep", None),
            P("ep", None, "tp"),
            P("ep", None, "tp"),
            P("ep", "tp", None),
        ),
        out_specs=(P("ep", None), P("ep", None)),
        check_vma=False,
    )
```

profile of v0, /device:TPU:1, one launch (start us, length us, event | category | flops | bytes accessed | tf_op | source)
XLA Modules:
  0.0 321.4 jit_solution(4402862292982536007)
XLA Ops:
  7.2 0.9 copy.70
  8.5 1.2 reduce-window.6
  10.0 0.3 fusion.3
  10.3 0.3 select_reduce_fusion
  10.8 1.5 fusion
  12.4 1.0 fusion.2
  13.5 0.7 gather_fusion
  14.3 0.3 broadcast_select_fusion.1
  14.6 24.8 %all_to_all.10 = bf16[2,32,2048]{2,0,1:T(2,128)(2,1)S(1)} all-to-all(bf16[2,32,2048]{2,0,1:T(2,128)(2,1)S(1)} %broadcast_select_fusion.1), channel_id=1, replica_groups=mesh['ep'=32,'tp'=16] {'ep'}, dimensions={1} | all-to-all | bytes 524288 | tf_op jit(solution)/shard_map/all_to_all | solution.py:84
  39.5 0.8 copy.81
  40.3 42.1 %all-gather.2.cloned.1.call-done = bf16[32,32,2048]{2,1,0:T(8,128)(2,1)} async-done(((bf16[2,32,2048]{2,1,0:T(8,128)(2,1)}), bf16[32,32,2048]{2,1,0:T(8,128)(2,1)}) %all-gather.2.cloned.1.call-update) | async-done | bytes 4194320 | tf_op jit(solution)/shard_map/all_gather | solution.py:85
  82.4 3.5 %fusion.14 = f32[1024,128]{1,0:T(8,128)S(1)} fusion(bf16[1024,2048]{1,0:T(8,128)(2,1)} %bitcast.56, bf16[1,2048,128]{2,1,0:T(8,128)(2,1)S(1)} %copy-done.3), kind=kOutput, calls=%fused_computation.30 | convolution fusion | flops 536870912 | bytes 5242880 | tf_op jit(solution)/shard_map/dot_general | solution.py:87
  86.0 8.5 %convolution_convert_fusion = bf16[1024,2048]{1,0:T(8,128)(2,1)} fusion(bf16[1024,2048]{1,0:T(8,128)(2,1)} %bitcast.57, bf16[1,128,2048]{2,1,0:T(8,128)(2,1)S(1)} %copy-done, bf16[1,2048,128]{2,1,0:T(8,128)(2,1)S(1)} %copy-done.4, f32[1024,128]{1,0:T(8,128)S(1)} %fusion.14), kind=kOutput, calls=%fused_computation.4 | convolution fusion | flops 1076625408 | bytes 9961472 | tf_op jit(solution)/shard_map/dot_general | solution.py:91
  94.5 1.0 copy-done.2
  95.7 0.4 fusion.39
  96.1 0.4 fusion.7
  96.5 3.1 collective-permute-start
  100.1 56.6 %reduce-scatter.2.cloned.1.call-done = bf16[64,2048]{1,0:T(8,128)(2,1)} async-done(((bf16[1024,2048]{1,0:T(8,128)(2,1)}), bf16[64,2048]{1,0:T(8,128)(2,1)}) %reduce-scatter.2.cloned.1.call-update) | async-done | bytes 262160 | tf_op jit(solution)/shard_map/reduce_scatter | solution.py:90
  156.7 1.9 copy.82
  158.6 9.1 %all-to-all-start.1 = ((bf16[2,32,2048]{2,0,1:T(2,128)(2,1)}), bf16[2,32,2048]{2,0,1:T(2,128)(2,1)S(1)}, u32[]{:S(2)}, u32[]{:S(2)}) async-start(bf16[2,32,2048]{2,0,1:T(2,128)(2,1)} %copy.82), calls=%async_computation.2 | async-start | bytes 524288 | tf_op jit(solution)/shard_map/all_to_all | solution.py:96
  168.1 0.8 copy.85
  169.0 0.9 fusion.4
  170.1 8.1 %all-to-all-done.1 = bf16[2,32,2048]{2,0,1:T(2,128)(2,1)S(1)} async-done(((bf16[2,32,2048]{2,0,1:T(2,128)(2,1)}), bf16[2,32,2048]{2,0,1:T(2,128)(2,1)S(1)}, u32[]{:S(2)}, u32[]{:S(2)}) %all-to-all-start.1) | async-done | bytes 262176 | tf_op jit(solution)/shard_map/all_to_all | solution.py:96
  178.3 2.5 gather_fusion.1
  180.8 2.7 gather.15
  183.4 9.9 %multiply_reduce_fusion = bf16[256,2048]{1,0:T(8,128)(2,1)S(1)} fusion(bf16[256,2,2048]{2,1,0:T(2,128)(2,1)} %gather.15, pred[256,2]{1,0:T(8,128)(4,1)S(1)} %copy.78, f32[256,2]{1,0:T(8,128)S(1)} %copy-done.5), kind=kLoop, calls=%fused_computation.2 | loop fusion | flops 3670016 | bytes 3148288 | tf_op jit(solution)/shard_map/reduce_sum | solution.py:119
  193.3 0.2 copy.88
  193.5 1.3 pad_maximum_fusion
  194.8 116.5 %all-reduce.4.cloned.1.call-done = bf16[786432]{0:T(1024)(128)(2,1)} async-done(((bf16[786432]{0:T(1024)(128)(2,1)}), bf16[786432]{0:T(1024)(128)(2,1)}) %all-reduce.4.cloned.1.call-update) | async-done | bytes 1572880 | tf_op jit(solution)/shard_map/psum | solution.py:17
  311.4 1.2 slice-done
  312.6 1.3 slice.65
  313.8 1.0 slice.63
  (69 shorter events, 2.6 us)
Async XLA Ops:
  7.2 78.8 %copy-start = (bf16[1,128,2048]{2,1,0:T(8,128)(2,1)S(1)}, bf16[1,128,2048]{2,1,0:T(8,128)(2,1)}, u32[]{:S(2)}) copy-start(bf16[1,128,2048]{2,1,0:T(8,128)(2,1)} %param.27) | copy-start | bytes 1572868
  7.2 5.3 %copy-start.1 = (bf16[256,2048]{1,0:T(8,128)(2,1)S(1)}, bf16[256,2048]{1,0:T(8,128)(2,1)}, u32[]{:S(2)}) copy-start(bf16[256,2048]{1,0:T(8,128)(2,1)} %param.21) | copy-start | bytes 3145732
  7.2 75.2 %all-gather.2.cloned.1.call-start = ((), (), s32[]{:S(2)}) async-start(), calls=%async_computation.3 | async-start | bytes 4456448 | tf_op jit(solution)/shard_map/all_gather | solution.py:85
  13.5 68.9 %copy-start.3 = (bf16[1,2048,128]{2,1,0:T(8,128)(2,1)S(1)}, bf16[1,2048,128]{2,1,0:T(8,128)(2,1)}, u32[]{:S(2)}) copy-start(bf16[1,2048,128]{2,1,0:T(8,128)(2,1)} %param.25) | copy-start | bytes 1572868
  40.3 116.4 %reduce-scatter.2.cloned.1.call-start = ((), (), s32[]{:S(2)}) async-start(), calls=%async_computation.4 | async-start | bytes 4456448 | tf_op jit(solution)/shard_map/reduce_scatter | solution.py:90
  82.4 3.5 %copy-start.4 = (bf16[1,2048,128]{2,1,0:T(8,128)(2,1)S(1)}, bf16[1,2048,128]{2,1,0:T(8,128)(2,1)}, u32[]{:S(2)}) copy-start(bf16[1,2048,128]{2,1,0:T(8,128)(2,1)} %param.26) | copy-start | bytes 1572868
  94.4 1.0 copy-start.2
  94.4 1.3 copy-start.8
  94.4 1.3 copy-start.12
  94.4 1.7 copy-start.13
  95.5 4.5 %copy-start.9 = (s32[256,2]{0,1:T(2,128)S(1)}, s32[256,2]{0,1:T(2,128)}, u32[]{:S(2)}) copy-start(s32[256,2]{0,1:T(2,128)} %param.23) | copy-start | bytes 6148
  95.5 72.4 %copy-start.11 = (f32[3,64]{1,0:T(4,128)S(1)}, f32[3,64]{1,0:T(4,128)}, u32[]{:S(2)}) copy-start(f32[3,64]{1,0:T(4,128)} %param.19) | copy-start | bytes 2308
  95.5 72.7 %copy-start.10 = (f32[256,2]{0,1:T(2,128)S(1)}, f32[256,2]{0,1:T(2,128)}, u32[]{:S(2)}) copy-start(f32[256,2]{0,1:T(2,128)} %param.24) | copy-start | bytes 6148
  95.7 73.4 %copy-start.6 = (bf16[64,2048]{1,0:T(8,128)(2,1)S(1)}, bf16[64,2048]{1,0:T(8,128)(2,1)}, u32[]{:S(2)}) copy-start(bf16[64,2048]{1,0:T(8,128)(2,1)} %param.20) | copy-start | bytes 786436
  95.7 73.4 %copy-start.7 = (bf16[2048,64]{0,1:T(8,128)(2,1)S(1)}, bf16[2048,64]{0,1:T(8,128)(2,1)}, u32[]{:S(2)}) copy-start(bf16[2048,64]{0,1:T(8,128)(2,1)} %param.18) | copy-start | bytes 786436
  96.5 72.4 %collective-permute-start = (bf16[2,64]{0,1:T(8,128)(2,1)S(1)}, bf16[2,64]{0,1:T(8,128)(2,1)S(1)}, u32[]{:S(2)}, u32[]{:S(2)}) collective-permute-start(bf16[2,64]{0,1:T(8,128)(2,1)S(1)} %slice.70), channel_id=1, source_target_pairs={{0,16},{16,32},{32,48},{48,64},{64,80},{80,96},{96,112},{112,128},... | collective-permute-start | bytes 776 | tf_op jit(solution)/shard_map/ppermute | solution.py:10
  158.6 19.6 %all-to-all-start.1 = ((bf16[2,32,2048]{2,0,1:T(2,128)(2,1)}), bf16[2,32,2048]{2,0,1:T(2,128)(2,1)S(1)}, u32[]{:S(2)}, u32[]{:S(2)}) async-start(bf16[2,32,2048]{2,0,1:T(2,128)(2,1)} %copy.82), calls=%async_computation.2 | async-start | bytes 524288 | tf_op jit(solution)/shard_map/all_to_all | solution.py:96
  167.7 143.7 %all-reduce.4.cloned.1.call-start = ((), (), s32[]{:S(2)}) async-start(), calls=%async_computation.5 | async-start | bytes 3145728 | tf_op jit(solution)/shard_map/psum | solution.py:17
  180.8 2.7 copy-start.5
  311.3 1.2 slice-start
  312.6 1.3 slice-start.1
Sparse Core Ops, SparseCore 0:
  40.4 42.0 all-gather.1
  94.6 62.0 reduce-scatter.1
  194.9 116.3 all-reduce.3
where the time goes:
time: 322 us; the launch traced here: 321 us
  waiting for transfers between devices  223 us (69%)
  blocking collectives  24.8 us (8%)
  local copies, waits for them, and re-layouts  16.8 us (5%)
  other arithmetic  16.3 us (5%)
  between operations  14.1 us (4%)
  matrix products  13.6 us (4%)
  starting transfers between devices  12.5 us (4%)
    psum x1, waiting for transfers between devices, packed_total(): so_far = lax.psum(jnp.concatenate([a.ravel() for a in arrays]), axis)  117 us
    reduce_scatter x1, waiting for transfers between devices, on_device(): lax.psum_scatter(jnp.dot(hidden, expert_down[0], preferred_element_type=j...  56.6 us
    all_gather x1, waiting for transfers between devices, on_device(): incoming = lax.all_gather(arrived, 'tp', axis=0, tiled=True)  42.1 us
    all_to_all x1, blocking collectives, on_device(): lax.all_to_all(outgoing, 'ep', split_axis=1, concat_axis=1, tiled=True)  24.8 us
    reduce_sum x1, other arithmetic, on_device(): jnp.sum(contrib.reshape(tok_count, pick_count, model_width), axis=1)  9.87 us
    all_to_all x1, starting transfers between devices, on_device(): lax.all_to_all(summed.reshape(share_rows, experts, model_width), 'ep', sp...  9.09 us
    dot_general x1, matrix products, on_device(): jnp.dot(hidden, expert_down[0], preferred_element_type=jnp.float32)  8.47 us
    all_to_all x1, waiting for transfers between devices, on_device(): lax.all_to_all(summed.reshape(share_rows, experts, model_width), 'ep', sp...  8.08 us
  transfers between devices with their start and end apart: 5, of which 4 were waited for; matrix products, arithmetic and copies ran while one was open for 2% of the time, Pallas kernels for 0%

commit v1 on v0

v1 whole, which is shorter than its diff:
```python
import functools

import jax
import jax.numpy as jnp
from jax import lax
from jax.experimental import pallas as pl
from jax.experimental.pallas import tpu as pltpu
from jax.sharding import Mesh, PartitionSpec as P

TP = ("p", "q", "c")
ALL = ("ep", "p", "q", "c")
VM = pl.BlockSpec(memory_space=pltpu.VMEM)


def rms_scale(row_block, gain_row):
    values = row_block.astype(jnp.float32)
    scaled = values * lax.rsqrt(jnp.mean(values * values, axis=-1, keepdims=True) + 1e-06)
    return (scaled * gain_row).astype(jnp.bfloat16)


def flipped(value, axis):
    return lax.ppermute(value, axis, [(0, 1), (1, 0)])


def ffn_kernel(x_ref, a0, a1, a2, a3, d0, d1, d2, d3, out_ref, hid_ref):
    x = x_ref[...]
    width = x.shape[1]
    part = a0.shape[1]
    for i, a in enumerate((a0, a1, a2, a3)):
        gate = jnp.dot(x, a[:width, :], preferred_element_type=jnp.float32)
        up = jnp.dot(x, a[width:, :], preferred_element_type=jnp.float32)
        hid_ref[:, i * part : (i + 1) * part] = (gate / (1.0 + jnp.exp(-gate)) * up).astype(jnp.bfloat16)
    cols = 512
    for n in range(0, out_ref.shape[1], cols):
        total = None
        for i, d in enumerate((d0, d1, d2, d3)):
            term = jnp.dot(
                hid_ref[:, i * part : (i + 1) * part],
                d[:, n : n + cols],
                preferred_element_type=jnp.float32,
            )
            total = term if total is None else total + term
        out_ref[:, n : n + cols] = total.astype(jnp.bfloat16)


def expert_ffn(x, gates, downs):
    hidden = sum(d.shape[0] for d in downs)
    return pl.pallas_call(
        ffn_kernel,
        out_shape=jax.ShapeDtypeStruct(x.shape, jnp.bfloat16),
        in_specs=[VM] * 9,
        out_specs=VM,
        scratch_shapes=[pltpu.VMEM((x.shape[0], hidden), jnp.bfloat16)],
        name="expert_ffn",
    )(x, *gates, *downs)


def combine_kernel(keys_ref, weights_ref, rows_ref, out_ref):
    experts, groups, capacity, width = rows_ref.shape
    tokens, picks = keys_ref.shape
    slots = experts * capacity
    column = lax.broadcasted_iota(jnp.int32, (tokens, slots), 1)
    spread = jnp.zeros((tokens, slots), jnp.float32)
    for k in range(picks):
        spread = jnp.where(column == keys_ref[:, k : k + 1], weights_ref[:, k : k + 1], spread)
    high = spread.astype(jnp.bfloat16)
    low = (spread - high.astype(jnp.float32)).astype(jnp.bfloat16)
    total = jnp.zeros((tokens, width), jnp.float32)
    for g in range(groups):
        rows = rows_ref[:, g].reshape(slots, width)
        total = total + jnp.dot(high, rows, preferred_element_type=jnp.float32)
        total = total + jnp.dot(low, rows, preferred_element_type=jnp.float32)
    out_ref[...] = total.astype(jnp.bfloat16)


def combined(keys, weights, rows):
    return pl.pallas_call(
        combine_kernel,
        out_shape=jax.ShapeDtypeStruct((keys.shape[0], rows.shape[-1]), jnp.bfloat16),
        in_specs=[VM] * 3,
        out_specs=VM,
        name="combine",
    )(keys, weights, rows)


def on_device(
    mixer_rows,
    mixer_gain,
    inner_weight,
    gate_in_weight,
    gate_out_weight,
    conv_taps,
    mixer_out_weight,
    routed_rows,
    routed_gain,
    route_ids,
    route_weights,
    expert_gate,
    expert_up,
    expert_down,
):
    experts = lax.axis_size("ep")
    groups = lax.axis_size("p")
    parts = lax.axis_size(TP)
    sharers = lax.axis_size(("q", "c"))
    quarter = lax.axis_index(("q", "c"))
    tok_count, pick_count = route_ids.shape
    width = routed_rows.shape[1]
    capacity = 2 * tok_count * pick_count // experts
    share = capacity // sharers
    piece = width // parts

    gate_up = jnp.concatenate([expert_gate[0], expert_up[0]], axis=0)
    down = expert_down[0]
    gate_up_q = flipped(gate_up, "q")
    down_q = flipped(down, "q")
    gate_up_c = flipped(gate_up, "c")
    down_c = flipped(down, "c")
    gate_up_qc = flipped(gate_up_q, "c")
    down_qc = flipped(down_q, "c")

    flat_ids = route_ids.reshape(-1)
    choices = tok_count * pick_count
    onehot = flat_ids[:, None] == jnp.arange(experts, dtype=jnp.int32)[None, :]
    before = jnp.arange(choices)[:, None] > jnp.arange(choices)[None, :]
    earlier = jnp.dot(
        before.astype(jnp.bfloat16), onehot.astype(jnp.bfloat16), preferred_element_type=jnp.float32
    )
    slot_rank = jnp.sum(jnp.where(onehot, earlier, 0.0), axis=1).astype(jnp.int32)
    keys = (flat_ids * capacity + slot_rank).reshape(tok_count, pick_count)

    routed_normed = rms_scale(routed_rows, routed_gain)
    slot_of_row = jnp.arange(experts * share, dtype=jnp.int32)
    slot_of_row = slot_of_row // share * capacity + quarter * share + slot_of_row % share
    pick = jnp.any(keys.T[:, None, :] == slot_of_row[None, :, None], axis=0)
    outgoing = jnp.dot(
        pick.astype(jnp.bfloat16), routed_normed, preferred_element_type=jnp.float32
    ).astype(jnp.bfloat16)
    slot_rows = lax.all_to_all(
        outgoing.reshape(experts, share, width), "ep", split_axis=0, concat_axis=0, tiled=True
    ).reshape(experts * share, width)

    normed = rms_scale(mixer_rows, mixer_gain)
    inner_proj = jnp.dot(normed, inner_weight, preferred_element_type=jnp.float32)
    gate_in = jnp.dot(normed, gate_in_weight, preferred_element_type=jnp.float32)
    conv_input = (gate_in * inner_proj).astype(jnp.bfloat16)
    gate_out = jnp.dot(normed, gate_out_weight, preferred_element_type=jnp.float32)
    tap_total = conv_taps.shape[0]
    length = conv_input.shape[0]
    earlier_rows = lax.ppermute(
        conv_input[length - (tap_total - 1) :], "ep", [(i, i + 1) for i in range(experts - 1)]
    )
    extended = jnp.concatenate([earlier_rows, conv_input], axis=0).astype(jnp.float32)
    conv_out = jnp.zeros(conv_input.shape, jnp.float32)
    for tap_index in range(tap_total):
        conv_out = conv_out + conv_taps[tap_index] * extended[tap_index : tap_index + length]
    gated_conv = (gate_out * conv_out).astype(jnp.bfloat16)
    mixer_terms = jnp.dot(gated_conv, mixer_out_weight, preferred_element_type=jnp.float32).astype(jnp.bfloat16)
    mixer_parts = lax.all_to_all(
        mixer_terms.reshape(length, parts, piece).transpose(1, 0, 2), TP, split_axis=0, concat_axis=0, tiled=True
    )
    mixer_piece = jnp.sum(mixer_parts.astype(jnp.float32), axis=0).astype(jnp.bfloat16)

    results = expert_ffn(
        slot_rows,
        (gate_up, gate_up_c, gate_up_q, gate_up_qc),
        (down, down_c, down_q, down_qc),
    )
    back = results.reshape(experts, share, parts, piece).transpose(0, 2, 1, 3)
    back = lax.all_to_all(
        back.reshape(experts * parts, share, piece), ALL, split_axis=0, concat_axis=0, tiled=True
    )
    routed_piece = combined(keys, route_weights, back.reshape(experts, groups, capacity, piece))

    pieces = jnp.concatenate([mixer_piece, routed_piece], axis=0)
    mine = lax.all_gather(pieces, ("p", "q"), axis=0, tiled=False)
    other = flipped(mine, "c")
    core = lax.axis_index("c")
    even = jnp.where(core == 0, mine, other)
    odd = jnp.where(core == 0, other, mine)
    whole = jnp.stack([even, odd], axis=1).reshape(parts, length + tok_count, piece)
    whole = whole.transpose(1, 0, 2).reshape(length + tok_count, width)
    return whole[:length], whole[length:]


def solution(mesh):
    experts, parts = mesh.devices.shape
    finer = Mesh(mesh.devices.reshape(experts, parts // 4, 2, 2), ALL)
    return jax.shard_map(
        on_device,
        mesh=finer,
        in_specs=(
            P("ep", None),
            P(),
            P(None, TP),
            P(None, TP),
            P(None, TP),
            P(None, TP),
            P(TP, None),
            P("ep", None),
            P(),
            P("ep", None),
            P("ep", None),
            P("ep", None, TP),
            P("ep", None, TP),
            P("ep", TP, None),
        ),
        out_specs=(P("ep", None), P("ep", None)),
        check_vma=False,
    )
```

time: 322 us -> 167 us (0.52)
  waiting for transfers between devices: 223 us -> 51.9 us
  starting transfers between devices: 12.5 us -> 64.8 us
  between operations: 14.1 us -> 1.05 us
  other arithmetic: 16.3 us -> 3.78 us
  Pallas kernels: 0 us -> 11 us
  matrix products: 13.6 us -> 4.43 us
  local copies, waits for them, and re-layouts: 16.8 us -> 8.46 us
  blocking collectives: 24.8 us -> 20.4 us
    psum x1 -> x0, waiting for transfers between devices: 117 us -> none  [packed_total(): so_far = lax.psum(jnp.concatenate([a.ravel() for a in arrays]), axis)]
    reduce_scatter x1 -> x0, waiting for transfers between devices: 56.6 us -> none  [on_device(): lax.psum_scatter(jnp.dot(hidden, expert_down[0], preferred_element_type=j...]
    all_gather x1 -> x0, waiting for transfers between devices: 42.1 us -> none  [on_device(): incoming = lax.all_gather(arrived, 'tp', axis=0, tiled=True)]
    all_to_all x1 -> x3, waiting for transfers between devices: 8.08 us -> 35.6 us  [the longest x1 32.7 us: on_device(): lax.all_to_all(back.reshape(experts * parts, share, piece), ALL, split_ax...]
    all_to_all x1 -> x3, starting transfers between devices: 9.09 us -> 35.6 us  [the longest x1 14.5 us: on_device(): lax.all_to_all(back.reshape(experts * parts, share, piece), ALL, split_ax...]
    ppermute x1 -> x8, starting transfers between devices: 3.08 us -> 29.2 us  [the longest x7 25.8 us: flipped(): return lax.ppermute(value, axis, [(0, 1), (1, 0)])]
    all_to_all x1 -> x0, blocking collectives: 24.8 us -> none  [on_device(): lax.all_to_all(outgoing, 'ep', split_axis=1, concat_axis=1, tiled=True)]
    all_gather x0 -> x1, blocking collectives: none -> 20.4 us  [on_device(): mine = lax.all_gather(pieces, ('p', 'q'), axis=0, tiled=False)]
  transfers between devices with their start and end apart: 5 -> 11, of which waited for: 4 -> 6; matrix products, arithmetic and copies ran while one was open for 2% -> 4% of each run, Pallas kernels for 0% -> 5%
where the time goes in v1:
time: 167 us; the launch traced here: 166 us
  starting transfers between devices  64.8 us (39%)
  waiting for transfers between devices  51.9 us (31%)
  blocking collectives  20.4 us (12%)
  Pallas kernels  11 us (7%)
  local copies, waits for them, and re-layouts  8.46 us (5%)
  matrix products  4.43 us (3%)
  other arithmetic  3.78 us (2%)
    all_to_all x1, waiting for transfers between devices, on_device(): lax.all_to_all(back.reshape(experts * parts, share, piece), ALL, split_ax...  32.7 us
    ppermute x7, starting transfers between devices, flipped(): return lax.ppermute(value, axis, [(0, 1), (1, 0)])  25.8 us
    all_gather x1, blocking collectives, on_device(): mine = lax.all_gather(pieces, ('p', 'q'), axis=0, tiled=False)  20.4 us
    ppermute x7, waiting for transfers between devices, flipped(): return lax.ppermute(value, axis, [(0, 1), (1, 0)])  15.5 us
    all_to_all x1, starting transfers between devices, on_device(): lax.all_to_all(back.reshape(experts * parts, share, piece), ALL, split_ax...  14.5 us
    all_to_all x1, starting transfers between devices, on_device(): lax.all_to_all(outgoing.reshape(experts, share, width), 'ep', split_axis=...  13.8 us
    pallas_call x1, Pallas kernels, expert_ffn(): pl.pallas_call(ffn_kernel, out_shape=jax.ShapeDtypeStruct(x.shape, jnp.bf...  7.47 us
    all_to_all x1, starting transfers between devices, on_device(): lax.all_to_all(mixer_terms.reshape(length, parts, piece).transpose(1, 0,...  7.22 us
  transfers between devices with their start and end apart: 11, of which 6 were waited for; matrix products, arithmetic and copies ran while one was open for 4% of the time, Pallas kernels for 5%

profile of v1, /device:TPU:1, one launch (start us, length us, event | category | flops | bytes accessed | tf_op | source)
XLA Modules:
  0.0 165.8 jit_solution(1763237092744963262)
XLA Ops:
  0.7 0.9 copy.59
  1.6 0.7 broadcast_multiply_fusion
  3.6 1.5 fusion
  5.1 13.8 %all-to-all-start.1 = ((bf16[32,8,2048]{2,1,0:T(8,128)(2,1)}), bf16[32,8,2048]{2,1,0:T(8,128)(2,1)S(1)}, u32[]{:S(2)}, u32[]{:S(2)}) async-start(bf16[32,8,2048]{2,1,0:T(8,128)(2,1)} %fusion), calls=%async_computation.1 | async-start | bytes 2097152 | tf_op jit(solution)/shard_map/all_to_all | solution.py:139
  19.0 1.2 pad_maximum_fusion.1.a0
  20.2 3.3 %collective-permute-start.2 = (bf16[4096,128]{1,0:T(8,128)(2,1)S(1)}, bf16[4096,128]{1,0:T(8,128)(2,1)}, u32[]{:S(2)}, u32[]{:S(2)}) collective-permute-start(bf16[4096,128]{1,0:T(8,128)(2,1)S(1)} %pad_maximum_fusion.1.a0), channel_id=1, source_target_pairs={{0,2},{2,0},{1,3},{3,1},{4,6},{6,4},{5,7},{7,5},{8,10},{10,8},{9,1... | collective-permute-start | bytes 3145736 | tf_op jit(solution)/shard_map/ppermute | solution.py:22
  23.6 3.1 %collective-permute-start.1 = (bf16[4096,128]{1,0:T(8,128)(2,1)S(1)}, bf16[4096,128]{1,0:T(8,128)(2,1)}, u32[]{:S(2)}, u32[]{:S(2)}) collective-permute-start(bf16[4096,128]{1,0:T(8,128)(2,1)S(1)} %pad_maximum_fusion.1.a0), channel_id=1, source_target_pairs={{0,1},{1,0},{2,3},{3,2},{4,5},{5,4},{6,7},{7,6},{8,9},{9,8},{10,11... | collective-permute-start | bytes 3145736 | tf_op jit(solution)/shard_map/ppermute | solution.py:22
  26.7 2.1 %collective-permute-start.5 = (bf16[128,2048]{1,0:T(8,128)(2,1)}, bf16[128,2048]{1,0:T(8,128)(2,1)}, u32[]{:S(2)}, u32[]{:S(2)}) collective-permute-start(bf16[128,2048]{1,0:T(8,128)(2,1)} %bitcast.9.d0), channel_id=1, source_target_pairs={{0,2},{2,0},{1,3},{3,1},{4,6},{6,4},{5,7},{7,5},{8,10},{10,8},{9,1... | collective-permute-start | bytes 1572872 | tf_op jit(solution)/shard_map/ppermute | solution.py:22
  29.9 3.4 %collective-permute-start = (bf16[2,64]{0,1:T(8,128)(2,1)S(1)}, bf16[2,64]{0,1:T(8,128)(2,1)S(1)}, u32[]{:S(2)}, u32[]{:S(2)}) collective-permute-start(bf16[2,64]{0,1:T(8,128)(2,1)S(1)} %slice.44), channel_id=1, source_target_pairs={{0,16},{16,32},{32,48},{48,64},{64,80},{80,96},{96,112},{112,128},... | collective-permute-start | bytes 776 | tf_op jit(solution)/shard_map/ppermute | solution.py:150
  33.3 0.8 collective-permute-done
  34.2 11.9 %collective-permute-done.2.a2 = bf16[4096,128]{1,0:T(8,128)(2,1)} collective-permute-done((bf16[4096,128]{1,0:T(8,128)(2,1)S(1)}, bf16[4096,128]{1,0:T(8,128)(2,1)}, u32[]{:S(2)}, u32[]{:S(2)}) %collective-permute-start.2) | collective-permute-done | bytes 1048608 | tf_op jit(solution)/shard_map/ppermute | solution.py:22
  46.1 5.1 %collective-permute-start.3 = (bf16[4096,128]{1,0:T(8,128)(2,1)}, bf16[4096,128]{1,0:T(8,128)(2,1)}, u32[]{:S(2)}, u32[]{:S(2)}) collective-permute-start(bf16[4096,128]{1,0:T(8,128)(2,1)} %collective-permute-done.2.a2), channel_id=1, source_target_pairs={{0,1},{1,0},{2,3},{3,2},{4,5},{5,4},{6,7},{7,6},{8,9},{9,8},{10,11... | collective-permute-start | bytes 3145736 | tf_op jit(solution)/shard_map/ppermute | solution.py:22
  51.3 1.9 %fusion.4 = bf16[16,16,8,128]{3,2,1,0:T(8,128)(2,1)S(1)} fusion(bf16[64,2048]{1,0:T(8,128)(2,1)S(1)} %copy-done, bf16[2048,64]{0,1:T(8,128)(2,1)} %param.18, f32[130,64]{0,1:T(8,128)S(1)} %maximum_convert_fusion, f32[64]{0:T(128)S(1)} %get-tuple-element.13, f32[64]{0:T(128)S(1)} %get-tuple-element.14, f32[64]{0:T(128)S(1)} %get-tuple-element.12, ...), kind=kOutput, calls=%fused_computation.11 | convolution fusion | flops 68476928 | bytes 1681408 | tf_op jit(solution)/shard_map/dot_general | solution.py:158
  53.1 1.0 copy.70
  54.1 7.2 %all-to-all-start = ((bf16[16,128,128]{2,1,0:T(8,128)(2,1)}), bf16[16,128,128]{2,1,0:T(8,128)(2,1)S(1)}, u32[]{:S(2)}, u32[]{:S(2)}) async-start(bf16[16,128,128]{2,1,0:T(8,128)(2,1)} %bitcast.43), calls=%async_computation | async-start | bytes 1048576 | tf_op jit(solution)/shard_map/all_to_all | solution.py:159
  61.3 2.0 %collective-permute-start.4 = (bf16[128,2048]{1,0:T(8,128)(2,1)}, bf16[128,2048]{1,0:T(8,128)(2,1)S(1)}, u32[]{:S(2)}, u32[]{:S(2)}) collective-permute-start(bf16[128,2048]{1,0:T(8,128)(2,1)} %bitcast.9.d0), channel_id=1, source_target_pairs={{0,1},{1,0},{2,3},{3,2},{4,5},{5,4},{6,7},{7,6},{8,9},{9,8},{10,11... | collective-permute-start | bytes 1572872 | tf_op jit(solution)/shard_map/ppermute | solution.py:22
  63.4 2.3 %collective-permute-start.6 = (bf16[128,2048]{1,0:T(8,128)(2,1)}, bf16[128,2048]{1,0:T(8,128)(2,1)S(1)}, u32[]{:S(2)}, u32[]{:S(2)}) collective-permute-start(bf16[128,2048]{1,0:T(8,128)(2,1)} %collective-permute-done.5.d2), channel_id=1, source_target_pairs={{0,1},{1,0},{2,3},{3,2},{4,5},{5,4},{6,7},{7,6},{8,9},{9,8},{10,11... | collective-permute-start | bytes 1572872 | tf_op jit(solution)/shard_map/ppermute | solution.py:22
  65.7 1.7 %collective-permute-done.6.d3 = bf16[128,2048]{1,0:T(8,128)(2,1)S(1)} collective-permute-done((bf16[128,2048]{1,0:T(8,128)(2,1)}, bf16[128,2048]{1,0:T(8,128)(2,1)S(1)}, u32[]{:S(2)}, u32[]{:S(2)}) %collective-permute-start.6) | collective-permute-done | bytes 524320 | tf_op jit(solution)/shard_map/ppermute | solution.py:22
  67.4 0.8 copy-done.8
  68.2 7.5 %expert_ffn.1 = bf16[256,2048]{1,0:T(8,128)(2,1)} custom-call(bf16[256,2048]{1,0:T(8,128)(2,1)} %bitcast.48, bf16[4096,128]{1,0:T(8,128)(2,1)} %copy-done.4, bf16[4096,128]{1,0:T(8,128)(2,1)} %collective-permute-done.1.a1, bf16[4096,128]{1,0:T(8,128)(2,1)} %collective-permute-done.2.a2, bf16[4096,128]{1,0:T(8,128)(2,1)} %collective-permute-done.3.a3, ...), custom_call_target="tpu_custom_call" | custom-call | tf_op jit(solution)/shard_map/expert_ffn/pallas_call | solution.py:48
  75.7 2.8 %all-to-all-done = bf16[16,128,128]{2,1,0:T(8,128)(2,1)S(1)} async-done(((bf16[16,128,128]{2,1,0:T(8,128)(2,1)}), bf16[16,128,128]{2,1,0:T(8,128)(2,1)S(1)}, u32[]{:S(2)}, u32[]{:S(2)}) %all-to-all-start) | async-done | bytes 524320 | tf_op jit(solution)/shard_map/all_to_all | solution.py:159
  78.5 14.5 %all-to-all-start.2 = ((bf16[512,8,128]{2,1,0:T(8,128)(2,1)}), bf16[512,8,128]{2,1,0:T(8,128)(2,1)S(1)}, u32[]{:S(2)}, u32[]{:S(2)}) async-start(bf16[512,8,128]{2,1,0:T(8,128)(2,1)} %bitcast.49), calls=%async_computation.2 | async-start | bytes 2097152 | tf_op jit(solution)/shard_map/all_to_all | solution.py:170
  93.1 0.8 copy.62.weights_ref
  94.0 32.7 %all-to-all-done.2 = bf16[512,8,128]{2,1,0:T(8,128)(2,1)S(1)} async-done(((bf16[512,8,128]{2,1,0:T(8,128)(2,1)}), bf16[512,8,128]{2,1,0:T(8,128)(2,1)S(1)}, u32[]{:S(2)}, u32[]{:S(2)}) %all-to-all-start.2) | async-done | bytes 1048608 | tf_op jit(solution)/shard_map/all_to_all | solution.py:170
  126.7 1.0 copy-done.2
  127.7 3.5 %combine.1 = bf16[256,128]{1,0:T(8,128)(2,1)} custom-call(s32[256,2]{1,0:T(8,128)} %copy-done.6, f32[256,2]{1,0:T(8,128)} %copy.62.weights_ref, bf16[32,4,32,128]{3,2,1,0:T(8,128)(2,1)} %bitcast.46), custom_call_target="tpu_custom_call" | custom-call | tf_op jit(solution)/shard_map/combine/pallas_call | solution.py:77
  131.2 0.8 pad_maximum_fusion.2
  132.1 20.4 %all-gather = bf16[3072,128]{1,0:T(8,128)(2,1)S(1)} all-gather(bf16[384,128]{1,0:T(8,128)(2,1)S(1)} %pad_maximum_fusion.2), channel_id=2, replica_groups=mesh['ep'=32,'p'=4,'q'=2,'c'=2] {'p','q'}, dimensions={0}, use_global_device_ids=true | all-gather | bytes 884736 | tf_op jit(solution)/shard_map/all_gather | solution.py:176
  152.5 7.8 %collective-permute-start.7 = (bf16[8,384,128]{2,1,0:T(8,128)(2,1)S(1)}, bf16[8,384,128]{2,1,0:T(8,128)(2,1)S(1)}, u32[]{:S(2)}, u32[]{:S(2)}) collective-permute-start(bf16[8,384,128]{2,1,0:T(8,128)(2,1)S(1)} %bitcast.50), channel_id=1, source_target_pairs={{0,1},{1,0},{2,3},{3,2},{4,5},{5,4},{6,7},{7,6},{8,9},{9,8},{10,11... | collective-permute-start | bytes 2359304 | tf_op jit(solution)/shard_map/ppermute | solution.py:22
  160.2 1.9 %collective-permute-done.7 = bf16[8,384,128]{2,1,0:T(8,128)(2,1)S(1)} collective-permute-done((bf16[8,384,128]{2,1,0:T(8,128)(2,1)S(1)}, bf16[8,384,128]{2,1,0:T(8,128)(2,1)S(1)}, u32[]{:S(2)}, u32[]{:S(2)}) %collective-permute-start.7) | collective-permute-done | bytes 786464 | tf_op jit(solution)/shard_map/ppermute | solution.py:22
  163.1 1.4 copy.67
  164.8 1.0 copy.66
  (60 shorter events, 3.7 us)
Async XLA Ops:
  0.6 50.6 %copy-start = (bf16[64,2048]{1,0:T(8,128)(2,1)S(1)}, bf16[64,2048]{1,0:T(8,128)(2,1)}, u32[]{:S(2)}) copy-start(bf16[64,2048]{1,0:T(8,128)(2,1)} %param.20) | copy-start | bytes 786436
  0.6 2.5 %copy-start.1 = (bf16[256,2048]{1,0:T(8,128)(2,1)S(1)}, bf16[256,2048]{1,0:T(8,128)(2,1)}, u32[]{:S(2)}) copy-start(bf16[256,2048]{1,0:T(8,128)(2,1)} %param.21) | copy-start | bytes 3145732
  0.7 2.9 %copy-start.10 = (f32[2048]{0:T(1024)S(1)}, f32[2048]{0:T(1024)}, u32[]{:S(2)}) copy-start(f32[2048]{0:T(1024)} %param.22) | copy-start | bytes 24580
  3.0 2.1 %copy-start.6 = (s32[256,2]{1,0:T(8,128)}, s32[256,2]{1,0:T(8,128)S(1)}, u32[]{:S(2)}) copy-start(s32[256,2]{1,0:T(8,128)S(1)} %add.71.keys_ref) | copy-start | bytes 6148
  5.1 13.9 %copy-start.9 = (bf16[1,2048,128]{2,1,0:T(8,128)(2,1)S(1)}, bf16[1,2048,128]{2,1,0:T(8,128)(2,1)}, u32[]{:S(2)}) copy-start(bf16[1,2048,128]{2,1,0:T(8,128)(2,1)} %param.26) | copy-start | bytes 1572868
  5.1 49.0 %all-to-all-start.1 = ((bf16[32,8,2048]{2,1,0:T(8,128)(2,1)}), bf16[32,8,2048]{2,1,0:T(8,128)(2,1)S(1)}, u32[]{:S(2)}, u32[]{:S(2)}) async-start(bf16[32,8,2048]{2,1,0:T(8,128)(2,1)} %fusion), calls=%async_computation.1 | async-start | bytes 2097152 | tf_op jit(solution)/shard_map/all_to_all | solution.py:139
  18.9 9.9 %copy-start.5 = (bf16[128,2048]{1,0:T(8,128)(2,1)S(1)}, bf16[128,2048]{1,0:T(8,128)(2,1)}, u32[]{:S(2)}) copy-start(bf16[128,2048]{1,0:T(8,128)(2,1)} %param.14) | copy-start | bytes 1572868
  19.0 10.1 %copy-start.11 = (f32[2048]{0:T(1024)S(1)}, f32[2048]{0:T(1024)}, u32[]{:S(2)}) copy-start(f32[2048]{0:T(1024)} %param.15) | copy-start | bytes 24580
  19.0 10.1 %copy-start.14 = (bf16[2048,64]{0,1:T(8,128)(2,1)S(1)}, bf16[2048,64]{0,1:T(8,128)(2,1)}, u32[]{:S(2)}) copy-start(bf16[2048,64]{0,1:T(8,128)(2,1)} %param.17) | copy-start | bytes 786436
  19.0 10.4 %copy-start.15 = (bf16[2048,64]{0,1:T(8,128)(2,1)S(1)}, bf16[2048,64]{0,1:T(8,128)(2,1)}, u32[]{:S(2)}) copy-start(bf16[2048,64]{0,1:T(8,128)(2,1)} %param.16) | copy-start | bytes 786436
  20.2 32.9 %copy-start.4 = (bf16[4096,128]{1,0:T(8,128)(2,1)}, bf16[4096,128]{1,0:T(8,128)(2,1)S(1)}, u32[]{:S(2)}) copy-start(bf16[4096,128]{1,0:T(8,128)(2,1)S(1)} %pad_maximum_fusion.1.a0) | copy-start | bytes 3145732
  20.2 13.1 %copy-start.13 = (f32[3,64]{1,0:T(4,128)S(1)}, f32[3,64]{1,0:T(4,128)}, u32[]{:S(2)}) copy-start(f32[3,64]{1,0:T(4,128)} %param.19) | copy-start | bytes 2308
  20.2 25.9 %collective-permute-start.2 = (bf16[4096,128]{1,0:T(8,128)(2,1)S(1)}, bf16[4096,128]{1,0:T(8,128)(2,1)}, u32[]{:S(2)}, u32[]{:S(2)}) collective-permute-start(bf16[4096,128]{1,0:T(8,128)(2,1)S(1)} %pad_maximum_fusion.1.a0), channel_id=1, source_target_pairs={{0,2},{2,0},{1,3},{3,1},{4,6},{6,4},{5,7},{7,5},{8,10},{10,8},{9,1... | collective-permute-start | bytes 3145736 | tf_op jit(solution)/shard_map/ppermute | solution.py:22
  23.6 43.9 %collective-permute-start.1 = (bf16[4096,128]{1,0:T(8,128)(2,1)S(1)}, bf16[4096,128]{1,0:T(8,128)(2,1)}, u32[]{:S(2)}, u32[]{:S(2)}) collective-permute-start(bf16[4096,128]{1,0:T(8,128)(2,1)S(1)} %pad_maximum_fusion.1.a0), channel_id=1, source_target_pairs={{0,1},{1,0},{2,3},{3,2},{4,5},{5,4},{6,7},{7,6},{8,9},{9,8},{10,11... | collective-permute-start | bytes 3145736 | tf_op jit(solution)/shard_map/ppermute | solution.py:22
  26.7 36.7 %collective-permute-start.5 = (bf16[128,2048]{1,0:T(8,128)(2,1)}, bf16[128,2048]{1,0:T(8,128)(2,1)}, u32[]{:S(2)}, u32[]{:S(2)}) collective-permute-start(bf16[128,2048]{1,0:T(8,128)(2,1)} %bitcast.9.d0), channel_id=1, source_target_pairs={{0,2},{2,0},{1,3},{3,1},{4,6},{6,4},{5,7},{7,5},{8,10},{10,8},{9,1... | collective-permute-start | bytes 1572872 | tf_op jit(solution)/shard_map/ppermute | solution.py:22
  29.9 4.3 %collective-permute-start = (bf16[2,64]{0,1:T(8,128)(2,1)S(1)}, bf16[2,64]{0,1:T(8,128)(2,1)S(1)}, u32[]{:S(2)}, u32[]{:S(2)}) collective-permute-start(bf16[2,64]{0,1:T(8,128)(2,1)S(1)} %slice.44), channel_id=1, source_target_pairs={{0,16},{16,32},{32,48},{48,64},{64,80},{80,96},{96,112},{112,128},... | collective-permute-start | bytes 776 | tf_op jit(solution)/shard_map/ppermute | solution.py:150
  46.1 22.1 %collective-permute-start.3 = (bf16[4096,128]{1,0:T(8,128)(2,1)}, bf16[4096,128]{1,0:T(8,128)(2,1)}, u32[]{:S(2)}, u32[]{:S(2)}) collective-permute-start(bf16[4096,128]{1,0:T(8,128)(2,1)} %collective-permute-done.2.a2), channel_id=1, source_target_pairs={{0,1},{1,0},{2,3},{3,2},{4,5},{5,4},{6,7},{7,6},{8,9},{9,8},{10,11... | collective-permute-start | bytes 3145736 | tf_op jit(solution)/shard_map/ppermute | solution.py:22
  54.1 14.1 %copy-start.3 = (bf16[32,8,2048]{2,1,0:T(8,128)(2,1)}, bf16[32,8,2048]{2,1,0:T(8,128)(2,1)S(1)}, u32[]{:S(2)}) copy-start(bf16[32,8,2048]{2,1,0:T(8,128)(2,1)S(1)} %all-to-all-done.1) | copy-start | bytes 3145732
  54.1 24.4 %all-to-all-start = ((bf16[16,128,128]{2,1,0:T(8,128)(2,1)}), bf16[16,128,128]{2,1,0:T(8,128)(2,1)S(1)}, u32[]{:S(2)}, u32[]{:S(2)}) async-start(bf16[16,128,128]{2,1,0:T(8,128)(2,1)} %bitcast.43), calls=%async_computation | async-start | bytes 1048576 | tf_op jit(solution)/shard_map/all_to_all | solution.py:159
  61.3 4.3 %collective-permute-start.4 = (bf16[128,2048]{1,0:T(8,128)(2,1)}, bf16[128,2048]{1,0:T(8,128)(2,1)S(1)}, u32[]{:S(2)}, u32[]{:S(2)}) collective-permute-start(bf16[128,2048]{1,0:T(8,128)(2,1)} %bitcast.9.d0), channel_id=1, source_target_pairs={{0,1},{1,0},{2,3},{3,2},{4,5},{5,4},{6,7},{7,6},{8,9},{9,8},{10,11... | collective-permute-start | bytes 1572872 | tf_op jit(solution)/shard_map/ppermute | solution.py:22
  63.4 4.0 %collective-permute-start.6 = (bf16[128,2048]{1,0:T(8,128)(2,1)}, bf16[128,2048]{1,0:T(8,128)(2,1)S(1)}, u32[]{:S(2)}, u32[]{:S(2)}) collective-permute-start(bf16[128,2048]{1,0:T(8,128)(2,1)} %collective-permute-done.5.d2), channel_id=1, source_target_pairs={{0,1},{1,0},{2,3},{3,2},{4,5},{5,4},{6,7},{7,6},{8,9},{9,8},{10,11... | collective-permute-start | bytes 1572872 | tf_op jit(solution)/shard_map/ppermute | solution.py:22
  65.7 2.5 %copy-start.7 = (bf16[128,2048]{1,0:T(8,128)(2,1)}, bf16[128,2048]{1,0:T(8,128)(2,1)S(1)}, u32[]{:S(2)}) copy-start(bf16[128,2048]{1,0:T(8,128)(2,1)S(1)} %collective-permute-done.4.d1) | copy-start | bytes 1572868
  67.4 0.8 copy-start.8
  75.7 17.4 %copy-start.12 = (f32[256,2]{0,1:T(2,128)S(1)}, f32[256,2]{0,1:T(2,128)}, u32[]{:S(2)}) copy-start(f32[256,2]{0,1:T(2,128)} %param.24) | copy-start | bytes 6148
  78.5 48.2 %all-to-all-start.2 = ((bf16[512,8,128]{2,1,0:T(8,128)(2,1)}), bf16[512,8,128]{2,1,0:T(8,128)(2,1)S(1)}, u32[]{:S(2)}, u32[]{:S(2)}) async-start(bf16[512,8,128]{2,1,0:T(8,128)(2,1)} %bitcast.49), calls=%async_computation.2 | async-start | bytes 2097152 | tf_op jit(solution)/shard_map/all_to_all | solution.py:170
  126.7 1.0 copy-start.2
  152.5 9.7 %collective-permute-start.7 = (bf16[8,384,128]{2,1,0:T(8,128)(2,1)S(1)}, bf16[8,384,128]{2,1,0:T(8,128)(2,1)S(1)}, u32[]{:S(2)}, u32[]{:S(2)}) collective-permute-start(bf16[8,384,128]{2,1,0:T(8,128)(2,1)S(1)} %bitcast.50), channel_id=1, source_target_pairs={{0,1},{1,0},{2,3},{3,2},{4,5},{5,4},{6,7},{7,6},{8,9},{9,8},{10,11... | collective-permute-start | bytes 2359304 | tf_op jit(solution)/shard_map/ppermute | solution.py:22

commit v2 on v1

v2 whole, which is shorter than its diff:
```python
import functools

import jax
import jax.numpy as jnp
from jax import lax
from jax.experimental import pallas as pl
from jax.experimental.pallas import tpu as pltpu
from jax.sharding import Mesh, PartitionSpec as P

TP = ("p", "q", "c")
ALL = ("ep", "p", "q", "c")
VM = pl.BlockSpec(memory_space=pltpu.VMEM)


def rms_scale(row_block, gain_row):
    values = row_block.astype(jnp.float32)
    scaled = values * lax.rsqrt(jnp.mean(values * values, axis=-1, keepdims=True) + 1e-06)
    return (scaled * gain_row).astype(jnp.bfloat16)


def flipped(value, axis):
    return lax.ppermute(value, axis, [(0, 1), (1, 0)])


def route_kernel(quarter_ref, ids_ref, rows_ref, gain_ref, out_ref, keys_ref, *, capacity, share):
    tokens, picks = ids_ref.shape
    slots = out_ref.shape[0]
    lane = lax.broadcasted_iota(jnp.int32, (tokens, 128), 1)
    named = [ids_ref[:, k : k + 1] == lane for k in range(picks)]
    both = functools.reduce(jnp.logical_or, named)
    row = lax.broadcasted_iota(jnp.int32, (tokens, tokens), 0)
    col = lax.broadcasted_iota(jnp.int32, (tokens, tokens), 1)
    earlier = jnp.dot(
        jnp.where(row > col, 1.0, 0.0).astype(jnp.bfloat16),
        jnp.where(both, 1.0, 0.0).astype(jnp.bfloat16),
        preferred_element_type=jnp.float32,
    )
    slot = lax.broadcasted_iota(jnp.int32, (tokens, slots), 1)
    slot_key = slot // share * capacity + slot % share + quarter_ref[0] * share
    chosen = None
    for k in range(picks):
        rank = jnp.sum(jnp.where(named[k], earlier, 0.0), axis=1, keepdims=True).astype(jnp.int32)
        key = ids_ref[:, k : k + 1] * capacity + rank
        keys_ref[:, k : k + 1] = key
        here = key == slot_key
        chosen = here if chosen is None else jnp.logical_or(chosen, here)
    values = rows_ref[...].astype(jnp.float32)
    scaled = values * lax.rsqrt(jnp.mean(values * values, axis=-1, keepdims=True) + 1e-06)
    normed = (scaled * gain_ref[...]).astype(jnp.bfloat16)
    out_ref[...] = lax.dot_general(
        jnp.where(chosen, 1.0, 0.0).astype(jnp.bfloat16),
        normed,
        (((0,), (0,)), ((), ())),
        preferred_element_type=jnp.float32,
    ).astype(jnp.bfloat16)


def routed_slots(quarter, ids, rows, gain, experts, capacity, share):
    return pl.pallas_call(
        functools.partial(route_kernel, capacity=capacity, share=share),
        out_shape=(
            jax.ShapeDtypeStruct((experts * share, rows.shape[1]), jnp.bfloat16),
            jax.ShapeDtypeStruct(ids.shape, jnp.int32),
        ),
        in_specs=[pl.BlockSpec(memory_space=pltpu.SMEM), VM, VM, VM],
        out_specs=(VM, VM),
        name="route",
    )(quarter.reshape(1), ids, rows, gain.reshape(1, -1))


def halved(value, axis, first):
    middle = value.shape[1] // 2
    left, right = value[:, :middle], value[:, middle:]
    received = flipped(jnp.where(first, right, left), axis)
    kept = jnp.where(first, left, right)
    return (kept.astype(jnp.float32) + received.astype(jnp.float32)).astype(jnp.bfloat16)


def ffn_kernel(x_hbm, a0, a1, a2, a3, b0, b1, b2, b3, out_ref, x_ref, gu_ref, down_ref, hid_ref, sems):
    width = x_ref.shape[1]
    part = a0.shape[1]
    lead = b0.shape[0] - part
    x_copy = pltpu.make_async_copy(x_hbm, x_ref, sems.at[0])
    x_copy.start()
    copies = []
    for i, (a, b) in enumerate(((a0, b0), (a1, b1), (a2, b2), (a3, b3))):
        gate = pltpu.make_async_copy(
            a.at[pl.ds(0, width), :], gu_ref.at[i, :, pl.ds(0, part)], sems.at[3 * i + 1]
        )
        up = pltpu.make_async_copy(
            a.at[pl.ds(width, width), :], gu_ref.at[i, :, pl.ds(part, part)], sems.at[3 * i + 2]
        )
        down = pltpu.make_async_copy(
            b.at[pl.ds(lead, part), :], down_ref.at[pl.ds(i * part, part), :], sems.at[3 * i + 3]
        )
        gate.start()
        up.start()
        copies.append((gate, up, down))
    for _, _, down in copies:
        down.start()
    x_copy.wait()
    for i, (gate, up, _) in enumerate(copies):
        gate.wait()
        up.wait()
        acts = jnp.dot(x_ref[...], gu_ref[i], preferred_element_type=jnp.float32)
        g = acts[:, :part]
        hid_ref[:, i * part : (i + 1) * part] = (g / (1.0 + jnp.exp(-g)) * acts[:, part:]).astype(jnp.bfloat16)
    for _, _, down in copies:
        down.wait()
    cols = 512
    for n in range(0, width, cols):
        out_ref[:, n : n + cols] = jnp.dot(
            hid_ref[...], down_ref[:, n : n + cols], preferred_element_type=jnp.float32
        ).astype(jnp.bfloat16)


def expert_ffn(x, packs, hidden):
    rows, width = x.shape
    part = packs[0].shape[1]
    hbm = pl.BlockSpec(memory_space=pltpu.HBM)
    views = [wide_view(w, width) for w in packs]
    return pl.pallas_call(
        ffn_kernel,
        out_shape=jax.ShapeDtypeStruct(x.shape, jnp.bfloat16),
        in_specs=[hbm] * 9,
        out_specs=VM,
        scratch_shapes=[
            pltpu.VMEM((rows, width), jnp.bfloat16),
            pltpu.VMEM((4, width, 2 * part), jnp.bfloat16),
            pltpu.VMEM((hidden, width), jnp.bfloat16),
            pltpu.VMEM((rows, hidden), jnp.bfloat16),
            pltpu.SemaphoreType.DMA((13,)),
        ],
        cost_estimate=pl.CostEstimate(
            flops=6 * rows * width * hidden, bytes_accessed=8 * 2**20, transcendentals=rows * hidden
        ),
        name="expert_ffn",
    )(x, *packs, *views)


def narrow_view(value, part):
    rows, width = value.shape
    return value.reshape(rows // 8, 8, width // part, part).transpose(0, 2, 1, 3).reshape(-1, part)


def wide_view(value, width):
    _, part = value.shape
    return value.reshape(-1, width // part, 8, part).transpose(0, 2, 1, 3).reshape(-1, width)


def combine_kernel(keys_ref, weights_ref, rows_ref, out_ref):
    experts, groups, capacity, width = rows_ref.shape
    tokens, picks = keys_ref.shape
    slots = experts * capacity
    column = lax.broadcasted_iota(jnp.int32, (tokens, slots), 1)
    spread = jnp.zeros((tokens, slots), jnp.float32)
    for k in range(picks):
        spread = jnp.where(column == keys_ref[:, k : k + 1], weights_ref[:, k : k + 1], spread)
    high = spread.astype(jnp.bfloat16)
    low = (spread - high.astype(jnp.float32)).astype(jnp.bfloat16)
    total = jnp.zeros((tokens, 2 * width), jnp.float32)
    for g in range(0, groups, 2):
        rows = jnp.concatenate(
            [rows_ref[:, g].reshape(slots, width), rows_ref[:, g + 1].reshape(slots, width)], axis=1
        )
        total = total + jnp.dot(high, rows, preferred_element_type=jnp.float32)
        total = total + jnp.dot(low, rows, preferred_element_type=jnp.float32)
    out_ref[...] = (total[:, :width] + total[:, width:]).astype(jnp.bfloat16)


def combined(keys, weights, rows):
    return pl.pallas_call(
        combine_kernel,
        out_shape=jax.ShapeDtypeStruct((keys.shape[0], rows.shape[-1]), jnp.bfloat16),
        in_specs=[VM] * 3,
        out_specs=VM,
        name="combine",
    )(keys, weights, rows)


def assemble_kernel(core_ref, mine_ref, other_ref, out_ref):
    count, _, piece = mine_ref.shape
    first = core_ref[0] == 0
    for i in range(count):
        mine, other = mine_ref[i], other_ref[i]
        at = 2 * i * piece
        out_ref[:, at : at + piece] = jnp.where(first, mine, other)
        out_ref[:, at + piece : at + 2 * piece] = jnp.where(first, other, mine)


def assembled(core, mine, other):
    count, rows, piece = mine.shape
    return pl.pallas_call(
        assemble_kernel,
        out_shape=jax.ShapeDtypeStruct((rows, 2 * count * piece), jnp.bfloat16),
        in_specs=[pl.BlockSpec(memory_space=pltpu.SMEM), VM, VM],
        out_specs=VM,
        name="assemble",
    )(core.reshape(1), mine, other)


def column_kernel(parts_ref, out_ref, *, places):
    width = parts_ref.shape[2]
    for i, place in enumerate(places):
        out_ref[:, place * width : (place + 1) * width] = parts_ref[i]


def side_by_side(parts, places):
    count, rows, width = parts.shape
    return pl.pallas_call(
        functools.partial(column_kernel, places=places),
        out_shape=jax.ShapeDtypeStruct((rows, count * width), parts.dtype),
        in_specs=[VM],
        out_specs=VM,
        name="side_by_side",
    )(parts)


def on_device(
    mixer_rows,
    mixer_gain,
    inner_weight,
    gate_in_weight,
    gate_out_weight,
    conv_taps,
    mixer_out_weight,
    routed_rows,
    routed_gain,
    route_ids,
    route_weights,
    expert_gate,
    expert_up,
    expert_down,
):
    experts = lax.axis_size("ep")
    groups = lax.axis_size("p")
    parts = lax.axis_size(TP)
    sharers = lax.axis_size(("q", "c"))
    quarter = lax.axis_index(("q", "c"))
    tok_count, pick_count = route_ids.shape
    width = routed_rows.shape[1]
    capacity = 2 * tok_count * pick_count // experts
    share = capacity // sharers
    piece = width // parts
    hidden_part = expert_gate.shape[2]

    pack = jnp.concatenate([expert_gate[0], expert_up[0], narrow_view(expert_down[0], hidden_part)], axis=0)
    pack_q = flipped(pack, "q")
    pack_c = flipped(pack, "c")
    pack_qc = flipped(pack_q, "c")

    outgoing, keys = routed_slots(quarter, route_ids, routed_rows, routed_gain, experts, capacity, share)
    slot_rows = lax.all_to_all(
        outgoing.reshape(experts, share, width), "ep", split_axis=0, concat_axis=0, tiled=True
    ).reshape(experts * share, width)

    normed = rms_scale(mixer_rows, mixer_gain)
    inner_proj = jnp.dot(normed, inner_weight, preferred_element_type=jnp.float32)
    gate_in = jnp.dot(normed, gate_in_weight, preferred_element_type=jnp.float32)
    conv_input = (gate_in * inner_proj).astype(jnp.bfloat16)
    gate_out = jnp.dot(normed, gate_out_weight, preferred_element_type=jnp.float32)
    tap_total = conv_taps.shape[0]
    length = conv_input.shape[0]
    earlier_rows = lax.ppermute(conv_input[length - (tap_total - 1) :], "ep", [(i, i + 1) for i in range(experts - 1)])
    extended = jnp.concatenate([earlier_rows, conv_input], axis=0).astype(jnp.float32)
    conv_out = jnp.zeros(conv_input.shape, jnp.float32)
    for tap_index in range(tap_total):
        conv_out = conv_out + conv_taps[tap_index] * extended[tap_index : tap_index + length]
    gated_conv = (gate_out * conv_out).astype(jnp.bfloat16)
    mixer_terms = jnp.dot(gated_conv, mixer_out_weight, preferred_element_type=jnp.float32).astype(jnp.bfloat16)
    core, side = lax.axis_index("c") == 0, lax.axis_index("q") == 0
    mixer_half = halved(mixer_terms, "c", core)
    mixer_quarter = halved(mixer_half, "q", side)

    results = expert_ffn(slot_rows, (pack, pack_c, pack_q, pack_qc), sharers * hidden_part)
    back = results.reshape(experts, share, parts, piece).transpose(0, 2, 1, 3)
    back = lax.all_to_all(
        back.reshape(experts * parts, share, piece), ALL, split_axis=0, concat_axis=0, tiled=True
    )
    mixer_parts = lax.all_gather(mixer_quarter, "p", axis=0, tiled=False)
    mixer_quarter = jnp.sum(mixer_parts.astype(jnp.float32), axis=0).astype(jnp.bfloat16)
    mixer_whole = lax.all_gather(mixer_quarter, ("q", "c"), axis=0, tiled=False)
    mixer_whole = side_by_side(mixer_whole, (0, 2, 1, 3))
    routed_piece = combined(keys, route_weights, back.reshape(experts, groups, capacity, piece))

    mine = lax.all_gather(routed_piece, ("p", "q"), axis=0, tiled=False)
    other = flipped(mine, "c")
    return mixer_whole, assembled(lax.axis_index("c"), mine, other)


def solution(mesh):
    experts, parts = mesh.devices.shape
    finer = Mesh(mesh.devices.reshape(experts, parts // 4, 2, 2), ALL)
    return jax.shard_map(
        on_device,
        mesh=finer,
        in_specs=(
            P("ep", None),
            P(),
            P(None, TP),
            P(None, TP),
            P(None, TP),
            P(None, TP),
            P(TP, None),
            P("ep", None),
            P(),
            P("ep", None),
            P("ep", None),
            P("ep", None, TP),
            P("ep", None, TP),
            P("ep", TP, None),
        ),
        out_specs=(P("ep", None), P("ep", None)),
        check_vma=False,
    )
```

time: 167 us -> 168 us (level)
  blocking collectives: 20.4 us -> 42.1 us
  waiting for transfers between devices: 51.9 us -> 34.3 us
  Pallas kernels: 11 us -> 16.5 us
  local copies, waits for them, and re-layouts: 8.46 us -> 3.51 us
  matrix products: 4.43 us -> 1.68 us
    all_gather x1 -> x3, blocking collectives: 20.4 us -> 42.1 us  [the longest x1 19.5 us: on_device(): mine = lax.all_gather(routed_piece, ('p', 'q'), axis=0, tiled=False)]
    all_to_all x1, waiting for transfers between devices: 32.7 us -> 19.5 us  [on_device(): lax.all_to_all(back.reshape(experts * parts, share, piece), ALL, split_ax...]
    pallas_call x0 -> x3, Pallas kernels: none -> 7.46 us  [the longest x1 3.24 us: routed_slots(): pl.pallas_call(functools.partial(route_kernel, capacity=capacity, share=s...]
    all_to_all x1 -> x0, starting transfers between devices: 7.22 us -> none  [on_device(): lax.all_to_all(mixer_terms.reshape(length, parts, piece).transpose(1, 0,...]
    ppermute x7 -> x6, waiting for transfers between devices: 15.5 us -> 9.36 us  [flipped(): return lax.ppermute(value, axis, [(0, 1), (1, 0)])]
    ppermute x7 -> x6, starting transfers between devices: 25.8 us -> 30.6 us  [flipped(): return lax.ppermute(value, axis, [(0, 1), (1, 0)])]
    all_to_all x1, waiting for transfers between devices: 0.01 us -> 4.63 us  [on_device(): lax.all_to_all(outgoing.reshape(experts, share, width), 'ep', split_axis=...]
    all_to_all x1, starting transfers between devices: 14.5 us -> 18.5 us  [on_device(): lax.all_to_all(back.reshape(experts * parts, share, piece), ALL, split_ax...]
  transfers between devices with their start and end apart: 11 -> 9, of which waited for: 6 -> 5; matrix products, arithmetic and copies ran while one was open for 4% -> 3% of each run, Pallas kernels for 5% -> 5%
where the time goes in v2:
time: 168 us
  starting transfers between devices  65.4 us (39%)
  blocking collectives  42.1 us (25%)
  waiting for transfers between devices  34.3 us (20%)
  Pallas kernels  16.5 us (10%)
  local copies, waits for them, and re-layouts  3.51 us (2%)
  other arithmetic  3.13 us (2%)
  matrix products  1.68 us (1%)
    ppermute x6, starting transfers between devices, flipped(): return lax.ppermute(value, axis, [(0, 1), (1, 0)])  30.6 us
    all_gather x1, blocking collectives, on_device(): mine = lax.all_gather(routed_piece, ('p', 'q'), axis=0, tiled=False)  19.5 us
    all_to_all x1, waiting for transfers between devices, on_device(): lax.all_to_all(back.reshape(experts * parts, share, piece), ALL, split_ax...  19.5 us
    all_to_all x1, starting transfers between devices, on_device(): lax.all_to_all(back.reshape(experts * parts, share, piece), ALL, split_ax...  18.5 us
    all_gather x1, blocking collectives, on_device(): mixer_parts = lax.all_gather(mixer_quarter, 'p', axis=0, tiled=False)  14.9 us
    all_to_all x1, starting transfers between devices, on_device(): lax.all_to_all(outgoing.reshape(experts, share, width), 'ep', split_axis=...  13 us
    ppermute x6, waiting for transfers between devices, flipped(): return lax.ppermute(value, axis, [(0, 1), (1, 0)])  9.36 us
    all_gather x1, blocking collectives, on_device(): mixer_whole = lax.all_gather(mixer_quarter, ('q', 'c'), axis=0, tiled=False)  7.73 us
  transfers between devices with their start and end apart: 9, of which 5 were waited for; matrix products, arithmetic and copies ran while one was open for 3% of the time, Pallas kernels for 5%

profile of v2, /device:TPU:1, one launch (start us, length us, event | category | flops | bytes accessed | tf_op | source)
XLA Modules:
  0.0 167.6 jit_solution(15870677772749671346)
XLA Ops:
  0.7 1.5 pad_maximum_fusion.a0
  2.2 4.0 %collective-permute-start.4 = (bf16[6144,128]{1,0:T(8,128)(2,1)S(1)}, bf16[6144,128]{1,0:T(8,128)(2,1)S(1)}, u32[]{:S(2)}, u32[]{:S(2)}) collective-permute-start(bf16[6144,128]{1,0:T(8,128)(2,1)S(1)} %pad_maximum_fusion.a0), channel_id=1, source_target_pairs={{0,2},{2,0},{1,3},{3,1},{4,6},{6,4},{5,7},{7,5},{8,10},{10,8},{9,1... | collective-permute-start | bytes 4718600 | tf_op jit(solution)/shard_map/ppermute | solution.py:22
  6.2 0.8 copy.16.ids_ref
  7.0 3.2 %route.1 = (bf16[256,2048]{1,0:T(8,128)(2,1)}, s32[256,2]{1,0:T(8,128)}) custom-call(s32[1]{0:T(128)} %bitcast.6.quarter_ref, s32[256,2]{1,0:T(8,128)} %copy.16.ids_ref, bf16[256,2048]{1,0:T(8,128)(2,1)} %rows_ref.1, f32[1,2048]{1,0:T(1,128)} %bitcast.63), custom_call_target="tpu_custom_call" | custom-call | tf_op jit(solution)/shard_map/route/pallas_call | solution.py:59
  10.3 13.0 %all-to-all-start = ((bf16[32,8,2048]{2,1,0:T(8,128)(2,1)}), bf16[32,8,2048]{2,1,0:T(8,128)(2,1)}, u32[]{:S(2)}, u32[]{:S(2)}) async-start(bf16[32,8,2048]{2,1,0:T(8,128)(2,1)} %bitcast.59), calls=%async_computation | async-start | bytes 2097152 | tf_op jit(solution)/shard_map/all_to_all | solution.py:253
  23.3 3.1 %collective-permute-start.3 = (bf16[6144,128]{1,0:T(8,128)(2,1)S(1)}, bf16[6144,128]{1,0:T(8,128)(2,1)}, u32[]{:S(2)}, u32[]{:S(2)}) collective-permute-start(bf16[6144,128]{1,0:T(8,128)(2,1)S(1)} %pad_maximum_fusion.a0), channel_id=1, source_target_pairs={{0,1},{1,0},{2,3},{3,2},{4,5},{5,4},{6,7},{7,6},{8,9},{9,8},{10,11... | collective-permute-start | bytes 4718600 | tf_op jit(solution)/shard_map/ppermute | solution.py:22
  26.4 9.0 %collective-permute-done.4.a2 = bf16[6144,128]{1,0:T(8,128)(2,1)S(1)} collective-permute-done((bf16[6144,128]{1,0:T(8,128)(2,1)S(1)}, bf16[6144,128]{1,0:T(8,128)(2,1)S(1)}, u32[]{:S(2)}, u32[]{:S(2)}) %collective-permute-start.4) | collective-permute-done | bytes 1572896 | tf_op jit(solution)/shard_map/ppermute | solution.py:22
  35.5 8.0 %collective-permute-start.5 = (bf16[6144,128]{1,0:T(8,128)(2,1)S(1)}, bf16[6144,128]{1,0:T(8,128)(2,1)}, u32[]{:S(2)}, u32[]{:S(2)}) collective-permute-start(bf16[6144,128]{1,0:T(8,128)(2,1)S(1)} %collective-permute-done.4.a2), channel_id=1, source_target_pairs={{0,1},{1,0},{2,3},{3,2},{4,5},{5,4},{6,7},{7,6},{8,9},{9,8},{10,11... | collective-permute-start | bytes 4718600 | tf_op jit(solution)/shard_map/ppermute | solution.py:22
  43.4 1.2 fusion.2
  44.7 4.6 %all-to-all-done = bf16[32,8,2048]{2,1,0:T(8,128)(2,1)} async-done(((bf16[32,8,2048]{2,1,0:T(8,128)(2,1)}), bf16[32,8,2048]{2,1,0:T(8,128)(2,1)}, u32[]{:S(2)}, u32[]{:S(2)}) %all-to-all-start) | async-done | bytes 1048608 | tf_op jit(solution)/shard_map/all_to_all | solution.py:253
  49.3 6.2 %expert_ffn.1 = bf16[256,2048]{1,0:T(8,128)(2,1)} custom-call(bf16[256,2048]{1,0:T(8,128)(2,1)} %bitcast.9.x_hbm, bf16[6144,128]{1,0:T(8,128)(2,1)} %copy-done.1, bf16[6144,128]{1,0:T(8,128)(2,1)} %collective-permute-done.3.a1, bf16[6144,128]{1,0:T(8,128)(2,1)} %copy-done.2, bf16[6144,128]{1,0:T(8,128)(2,1)} %collective-permute-done.5.a3, ...), custom_call_target="tpu_custom_call" | custom-call | flops 1610612736 | bytes 8388608 | tf_op jit(solution)/shard_map/expert_ffn/pallas_call | solution.py:122
  55.5 18.5 %all-to-all-start.1 = ((bf16[512,8,128]{2,1,0:T(8,128)(2,1)}), bf16[512,8,128]{2,1,0:T(8,128)(2,1)S(1)}, u32[]{:S(2)}, u32[]{:S(2)}) async-start(bf16[512,8,128]{2,1,0:T(8,128)(2,1)} %bitcast.53), calls=%async_computation.1 | async-start | bytes 2097152 | tf_op jit(solution)/shard_map/all_to_all | solution.py:277
  74.1 0.4 fusion.13
  74.5 0.4 fusion.1
  75.0 3.2 %collective-permute-start = (bf16[2,64]{0,1:T(8,128)(2,1)S(1)}, bf16[2,64]{0,1:T(8,128)(2,1)S(1)}, u32[]{:S(2)}, u32[]{:S(2)}) collective-permute-start(bf16[2,64]{0,1:T(8,128)(2,1)S(1)} %slice.44), channel_id=1, source_target_pairs={{0,16},{16,32},{32,48},{48,64},{64,80},{80,96},{96,112},{112,128},... | collective-permute-start | bytes 776 | tf_op jit(solution)/shard_map/ppermute | solution.py:264
  78.2 0.8 collective-permute-done
  79.2 0.9 convolution_convert_fusion
  80.1 4.8 %collective-permute-start.1 = (bf16[128,1024]{1,0:T(8,128)(2,1)S(1)}, bf16[128,1024]{1,0:T(8,128)(2,1)S(1)}, u32[]{:S(2)}, u32[]{:S(2)}) collective-permute-start(bf16[128,1024]{1,0:T(8,128)(2,1)S(1)} %broadcast_select_fusion), channel_id=1, source_target_pairs={{0,1},{1,0},{2,3},{3,2},{4,5},{5,4},{6,7},{7,6},{8,9},{9,8},{10,11... | collective-permute-start | bytes 786440 | tf_op jit(solution)/shard_map/ppermute | solution.py:22
  85.0 0.8 copy.17.weights_ref
  85.8 0.3 collective-permute-done.1
  86.1 0.1 add_convert_fusion
  86.2 1.9 %collective-permute-start.2 = (bf16[128,512]{1,0:T(8,128)(2,1)S(1)}, bf16[128,512]{1,0:T(8,128)(2,1)S(1)}, u32[]{:S(2)}, u32[]{:S(2)}) collective-permute-start(bf16[128,512]{1,0:T(8,128)(2,1)S(1)} %broadcast_select_fusion.1), channel_id=1, source_target_pairs={{0,2},{2,0},{1,3},{3,1},{4,6},{6,4},{5,7},{7,5},{8,10},{10,8},{9,1... | collective-permute-start | bytes 393224 | tf_op jit(solution)/shard_map/ppermute | solution.py:22
  88.2 19.5 %all-to-all-done.1 = bf16[512,8,128]{2,1,0:T(8,128)(2,1)S(1)} async-done(((bf16[512,8,128]{2,1,0:T(8,128)(2,1)}), bf16[512,8,128]{2,1,0:T(8,128)(2,1)S(1)}, u32[]{:S(2)}, u32[]{:S(2)}) %all-to-all-start.1) | async-done | bytes 1048608 | tf_op jit(solution)/shard_map/all_to_all | solution.py:277
  107.6 1.0 copy-done.3
  108.6 2.9 %combine.1 = bf16[256,128]{1,0:T(8,128)(2,1)} custom-call(s32[256,2]{1,0:T(8,128)} %get-tuple-element.4.keys_ref, f32[256,2]{1,0:T(8,128)} %copy.17.weights_ref, bf16[32,4,32,128]{3,2,1,0:T(8,128)(2,1)} %bitcast.54), custom_call_target="tpu_custom_call" | custom-call | tf_op jit(solution)/shard_map/combine/pallas_call | solution.py:172
  111.5 19.5 %all-gather.2 = bf16[2048,128]{1,0:T(8,128)(2,1)S(1)} all-gather(bf16[256,128]{1,0:T(8,128)(2,1)} %combine.1), channel_id=4, replica_groups=mesh['ep'=32,'p'=4,'q'=2,'c'=2] {'p','q'}, dimensions={0}, use_global_device_ids=true | all-gather | bytes 589824 | tf_op jit(solution)/shard_map/all_gather | solution.py:286
  131.0 8.8 %collective-permute-start.6 = (bf16[8,256,128]{2,1,0:T(8,128)(2,1)S(1)}, bf16[8,256,128]{2,1,0:T(8,128)(2,1)S(1)}, u32[]{:S(2)}, u32[]{:S(2)}) collective-permute-start(bf16[8,256,128]{2,1,0:T(8,128)(2,1)S(1)} %bitcast.55), channel_id=1, source_target_pairs={{0,1},{1,0},{2,3},{3,2},{4,5},{5,4},{6,7},{7,6},{8,9},{9,8},{10,11... | collective-permute-start | bytes 1572872 | tf_op jit(solution)/shard_map/ppermute | solution.py:22
  139.8 14.9 %all-gather = bf16[512,512]{1,0:T(8,128)(2,1)S(1)} all-gather(bf16[128,512]{1,0:T(8,128)(2,1)S(1)} %add_convert_fusion.1), channel_id=2, replica_groups=mesh['ep'=32,'p'=4,'q'=2,'c'=2] {'p'}, dimensions={0}, use_global_device_ids=true | all-gather | bytes 655360 | tf_op jit(solution)/shard_map/all_gather | solution.py:280
  154.8 7.7 %all-gather.1 = bf16[512,512]{1,0:T(8,128)(2,1)} all-gather(bf16[128,512]{1,0:T(8,128)(2,1)S(1)} %reduce_sum.22), channel_id=3, replica_groups=mesh['ep'=32,'p'=4,'q'=2,'c'=2] {'q','c'}, dimensions={0}, use_global_device_ids=true | all-gather | bytes 655360 | tf_op jit(solution)/shard_map/all_gather | solution.py:282
  162.5 1.9 %side_by_side.1 = bf16[128,2048]{1,0:T(8,128)(2,1)} custom-call(bf16[4,128,512]{2,1,0:T(8,128)(2,1)} %bitcast.58), custom_call_target="tpu_custom_call" | custom-call | tf_op jit(solution)/shard_map/side_by_side/pallas_call | solution.py:210
  164.4 0.8 copy-done.6
  165.2 2.4 %assemble.1 = bf16[256,2048]{1,0:T(8,128)(2,1)} custom-call(s32[1]{0:T(128)} %bitcast.5.core_ref, bf16[8,256,128]{2,1,0:T(8,128)(2,1)} %bitcast.56, bf16[8,256,128]{2,1,0:T(8,128)(2,1)} %copy-done.6), custom_call_target="tpu_custom_call" | custom-call | tf_op jit(solution)/shard_map/assemble/pallas_call | solution.py:193
  (38 shorter events, 0.4 us)
Async XLA Ops:
  0.6 78.5 %copy-start = (bf16[64,2048]{1,0:T(8,128)(2,1)S(1)}, bf16[64,2048]{1,0:T(8,128)(2,1)}, u32[]{:S(2)}) copy-start(bf16[64,2048]{1,0:T(8,128)(2,1)} %param.20) | copy-start | bytes 786436
  0.6 5.6 %copy-start.9 = (s32[256,2]{0,1:T(2,128)S(1)}, s32[256,2]{0,1:T(2,128)}, u32[]{:S(2)}) copy-start(s32[256,2]{0,1:T(2,128)} %param.23) | copy-start | bytes 6148
  2.2 21.1 %copy-start.1 = (bf16[6144,128]{1,0:T(8,128)(2,1)}, bf16[6144,128]{1,0:T(8,128)(2,1)S(1)}, u32[]{:S(2)}) copy-start(bf16[6144,128]{1,0:T(8,128)(2,1)S(1)} %pad_maximum_fusion.a0) | copy-start | bytes 4718596
  2.2 33.3 %collective-permute-start.4 = (bf16[6144,128]{1,0:T(8,128)(2,1)S(1)}, bf16[6144,128]{1,0:T(8,128)(2,1)S(1)}, u32[]{:S(2)}, u32[]{:S(2)}) collective-permute-start(bf16[6144,128]{1,0:T(8,128)(2,1)S(1)} %pad_maximum_fusion.a0), channel_id=1, source_target_pairs={{0,2},{2,0},{1,3},{3,1},{4,6},{6,4},{5,7},{7,5},{8,10},{10,8},{9,1... | collective-permute-start | bytes 4718600 | tf_op jit(solution)/shard_map/ppermute | solution.py:22
  10.3 39.0 %all-to-all-start = ((bf16[32,8,2048]{2,1,0:T(8,128)(2,1)}), bf16[32,8,2048]{2,1,0:T(8,128)(2,1)}, u32[]{:S(2)}, u32[]{:S(2)}) async-start(bf16[32,8,2048]{2,1,0:T(8,128)(2,1)} %bitcast.59), calls=%async_computation | async-start | bytes 2097152 | tf_op jit(solution)/shard_map/all_to_all | solution.py:253
  23.3 21.4 %collective-permute-start.3 = (bf16[6144,128]{1,0:T(8,128)(2,1)S(1)}, bf16[6144,128]{1,0:T(8,128)(2,1)}, u32[]{:S(2)}, u32[]{:S(2)}) collective-permute-start(bf16[6144,128]{1,0:T(8,128)(2,1)S(1)} %pad_maximum_fusion.a0), channel_id=1, source_target_pairs={{0,1},{1,0},{2,3},{3,2},{4,5},{5,4},{6,7},{7,6},{8,9},{9,8},{10,11... | collective-permute-start | bytes 4718600 | tf_op jit(solution)/shard_map/ppermute | solution.py:22
  35.5 13.8 %copy-start.2 = (bf16[6144,128]{1,0:T(8,128)(2,1)}, bf16[6144,128]{1,0:T(8,128)(2,1)S(1)}, u32[]{:S(2)}) copy-start(bf16[6144,128]{1,0:T(8,128)(2,1)S(1)} %collective-permute-done.4.a2) | copy-start | bytes 4718596
  35.5 13.8 %collective-permute-start.5 = (bf16[6144,128]{1,0:T(8,128)(2,1)S(1)}, bf16[6144,128]{1,0:T(8,128)(2,1)}, u32[]{:S(2)}, u32[]{:S(2)}) collective-permute-start(bf16[6144,128]{1,0:T(8,128)(2,1)S(1)} %collective-permute-done.4.a2), channel_id=1, source_target_pairs={{0,1},{1,0},{2,3},{3,2},{4,5},{5,4},{6,7},{7,6},{8,9},{9,8},{10,11... | collective-permute-start | bytes 4718600 | tf_op jit(solution)/shard_map/ppermute | solution.py:22
  55.5 18.6 %copy-start.5 = (bf16[128,2048]{1,0:T(8,128)(2,1)S(1)}, bf16[128,2048]{1,0:T(8,128)(2,1)}, u32[]{:S(2)}) copy-start(bf16[128,2048]{1,0:T(8,128)(2,1)} %param.14) | copy-start | bytes 1572868
  55.5 18.6 %copy-start.8 = (f32[2048]{0:T(1024)S(1)}, f32[2048]{0:T(1024)}, u32[]{:S(2)}) copy-start(f32[2048]{0:T(1024)} %param.15) | copy-start | bytes 24580
  55.5 18.6 %copy-start.12 = (bf16[2048,64]{0,1:T(8,128)(2,1)S(1)}, bf16[2048,64]{0,1:T(8,128)(2,1)}, u32[]{:S(2)}) copy-start(bf16[2048,64]{0,1:T(8,128)(2,1)} %param.17) | copy-start | bytes 786436
  55.5 18.9 %copy-start.13 = (bf16[2048,64]{0,1:T(8,128)(2,1)S(1)}, bf16[2048,64]{0,1:T(8,128)(2,1)}, u32[]{:S(2)}) copy-start(bf16[2048,64]{0,1:T(8,128)(2,1)} %param.16) | copy-start | bytes 786436
  55.5 52.1 %all-to-all-start.1 = ((bf16[512,8,128]{2,1,0:T(8,128)(2,1)}), bf16[512,8,128]{2,1,0:T(8,128)(2,1)S(1)}, u32[]{:S(2)}, u32[]{:S(2)}) async-start(bf16[512,8,128]{2,1,0:T(8,128)(2,1)} %bitcast.53), calls=%async_computation.1 | async-start | bytes 2097152 | tf_op jit(solution)/shard_map/all_to_all | solution.py:277
  74.0 4.2 %copy-start.11 = (f32[3,64]{1,0:T(4,128)S(1)}, f32[3,64]{1,0:T(4,128)}, u32[]{:S(2)}) copy-start(f32[3,64]{1,0:T(4,128)} %param.19) | copy-start | bytes 2308
  74.0 5.1 %copy-start.7 = (bf16[2048,64]{0,1:T(8,128)(2,1)S(1)}, bf16[2048,64]{0,1:T(8,128)(2,1)}, u32[]{:S(2)}) copy-start(bf16[2048,64]{0,1:T(8,128)(2,1)} %param.18) | copy-start | bytes 786436
  74.5 10.5 %copy-start.10 = (f32[256,2]{0,1:T(2,128)S(1)}, f32[256,2]{0,1:T(2,128)}, u32[]{:S(2)}) copy-start(f32[256,2]{0,1:T(2,128)} %param.24) | copy-start | bytes 6148
  75.0 4.1 %collective-permute-start = (bf16[2,64]{0,1:T(8,128)(2,1)S(1)}, bf16[2,64]{0,1:T(8,128)(2,1)S(1)}, u32[]{:S(2)}, u32[]{:S(2)}) collective-permute-start(bf16[2,64]{0,1:T(8,128)(2,1)S(1)} %slice.44), channel_id=1, source_target_pairs={{0,16},{16,32},{32,48},{48,64},{64,80},{80,96},{96,112},{112,128},... | collective-permute-start | bytes 776 | tf_op jit(solution)/shard_map/ppermute | solution.py:264
  80.1 6.0 %collective-permute-start.1 = (bf16[128,1024]{1,0:T(8,128)(2,1)S(1)}, bf16[128,1024]{1,0:T(8,128)(2,1)S(1)}, u32[]{:S(2)}, u32[]{:S(2)}) collective-permute-start(bf16[128,1024]{1,0:T(8,128)(2,1)S(1)} %broadcast_select_fusion), channel_id=1, source_target_pairs={{0,1},{1,0},{2,3},{3,2},{4,5},{5,4},{6,7},{7,6},{8,9},{9,8},{10,11... | collective-permute-start | bytes 786440 | tf_op jit(solution)/shard_map/ppermute | solution.py:22
  86.2 53.5 %collective-permute-start.2 = (bf16[128,512]{1,0:T(8,128)(2,1)S(1)}, bf16[128,512]{1,0:T(8,128)(2,1)S(1)}, u32[]{:S(2)}, u32[]{:S(2)}) collective-permute-start(bf16[128,512]{1,0:T(8,128)(2,1)S(1)} %broadcast_select_fusion.1), channel_id=1, source_target_pairs={{0,2},{2,0},{1,3},{3,1},{4,6},{6,4},{5,7},{7,5},{8,10},{10,8},{9,1... | collective-permute-start | bytes 393224 | tf_op jit(solution)/shard_map/ppermute | solution.py:22
  107.6 1.0 copy-start.3
  131.0 33.4 %copy-start.4 = (bf16[2048,128]{1,0:T(8,128)(2,1)}, bf16[2048,128]{1,0:T(8,128)(2,1)S(1)}, u32[]{:S(2)}) copy-start(bf16[2048,128]{1,0:T(8,128)(2,1)S(1)} %all-gather.2) | copy-start | bytes 1572868
  131.0 33.4 %collective-permute-start.6 = (bf16[8,256,128]{2,1,0:T(8,128)(2,1)S(1)}, bf16[8,256,128]{2,1,0:T(8,128)(2,1)S(1)}, u32[]{:S(2)}, u32[]{:S(2)}) collective-permute-start(bf16[8,256,128]{2,1,0:T(8,128)(2,1)S(1)} %bitcast.55), channel_id=1, source_target_pairs={{0,1},{1,0},{2,3},{3,2},{4,5},{5,4},{6,7},{7,6},{8,9},{9,8},{10,11... | collective-permute-start | bytes 1572872 | tf_op jit(solution)/shard_map/ppermute | solution.py:22
  164.4 0.8 copy-start.6

commit v3 on v2

v3 whole, which is shorter than its diff:
```python
import functools

import jax
import jax.numpy as jnp
from jax import lax
from jax.experimental import pallas as pl
from jax.experimental.pallas import tpu as pltpu
from jax.sharding import Mesh, PartitionSpec as P

TP = ("p", "q", "c")
ALL = ("ep", "p", "q", "c")
VM = pl.BlockSpec(memory_space=pltpu.VMEM)
HBM = pl.BlockSpec(memory_space=pltpu.HBM)


def flipped(value, axis):
    return lax.ppermute(value, axis, [(0, 1), (1, 0)])


def route_kernel(
    quarter_ref,
    ids_ref,
    weights_ref,
    rows_ref,
    gain_ref,
    gate_hbm,
    up_hbm,
    down_hbm,
    out_ref,
    picks_ref,
    pack_hbm,
    sems,
    *,
    experts,
    capacity,
    share,
):
    copies, at = [], 0
    for i, source in enumerate((gate_hbm, up_hbm, down_hbm)):
        size = source.shape[0]
        copies.append(pltpu.make_async_copy(source, pack_hbm.at[pl.ds(at, size), :], sems.at[i]))
        copies[-1].start()
        at += size
    picks, tokens = ids_ref.shape
    slots = out_ref.shape[0]
    expert = lax.broadcasted_iota(jnp.int32, (experts, tokens), 0)
    named = [ids_ref[k : k + 1, :] == expert for k in range(picks)]
    both = functools.reduce(jnp.logical_or, named)
    row = lax.broadcasted_iota(jnp.int32, (tokens, tokens), 0)
    col = lax.broadcasted_iota(jnp.int32, (tokens, tokens), 1)
    earlier = jnp.dot(
        jnp.where(both, 1.0, 0.0).astype(jnp.bfloat16),
        jnp.where(row < col, 1.0, 0.0).astype(jnp.bfloat16),
        preferred_element_type=jnp.float32,
    )
    slot = lax.broadcasted_iota(jnp.int32, (slots, tokens), 0)
    slot_key = slot // share * capacity + slot % share + quarter_ref[0] * share
    chosen, lines = None, []
    for k in range(picks):
        rank = jnp.sum(jnp.where(named[k], earlier, 0.0), axis=0, keepdims=True).astype(jnp.int32)
        key = ids_ref[k : k + 1, :] * capacity + rank
        lines.append(key.astype(jnp.float32))
        here = slot_key == key
        chosen = here if chosen is None else jnp.logical_or(chosen, here)
    lines += [weights_ref[k : k + 1, :] for k in range(picks)]
    line = lax.broadcasted_iota(jnp.int32, (128, tokens), 0)
    table = jnp.zeros((128, tokens), jnp.float32)
    for i, value in enumerate(lines):
        table = jnp.where(line == i, value, table)
    picks_ref[...] = table.T
    values = rows_ref[...].astype(jnp.float32)
    scaled = values * lax.rsqrt(jnp.mean(values * values, axis=-1, keepdims=True) + 1e-06)
    normed = (scaled * gain_ref[...]).astype(jnp.bfloat16)
    out_ref[...] = jnp.dot(
        jnp.where(chosen, 1.0, 0.0).astype(jnp.bfloat16), normed, preferred_element_type=jnp.float32
    ).astype(jnp.bfloat16)
    for copy in copies:
        copy.wait()


def routed_slots(quarter, ids, weights, rows, gain, gate, up, down, experts, capacity, share):
    tokens, width = rows.shape
    packed = gate.shape[0] + up.shape[0] + down.shape[0]
    return pl.pallas_call(
        functools.partial(route_kernel, experts=experts, capacity=capacity, share=share),
        out_shape=(
            jax.ShapeDtypeStruct((experts * share, width), jnp.bfloat16),
            jax.ShapeDtypeStruct((tokens, 128), jnp.float32),
            jax.ShapeDtypeStruct((packed, gate.shape[1]), jnp.bfloat16),
        ),
        in_specs=[pl.BlockSpec(memory_space=pltpu.SMEM), VM, VM, VM, VM, HBM, HBM, HBM],
        out_specs=(VM, VM, HBM),
        scratch_shapes=[pltpu.SemaphoreType.DMA((3,))],
        name="route",
    )(quarter.reshape(1), ids.T, weights.T, rows, gain.reshape(1, -1), gate, up, down)


def mixer_kernel(
    core_ref, before_ref, rows_ref, gain_ref, inner_ref, gate_in_ref, gate_out_ref, taps_ref, out_w_ref, keep_ref, send_ref, ext_ref
):
    def normed(ref):
        values = ref[...].astype(jnp.float32)
        scaled = values * lax.rsqrt(jnp.mean(values * values, axis=-1, keepdims=True) + 1e-06)
        return (scaled * gain_ref[...]).astype(jnp.bfloat16)

    def projected(x, ref):
        return lax.dot_general(x, ref[...], (((1,), (1,)), ((), ())), preferred_element_type=jnp.float32)

    def conv_input(x):
        return (projected(x, gate_in_ref) * projected(x, inner_ref)).astype(jnp.bfloat16).astype(jnp.float32)

    lead, length = before_ref.shape[0], rows_ref.shape[0]
    x = normed(rows_ref)
    ext_ref[:lead, :] = conv_input(normed(before_ref))
    ext_ref[lead:, :] = conv_input(x)
    taps = taps_ref.shape[0]
    conv_out = None
    for j in range(taps):
        at = lead - (taps - 1) + j
        term = taps_ref[j : j + 1, :] * ext_ref[at : at + length, :]
        conv_out = term if conv_out is None else conv_out + term
    gated = (projected(x, gate_out_ref) * conv_out).astype(jnp.bfloat16)
    middle = out_w_ref.shape[1] // 2
    left = jnp.dot(gated, out_w_ref[:, :middle], preferred_element_type=jnp.float32).astype(jnp.bfloat16)
    right = jnp.dot(gated, out_w_ref[:, middle:], preferred_element_type=jnp.float32).astype(jnp.bfloat16)
    first = core_ref[0] == 0
    keep_ref[...] = jnp.where(first, left, right)
    send_ref[...] = jnp.where(first, right, left)


def mixer_terms(core, before, rows, gain, inner, gate_in, gate_out, taps, out_weight):
    length, width = rows.shape
    half = jax.ShapeDtypeStruct((length, width // 2), jnp.bfloat16)
    return pl.pallas_call(
        mixer_kernel,
        out_shape=(half, half),
        in_specs=[pl.BlockSpec(memory_space=pltpu.SMEM)] + [VM] * 8,
        out_specs=(VM, VM),
        scratch_shapes=[pltpu.VMEM((before.shape[0] + length, taps.shape[1]), jnp.float32)],
        name="mixer",
    )(core.reshape(1), before, rows, gain.reshape(1, -1), inner.T, gate_in.T, gate_out.T, taps, out_weight)


def summed(kept, sent, axis, pairs):
    received = lax.ppermute(sent, axis, pairs)
    return (kept.astype(jnp.float32) + received.astype(jnp.float32)).astype(jnp.bfloat16)


def halves(value, first):
    middle = value.shape[1] // 2
    left, right = value[:, :middle], value[:, middle:]
    return jnp.where(first, left, right), jnp.where(first, right, left)


def ffn_kernel(x_hbm, a0, a1, a2, a3, b0, b1, b2, b3, out_ref, x_ref, gu_ref, down_ref, hid_ref, sems):
    width = x_ref.shape[1]
    part = a0.shape[1]
    lead = b0.shape[0] - part
    x_copy = pltpu.make_async_copy(x_hbm, x_ref, sems.at[0])
    x_copy.start()
    copies = []
    for i, (a, b) in enumerate(((a0, b0), (a1, b1), (a2, b2), (a3, b3))):
        gate = pltpu.make_async_copy(
            a.at[pl.ds(0, width), :], gu_ref.at[i, :, pl.ds(0, part)], sems.at[3 * i + 1]
        )
        up = pltpu.make_async_copy(
            a.at[pl.ds(width, width), :], gu_ref.at[i, :, pl.ds(part, part)], sems.at[3 * i + 2]
        )
        down = pltpu.make_async_copy(
            b.at[pl.ds(lead, part), :], down_ref.at[pl.ds(i * part, part), :], sems.at[3 * i + 3]
        )
        gate.start()
        up.start()
        copies.append((gate, up, down))
    for _, _, down in copies:
        down.start()
    x_copy.wait()
    for i, (gate, up, _) in enumerate(copies):
        gate.wait()
        up.wait()
        acts = jnp.dot(x_ref[...], gu_ref[i], preferred_element_type=jnp.float32)
        g = acts[:, :part]
        hid_ref[:, i * part : (i + 1) * part] = (g / (1.0 + jnp.exp(-g)) * acts[:, part:]).astype(jnp.bfloat16)
    for _, _, down in copies:
        down.wait()
    cols = 512
    for n in range(0, width, cols):
        out_ref[:, n : n + cols] = jnp.dot(
            hid_ref[...], down_ref[:, n : n + cols], preferred_element_type=jnp.float32
        ).astype(jnp.bfloat16)


def expert_ffn(x, packs, hidden):
    rows, width = x.shape
    part = packs[0].shape[1]
    views = [wide_view(w, width) for w in packs]
    return pl.pallas_call(
        ffn_kernel,
        out_shape=jax.ShapeDtypeStruct(x.shape, jnp.bfloat16),
        in_specs=[HBM] * 9,
        out_specs=VM,
        scratch_shapes=[
            pltpu.VMEM((rows, width), jnp.bfloat16),
            pltpu.VMEM((4, width, 2 * part), jnp.bfloat16),
            pltpu.VMEM((hidden, width), jnp.bfloat16),
            pltpu.VMEM((rows, hidden), jnp.bfloat16),
            pltpu.SemaphoreType.DMA((13,)),
        ],
        cost_estimate=pl.CostEstimate(
            flops=6 * rows * width * hidden, bytes_accessed=8 * 2**20, transcendentals=rows * hidden
        ),
        name="expert_ffn",
    )(x, *packs, *views)


def narrow_view(value, part):
    rows, width = value.shape
    return value.reshape(rows // 8, 8, width // part, part).transpose(0, 2, 1, 3).reshape(-1, part)


def wide_view(value, width):
    _, part = value.shape
    return value.reshape(-1, width // part, 8, part).transpose(0, 2, 1, 3).reshape(-1, width)


def combine_kernel(picks_ref, rows_ref, out_ref, *, picks):
    experts, groups, capacity, width = rows_ref.shape
    tokens = picks_ref.shape[0]
    slots = experts * capacity
    column = lax.broadcasted_iota(jnp.int32, (tokens, slots), 1)
    spread = jnp.zeros((tokens, slots), jnp.float32)
    for k in range(picks):
        key = picks_ref[:, k : k + 1].astype(jnp.int32)
        spread = jnp.where(column == key, picks_ref[:, picks + k : picks + k + 1], spread)
    high = spread.astype(jnp.bfloat16)
    low = (spread - high.astype(jnp.float32)).astype(jnp.bfloat16)
    total = jnp.zeros((tokens, 2 * width), jnp.float32)
    for g in range(0, groups, 2):
        rows = jnp.concatenate(
            [rows_ref[:, g].reshape(slots, width), rows_ref[:, g + 1].reshape(slots, width)], axis=1
        )
        total = total + jnp.dot(high, rows, preferred_element_type=jnp.float32)
        total = total + jnp.dot(low, rows, preferred_element_type=jnp.float32)
    out_ref[...] = (total[:, :width] + total[:, width:]).astype(jnp.bfloat16)


def combined(table, rows, picks):
    return pl.pallas_call(
        functools.partial(combine_kernel, picks=picks),
        out_shape=jax.ShapeDtypeStruct((table.shape[0], rows.shape[-1]), jnp.bfloat16),
        in_specs=[VM] * 2,
        out_specs=VM,
        name="combine",
    )(table, rows)


def assemble_kernel(core_ref, mine_ref, other_ref, mixer_ref, routed_ref):
    count, _, piece = mine_ref.shape
    length = mixer_ref.shape[0]
    first = core_ref[0] == 0
    for i in range(count):
        mine, other = mine_ref[i], other_ref[i]
        lower = jnp.where(first, mine, other)
        upper = jnp.where(first, other, mine)
        at = 2 * i * piece
        routed_ref[:, at : at + piece] = lower[length:]
        routed_ref[:, at + piece : at + 2 * piece] = upper[length:]
        at = (i % 2 * (count // 2) + i // 2) * piece
        mixer_ref[:, at : at + piece] = lower[:length]
        at += count * piece
        mixer_ref[:, at : at + piece] = upper[:length]


def assembled(core, mine, other, length):
    count, rows, piece = mine.shape
    return pl.pallas_call(
        assemble_kernel,
        out_shape=(
            jax.ShapeDtypeStruct((length, 2 * count * piece), jnp.bfloat16),
            jax.ShapeDtypeStruct((rows - length, 2 * count * piece), jnp.bfloat16),
        ),
        in_specs=[pl.BlockSpec(memory_space=pltpu.SMEM), VM, VM],
        out_specs=(VM, VM),
        name="assemble",
    )(core.reshape(1), mine, other)


def on_device(
    mixer_rows,
    mixer_gain,
    inner_weight,
    gate_in_weight,
    gate_out_weight,
    conv_taps,
    mixer_out_weight,
    routed_rows,
    routed_gain,
    route_ids,
    route_weights,
    expert_gate,
    expert_up,
    expert_down,
):
    experts = lax.axis_size("ep")
    groups = lax.axis_size("p")
    parts = lax.axis_size(TP)
    sharers = lax.axis_size(("q", "c"))
    quarter = lax.axis_index(("q", "c"))
    tok_count, pick_count = route_ids.shape
    width = routed_rows.shape[1]
    capacity = 2 * tok_count * pick_count // experts
    share = capacity // sharers
    piece = width // parts
    hidden_part = expert_gate.shape[2]

    core, side = lax.axis_index("c"), lax.axis_index("q")
    column = lax.axis_index("p")
    length = mixer_rows.shape[0]

    lead = 8
    before = lax.ppermute(mixer_rows[length - lead :], "ep", [(i, i + 1) for i in range(experts - 1)])

    outgoing, table, pack = routed_slots(
        quarter,
        route_ids,
        route_weights,
        routed_rows,
        routed_gain,
        expert_gate[0],
        expert_up[0],
        narrow_view(expert_down[0], hidden_part),
        experts,
        capacity,
        share,
    )
    pack_q = flipped(pack, "q")
    slot_rows = lax.all_to_all(
        outgoing.reshape(experts, share, width), "ep", split_axis=0, concat_axis=0, tiled=True
    ).reshape(experts * share, width)
    pack_c = flipped(pack, "c")
    pack_qc = flipped(pack_q, "c")

    keep, send = mixer_terms(
        core, before, mixer_rows, mixer_gain, inner_weight, gate_in_weight, gate_out_weight, conv_taps, mixer_out_weight
    )
    swap = [(0, 1), (1, 0)]
    mixer_part = summed(keep, send, "c", swap)
    mixer_part = summed(*halves(mixer_part, side == 0), "q", swap)
    mixer_part = summed(*halves(mixer_part, column < 2), "p", [(i, i ^ 2) for i in range(groups)])
    mixer_part = summed(*halves(mixer_part, column % 2 == 0), "p", [(i, i ^ 1) for i in range(groups)])

    results = expert_ffn(slot_rows, (pack, pack_c, pack_q, pack_qc), sharers * hidden_part)
    back = results.reshape(experts, share, parts, piece).transpose(0, 2, 1, 3)
    back = lax.all_to_all(
        back.reshape(experts * parts, share, piece), ALL, split_axis=0, concat_axis=0, tiled=True
    )
    routed_part = combined(table, back.reshape(experts, groups, capacity, piece), pick_count)

    pieces = jnp.concatenate([mixer_part, routed_part], axis=0)
    mine = lax.all_gather(pieces, ("p", "q"), axis=0, tiled=False)
    other = flipped(mine, "c")
    return assembled(core, mine, other, length)


def solution(mesh):
    experts, parts = mesh.devices.shape
    finer = Mesh(mesh.devices.reshape(experts, parts // 4, 2, 2), ALL)
    return jax.shard_map(
        on_device,
        mesh=finer,
        in_specs=(
            P("ep", None),
            P(),
            P(None, TP),
            P(None, TP),
            P(None, TP),
            P(None, TP),
            P(TP, None),
            P("ep", None),
            P(),
            P("ep", None),
            P("ep", None),
            P("ep", None, TP),
            P("ep", None, TP),
            P("ep", TP, None),
        ),
        out_specs=(P("ep", None), P("ep", None)),
        check_vma=False,
    )
```

time: 168 us -> 215 us (1.28)
  Pallas kernels: 16.5 us -> 66.4 us
  blocking collectives: 42.1 us -> 22 us
  starting transfers between devices: 65.4 us -> 80.2 us
  waiting for transfers between devices: 34.3 us -> 40.7 us
    pallas_call x4, Pallas kernels: 10.3 us -> 60.2 us  [the longest x1 51 us: routed_slots(): pl.pallas_call(functools.partial(route_kernel, experts=experts, capacity=...]
    ppermute x1 -> x5, waiting for transfers between devices: 0.82 us -> 25.4 us  [the longest x4 24.4 us: summed(): received = lax.ppermute(sent, axis, pairs)]
    all_gather x3 -> x1, blocking collectives: 42.1 us -> 22 us  [on_device(): mine = lax.all_gather(pieces, ('p', 'q'), axis=0, tiled=False)]
    all_to_all x1, waiting for transfers between devices: 19.5 us -> 0.01 us  [on_device(): lax.all_to_all(back.reshape(experts * parts, share, piece), ALL, split_ax...]
    ppermute x1 -> x5, starting transfers between devices: 3.25 us -> 20.3 us  [the longest x4 17 us: summed(): received = lax.ppermute(sent, axis, pairs)]
    ppermute x6 -> x4, starting transfers between devices: 30.6 us -> 24.5 us  [flipped(): return lax.ppermute(value, axis, [(0, 1), (1, 0)])]
    ppermute x6 -> x4, waiting for transfers between devices: 9.36 us -> 15.3 us  [flipped(): return lax.ppermute(value, axis, [(0, 1), (1, 0)])]
    all_to_all x1, waiting for transfers between devices: 4.63 us -> 0.01 us  [on_device(): lax.all_to_all(outgoing.reshape(experts, share, width), 'ep', split_axis=...]
  transfers between devices with their start and end apart: 9 -> 11, of which waited for: 5 -> 6; matrix products, arithmetic and copies ran while one was open for 3% -> 0% of each run, Pallas kernels for 5% -> 4%
where the time goes in v3:
time: 215 us; the launch traced here: 214 us
  starting transfers between devices  80.2 us (37%)
  Pallas kernels  66.4 us (31%)
  waiting for transfers between devices  40.7 us (19%)
  blocking collectives  22 us (10%)
  local copies, waits for them, and re-layouts  3.26 us (2%)
    pallas_call x1, Pallas kernels, routed_slots(): pl.pallas_call(functools.partial(route_kernel, experts=experts, capacity=...  51 us
    ppermute x4, starting transfers between devices, flipped(): return lax.ppermute(value, axis, [(0, 1), (1, 0)])  24.5 us
    ppermute x4, waiting for transfers between devices, summed(): received = lax.ppermute(sent, axis, pairs)  24.4 us
    all_to_all x1, starting transfers between devices, on_device(): lax.all_to_all(back.reshape(experts * parts, share, piece), ALL, split_ax...  22.4 us
    all_gather x1, blocking collectives, on_device(): mine = lax.all_gather(pieces, ('p', 'q'), axis=0, tiled=False)  22 us
    ppermute x4, starting transfers between devices, summed(): received = lax.ppermute(sent, axis, pairs)  17 us
    ppermute x4, waiting for transfers between devices, flipped(): return lax.ppermute(value, axis, [(0, 1), (1, 0)])  15.3 us
    all_to_all x1, starting transfers between devices, on_device(): lax.all_to_all(outgoing.reshape(experts, share, width), 'ep', split_axis=...  13 us
  transfers between devices with their start and end apart: 11, of which 6 were waited for; matrix products, arithmetic and copies ran while one was open for 0% of the time, Pallas kernels for 4%

profile of v3, /device:TPU:1, one launch (start us, length us, event | category | flops | bytes accessed | tf_op | source)
XLA Modules:
  0.0 214.5 jit_solution(5467422170912419586)
XLA Ops:
  0.6 51.0 %route.1 = (bf16[256,2048]{1,0:T(8,128)(2,1)}, f32[256,128]{1,0:T(8,128)}, bf16[6144,128]{1,0:T(8,128)(2,1)}) custom-call(s32[1]{0:T(128)} %bitcast.5.quarter_ref, s32[2,256]{1,0:T(2,128)} %bitcast.60, f32[2,256]{1,0:T(2,128)} %bitcast.61, bf16[256,2048]{1,0:T(8,128)(2,1)} %rows_ref.3, f32[1,2048]{1,0:T(1,128)} %bitcast.58, bf16[2048,128]{1,0:T(8,128)(2,1)} %bitcast.52, ...), custom_call_target="tpu_custom_call" | custom-call | tf_op jit(solution)/shard_map/route/pallas_call | solution.py:84
  51.7 4.2 %collective-permute-start.6 = (bf16[6144,128]{1,0:T(8,128)(2,1)}, bf16[6144,128]{1,0:T(8,128)(2,1)S(1)}, u32[]{:S(2)}, u32[]{:S(2)}) collective-permute-start(bf16[6144,128]{1,0:T(8,128)(2,1)} %get-tuple-element.11.a0), channel_id=1, source_target_pairs={{0,2},{2,0},{1,3},{3,1},{4,6},{6,4},{5,7},{7,5},{8,10},{10,8},{9,1... | collective-permute-start | bytes 4718600 | tf_op jit(solution)/shard_map/ppermute | solution.py:17
  55.9 13.0 %all-to-all-start = ((bf16[32,8,2048]{2,1,0:T(8,128)(2,1)}), bf16[32,8,2048]{2,1,0:T(8,128)(2,1)}, u32[]{:S(2)}, u32[]{:S(2)}) async-start(bf16[32,8,2048]{2,1,0:T(8,128)(2,1)} %bitcast.51), calls=%async_computation | async-start | bytes 2097152 | tf_op jit(solution)/shard_map/all_to_all | solution.py:337
  68.9 3.1 %collective-permute-start.5 = (bf16[6144,128]{1,0:T(8,128)(2,1)S(1)}, bf16[6144,128]{1,0:T(8,128)(2,1)}, u32[]{:S(2)}, u32[]{:S(2)}) collective-permute-start(bf16[6144,128]{1,0:T(8,128)(2,1)S(1)} %copy-done), channel_id=1, source_target_pairs={{0,1},{1,0},{2,3},{3,2},{4,5},{5,4},{6,7},{7,6},{8,9},{9,8},{10,11... | collective-permute-start | bytes 4718600 | tf_op jit(solution)/shard_map/ppermute | solution.py:17
  72.0 13.4 %collective-permute-done.6.a2 = bf16[6144,128]{1,0:T(8,128)(2,1)S(1)} collective-permute-done((bf16[6144,128]{1,0:T(8,128)(2,1)}, bf16[6144,128]{1,0:T(8,128)(2,1)S(1)}, u32[]{:S(2)}, u32[]{:S(2)}) %collective-permute-start.6) | collective-permute-done | bytes 1572896 | tf_op jit(solution)/shard_map/ppermute | solution.py:17
  85.4 7.9 %collective-permute-start.7 = (bf16[6144,128]{1,0:T(8,128)(2,1)S(1)}, bf16[6144,128]{1,0:T(8,128)(2,1)}, u32[]{:S(2)}, u32[]{:S(2)}) collective-permute-start(bf16[6144,128]{1,0:T(8,128)(2,1)S(1)} %collective-permute-done.6.a2), channel_id=1, source_target_pairs={{0,1},{1,0},{2,3},{3,2},{4,5},{5,4},{6,7},{7,6},{8,9},{9,8},{10,11... | collective-permute-start | bytes 4718600 | tf_op jit(solution)/shard_map/ppermute | solution.py:17
  93.3 0.8 slice.21
  94.1 3.3 %collective-permute-start = (bf16[8,2048]{1,0:T(8,128)(2,1)S(1)}, bf16[8,2048]{1,0:T(8,128)(2,1)S(1)}, u32[]{:S(2)}, u32[]{:S(2)}) collective-permute-start(bf16[8,2048]{1,0:T(8,128)(2,1)S(1)} %slice.21), channel_id=1, source_target_pairs={{0,16},{16,32},{32,48},{48,64},{64,80},{80,96},{96,112},{112,128},... | collective-permute-start | bytes 98312 | tf_op jit(solution)/shard_map/ppermute | solution.py:321
  97.3 1.0 collective-permute-done.before_ref
  98.3 0.6 copy-done.6
  98.9 3.5 %mixer.1 = (bf16[128,1024]{1,0:T(8,128)(2,1)}, bf16[128,1024]{1,0:T(8,128)(2,1)}) custom-call(s32[1]{0:T(128)} %bitcast.core_ref, bf16[8,2048]{1,0:T(8,128)(2,1)} %copy-done.6, bf16[128,2048]{1,0:T(8,128)(2,1)} %rows_ref.2, f32[1,2048]{1,0:T(1,128)} %bitcast.59, bf16[64,2048]{1,0:T(8,128)(2,1)} %bitcast.55, bf16[64,2048]{1,0:T(8,128)(2,1)} %bitcast.56, ...), custom_call_target="tpu_custom_call" | custom-call | tf_op jit(solution)/shard_map/mixer/pallas_call | solution.py:134
  102.4 2.8 %collective-permute-start.1 = (bf16[128,1024]{1,0:T(8,128)(2,1)}, bf16[128,1024]{1,0:T(8,128)(2,1)S(1)}, u32[]{:S(2)}, u32[]{:S(2)}) collective-permute-start(bf16[128,1024]{1,0:T(8,128)(2,1)} %get-tuple-element.8), channel_id=1, source_target_pairs={{0,1},{1,0},{2,3},{3,2},{4,5},{5,4},{6,7},{7,6},{8,9},{9,8},{10,11... | collective-permute-start | bytes 786440 | tf_op jit(solution)/shard_map/ppermute | solution.py:145
  105.2 6.2 %expert_ffn.1 = bf16[256,2048]{1,0:T(8,128)(2,1)} custom-call(bf16[256,2048]{1,0:T(8,128)(2,1)} %bitcast.15.x_hbm, bf16[6144,128]{1,0:T(8,128)(2,1)} %get-tuple-element.11.a0, bf16[6144,128]{1,0:T(8,128)(2,1)} %collective-permute-done.5.a1, bf16[6144,128]{1,0:T(8,128)(2,1)} %copy-done.1, bf16[6144,128]{1,0:T(8,128)(2,1)} %collective-permute-done.7.a3, ...), custom_call_target="tpu_custom_call" | custom-call | flops 1610612736 | bytes 8388608 | tf_op jit(solution)/shard_map/expert_ffn/pallas_call | solution.py:197
  111.4 0.0 copy-start.5
  111.4 22.4 %all-to-all-start.1 = ((bf16[512,8,128]{2,1,0:T(8,128)(2,1)}), bf16[512,8,128]{2,1,0:T(8,128)(2,1)S(1)}, u32[]{:S(2)}, u32[]{:S(2)}) async-start(bf16[512,8,128]{2,1,0:T(8,128)(2,1)} %bitcast.47), calls=%async_computation.1 | async-start | bytes 2097152 | tf_op jit(solution)/shard_map/all_to_all | solution.py:354
  133.9 0.1 add_convert_fusion
  134.0 3.3 %collective-permute-start.2 = (bf16[128,512]{1,0:T(8,128)(2,1)S(1)}, bf16[128,512]{1,0:T(8,128)(2,1)S(1)}, u32[]{:S(2)}, u32[]{:S(2)}) collective-permute-start(bf16[128,512]{1,0:T(8,128)(2,1)S(1)} %broadcast_select_fusion), channel_id=1, source_target_pairs={{0,2},{2,0},{1,3},{3,1},{4,6},{6,4},{5,7},{7,5},{8,10},{10,8},{9,1... | collective-permute-start | bytes 393224 | tf_op jit(solution)/shard_map/ppermute | solution.py:145
  137.3 20.2 %collective-permute-done.2 = bf16[128,512]{1,0:T(8,128)(2,1)S(1)} collective-permute-done((bf16[128,512]{1,0:T(8,128)(2,1)S(1)}, bf16[128,512]{1,0:T(8,128)(2,1)S(1)}, u32[]{:S(2)}, u32[]{:S(2)}) %collective-permute-start.2) | collective-permute-done | bytes 131104 | tf_op jit(solution)/shard_map/ppermute | solution.py:145
  157.5 0.1 add_convert_fusion.1
  157.5 6.5 %collective-permute-start.3 = (bf16[128,256]{1,0:T(8,128)(2,1)S(1)}, bf16[128,256]{1,0:T(8,128)(2,1)S(1)}, u32[]{:S(2)}, u32[]{:S(2)}) collective-permute-start(bf16[128,256]{1,0:T(8,128)(2,1)S(1)} %broadcast_select_fusion.1), channel_id=1, source_target_pairs={{0,8},{4,12},{8,0},{12,4},{1,9},{5,13},{9,1},{13,5},{2,10},{6,14},... | collective-permute-start | bytes 196616 | tf_op jit(solution)/shard_map/ppermute | solution.py:145
  164.1 2.6 %collective-permute-done.3 = bf16[128,256]{1,0:T(8,128)(2,1)S(1)} collective-permute-done((bf16[128,256]{1,0:T(8,128)(2,1)S(1)}, bf16[128,256]{1,0:T(8,128)(2,1)S(1)}, u32[]{:S(2)}, u32[]{:S(2)}) %collective-permute-start.3) | collective-permute-done | bytes 65568 | tf_op jit(solution)/shard_map/ppermute | solution.py:145
  166.8 4.4 %collective-permute-start.4 = (bf16[128,128]{1,0:T(8,128)(2,1)S(1)}, bf16[128,128]{1,0:T(8,128)(2,1)S(1)}, u32[]{:S(2)}, u32[]{:S(2)}) collective-permute-start(bf16[128,128]{1,0:T(8,128)(2,1)S(1)} %broadcast_select_fusion.2), channel_id=1, source_target_pairs={{0,4},{4,0},{8,12},{12,8},{1,5},{5,1},{9,13},{13,9},{2,6},{6,2},{1... | collective-permute-start | bytes 98312 | tf_op jit(solution)/shard_map/ppermute | solution.py:145
  171.2 1.6 collective-permute-done.4
  172.8 0.0 copy-start.2
  172.8 1.0 copy-done.2
  173.8 2.9 %combine.1 = bf16[256,128]{1,0:T(8,128)(2,1)} custom-call(f32[256,128]{1,0:T(8,128)} %get-tuple-element.9.picks_ref, bf16[32,4,32,128]{3,2,1,0:T(8,128)(2,1)} %bitcast.48), custom_call_target="tpu_custom_call" | custom-call | tf_op jit(solution)/shard_map/combine/pallas_call | solution.py:248
  176.6 0.8 pad_maximum_fusion
  177.5 22.0 %all-gather = bf16[3072,128]{1,0:T(8,128)(2,1)S(1)} all-gather(bf16[384,128]{1,0:T(8,128)(2,1)S(1)} %pad_maximum_fusion), channel_id=2, replica_groups=mesh['ep'=32,'p'=4,'q'=2,'c'=2] {'p','q'}, dimensions={0}, use_global_device_ids=true | all-gather | bytes 884736 | tf_op jit(solution)/shard_map/all_gather | solution.py:360
  199.5 9.4 %collective-permute-start.8 = (bf16[8,384,128]{2,1,0:T(8,128)(2,1)S(1)}, bf16[8,384,128]{2,1,0:T(8,128)(2,1)S(1)}, u32[]{:S(2)}, u32[]{:S(2)}) collective-permute-start(bf16[8,384,128]{2,1,0:T(8,128)(2,1)S(1)} %bitcast.49), channel_id=1, source_target_pairs={{0,1},{1,0},{2,3},{3,2},{4,5},{5,4},{6,7},{7,6},{8,9},{9,8},{10,11... | collective-permute-start | bytes 2359304 | tf_op jit(solution)/shard_map/ppermute | solution.py:17
  208.8 1.9 collective-permute-done.8.other_ref
  210.7 0.9 copy-done.4
  211.6 2.8 %assemble.1 = (bf16[128,2048]{1,0:T(8,128)(2,1)}, bf16[256,2048]{1,0:T(8,128)(2,1)}) custom-call(s32[1]{0:T(128)} %bitcast.core_ref, bf16[8,384,128]{2,1,0:T(8,128)(2,1)} %bitcast.50, bf16[8,384,128]{2,1,0:T(8,128)(2,1)} %copy-done.4), custom_call_target="tpu_custom_call" | custom-call | tf_op jit(solution)/shard_map/assemble/pallas_call | solution.py:276
  (19 shorter events, 0.1 us)
Async XLA Ops:
  51.7 17.2 %copy-start = (bf16[6144,128]{1,0:T(8,128)(2,1)S(1)}, bf16[6144,128]{1,0:T(8,128)(2,1)}, u32[]{:S(2)}) copy-start(bf16[6144,128]{1,0:T(8,128)(2,1)} %get-tuple-element.11.a0) | copy-start | bytes 4718596
  51.7 33.7 %collective-permute-start.6 = (bf16[6144,128]{1,0:T(8,128)(2,1)}, bf16[6144,128]{1,0:T(8,128)(2,1)S(1)}, u32[]{:S(2)}, u32[]{:S(2)}) collective-permute-start(bf16[6144,128]{1,0:T(8,128)(2,1)} %get-tuple-element.11.a0), channel_id=1, source_target_pairs={{0,2},{2,0},{1,3},{3,1},{4,6},{6,4},{5,7},{7,5},{8,10},{10,8},{9,1... | collective-permute-start | bytes 4718600 | tf_op jit(solution)/shard_map/ppermute | solution.py:17
  55.9 49.3 %all-to-all-start = ((bf16[32,8,2048]{2,1,0:T(8,128)(2,1)}), bf16[32,8,2048]{2,1,0:T(8,128)(2,1)}, u32[]{:S(2)}, u32[]{:S(2)}) async-start(bf16[32,8,2048]{2,1,0:T(8,128)(2,1)} %bitcast.51), calls=%async_computation | async-start | bytes 2097152 | tf_op jit(solution)/shard_map/all_to_all | solution.py:337
  68.9 36.3 %collective-permute-start.5 = (bf16[6144,128]{1,0:T(8,128)(2,1)S(1)}, bf16[6144,128]{1,0:T(8,128)(2,1)}, u32[]{:S(2)}, u32[]{:S(2)}) collective-permute-start(bf16[6144,128]{1,0:T(8,128)(2,1)S(1)} %copy-done), channel_id=1, source_target_pairs={{0,1},{1,0},{2,3},{3,2},{4,5},{5,4},{6,7},{7,6},{8,9},{9,8},{10,11... | collective-permute-start | bytes 4718600 | tf_op jit(solution)/shard_map/ppermute | solution.py:17
  85.4 19.8 %copy-start.1 = (bf16[6144,128]{1,0:T(8,128)(2,1)}, bf16[6144,128]{1,0:T(8,128)(2,1)S(1)}, u32[]{:S(2)}) copy-start(bf16[6144,128]{1,0:T(8,128)(2,1)S(1)} %collective-permute-done.6.a2) | copy-start | bytes 4718596
  85.4 19.8 %collective-permute-start.7 = (bf16[6144,128]{1,0:T(8,128)(2,1)S(1)}, bf16[6144,128]{1,0:T(8,128)(2,1)}, u32[]{:S(2)}, u32[]{:S(2)}) collective-permute-start(bf16[6144,128]{1,0:T(8,128)(2,1)S(1)} %collective-permute-done.6.a2), channel_id=1, source_target_pairs={{0,1},{1,0},{2,3},{3,2},{4,5},{5,4},{6,7},{7,6},{8,9},{9,8},{10,11... | collective-permute-start | bytes 4718600 | tf_op jit(solution)/shard_map/ppermute | solution.py:17
  94.1 4.3 %collective-permute-start = (bf16[8,2048]{1,0:T(8,128)(2,1)S(1)}, bf16[8,2048]{1,0:T(8,128)(2,1)S(1)}, u32[]{:S(2)}, u32[]{:S(2)}) collective-permute-start(bf16[8,2048]{1,0:T(8,128)(2,1)S(1)} %slice.21), channel_id=1, source_target_pairs={{0,16},{16,32},{32,48},{48,64},{64,80},{80,96},{96,112},{112,128},... | collective-permute-start | bytes 98312 | tf_op jit(solution)/shard_map/ppermute | solution.py:321
  98.3 0.6 copy-start.6
  102.4 31.4 %collective-permute-start.1 = (bf16[128,1024]{1,0:T(8,128)(2,1)}, bf16[128,1024]{1,0:T(8,128)(2,1)S(1)}, u32[]{:S(2)}, u32[]{:S(2)}) collective-permute-start(bf16[128,1024]{1,0:T(8,128)(2,1)} %get-tuple-element.8), channel_id=1, source_target_pairs={{0,1},{1,0},{2,3},{3,2},{4,5},{5,4},{6,7},{7,6},{8,9},{9,8},{10,11... | collective-permute-start | bytes 786440 | tf_op jit(solution)/shard_map/ppermute | solution.py:145
  111.4 22.5 %copy-start.5 = (bf16[128,1024]{1,0:T(8,128)(2,1)S(1)}, bf16[128,1024]{1,0:T(8,128)(2,1)}, u32[]{:S(2)}) copy-start(bf16[128,1024]{1,0:T(8,128)(2,1)} %get-tuple-element.7) | copy-start | bytes 786436
  111.4 61.4 %all-to-all-start.1 = ((bf16[512,8,128]{2,1,0:T(8,128)(2,1)}), bf16[512,8,128]{2,1,0:T(8,128)(2,1)S(1)}, u32[]{:S(2)}, u32[]{:S(2)}) async-start(bf16[512,8,128]{2,1,0:T(8,128)(2,1)} %bitcast.47), calls=%async_computation.1 | async-start | bytes 2097152 | tf_op jit(solution)/shard_map/all_to_all | solution.py:354
  134.0 23.5 %collective-permute-start.2 = (bf16[128,512]{1,0:T(8,128)(2,1)S(1)}, bf16[128,512]{1,0:T(8,128)(2,1)S(1)}, u32[]{:S(2)}, u32[]{:S(2)}) collective-permute-start(bf16[128,512]{1,0:T(8,128)(2,1)S(1)} %broadcast_select_fusion), channel_id=1, source_target_pairs={{0,2},{2,0},{1,3},{3,1},{4,6},{6,4},{5,7},{7,5},{8,10},{10,8},{9,1... | collective-permute-start | bytes 393224 | tf_op jit(solution)/shard_map/ppermute | solution.py:145
  157.5 9.2 %collective-permute-start.3 = (bf16[128,256]{1,0:T(8,128)(2,1)S(1)}, bf16[128,256]{1,0:T(8,128)(2,1)S(1)}, u32[]{:S(2)}, u32[]{:S(2)}) collective-permute-start(bf16[128,256]{1,0:T(8,128)(2,1)S(1)} %broadcast_select_fusion.1), channel_id=1, source_target_pairs={{0,8},{4,12},{8,0},{12,4},{1,9},{5,13},{9,1},{13,5},{2,10},{6,14},... | collective-permute-start | bytes 196616 | tf_op jit(solution)/shard_map/ppermute | solution.py:145
  166.8 6.0 %collective-permute-start.4 = (bf16[128,128]{1,0:T(8,128)(2,1)S(1)}, bf16[128,128]{1,0:T(8,128)(2,1)S(1)}, u32[]{:S(2)}, u32[]{:S(2)}) collective-permute-start(bf16[128,128]{1,0:T(8,128)(2,1)S(1)} %broadcast_select_fusion.2), channel_id=1, source_target_pairs={{0,4},{4,0},{8,12},{12,8},{1,5},{5,1},{9,13},{13,9},{2,6},{6,2},{1... | collective-permute-start | bytes 98312 | tf_op jit(solution)/shard_map/ppermute | solution.py:145
  172.8 1.0 copy-start.2
  199.5 11.3 %copy-start.3 = (bf16[3072,128]{1,0:T(8,128)(2,1)}, bf16[3072,128]{1,0:T(8,128)(2,1)S(1)}, u32[]{:S(2)}) copy-start(bf16[3072,128]{1,0:T(8,128)(2,1)S(1)} %all-gather) | copy-start | bytes 2359300
  199.5 11.3 %collective-permute-start.8 = (bf16[8,384,128]{2,1,0:T(8,128)(2,1)S(1)}, bf16[8,384,128]{2,1,0:T(8,128)(2,1)S(1)}, u32[]{:S(2)}, u32[]{:S(2)}) collective-permute-start(bf16[8,384,128]{2,1,0:T(8,128)(2,1)S(1)} %bitcast.49), channel_id=1, source_target_pairs={{0,1},{1,0},{2,3},{3,2},{4,5},{5,4},{6,7},{7,6},{8,9},{9,8},{10,11... | collective-permute-start | bytes 2359304 | tf_op jit(solution)/shard_map/ppermute | solution.py:17
  210.7 0.9 copy-start.4

commit v4 on v3

--- a/solution.py
+++ b/solution.py
@@ -23,24 +23,13 @@
     weights_ref,
     rows_ref,
     gain_ref,
-    gate_hbm,
-    up_hbm,
-    down_hbm,
     out_ref,
     picks_ref,
-    pack_hbm,
-    sems,
     *,
     experts,
     capacity,
     share,
 ):
-    copies, at = [], 0
-    for i, source in enumerate((gate_hbm, up_hbm, down_hbm)):
-        size = source.shape[0]
-        copies.append(pltpu.make_async_copy(source, pack_hbm.at[pl.ds(at, size), :], sems.at[i]))
-        copies[-1].start()
-        at += size
     picks, tokens = ids_ref.shape
     slots = out_ref.shape[0]
     expert = lax.broadcasted_iota(jnp.int32, (experts, tokens), 0)
@@ -74,25 +63,20 @@
     out_ref[...] = jnp.dot(
         jnp.where(chosen, 1.0, 0.0).astype(jnp.bfloat16), normed, preferred_element_type=jnp.float32
     ).astype(jnp.bfloat16)
-    for copy in copies:
-        copy.wait()
-
-
-def routed_slots(quarter, ids, weights, rows, gain, gate, up, down, experts, capacity, share):
+
+
+def routed_slots(quarter, ids, weights, rows, gain, experts, capacity, share):
     tokens, width = rows.shape
-    packed = gate.shape[0] + up.shape[0] + down.shape[0]
     return pl.pallas_call(
         functools.partial(route_kernel, experts=experts, capacity=capacity, share=share),
         out_shape=(
             jax.ShapeDtypeStruct((experts * share, width), jnp.bfloat16),
             jax.ShapeDtypeStruct((tokens, 128), jnp.float32),
-            jax.ShapeDtypeStruct((packed, gate.shape[1]), jnp.bfloat16),
         ),
-        in_specs=[pl.BlockSpec(memory_space=pltpu.SMEM), VM, VM, VM, VM, HBM, HBM, HBM],
-        out_specs=(VM, VM, HBM),
-        scratch_shapes=[pltpu.SemaphoreType.DMA((3,))],
+        in_specs=[pl.BlockSpec(memory_space=pltpu.SMEM), VM, VM, VM, VM],
+        out_specs=(VM, VM),
         name="route",
-    )(quarter.reshape(1), ids.T, weights.T, rows, gain.reshape(1, -1), gate, up, down)
+    )(quarter.reshape(1), ids.T, weights.T, rows, gain.reshape(1, -1))
 
 
 def mixer_kernel(
@@ -223,7 +207,7 @@
     return value.reshape(-1, width // part, 8, part).transpose(0, 2, 1, 3).reshape(-1, width)
 
 
-def combine_kernel(picks_ref, rows_ref, out_ref, *, picks):
+def combine_kernel(picks_ref, rows_ref, mixer_ref, out_ref, *, picks):
     experts, groups, capacity, width = rows_ref.shape
     tokens = picks_ref.shape[0]
     slots = experts * capacity
@@ -241,17 +225,19 @@
         )
         total = total + jnp.dot(high, rows, preferred_element_type=jnp.float32)
         total = total + jnp.dot(low, rows, preferred_element_type=jnp.float32)
-    out_ref[...] = (total[:, :width] + total[:, width:]).astype(jnp.bfloat16)
-
-
-def combined(table, rows, picks):
+    length = mixer_ref.shape[0]
+    out_ref[:length, :] = mixer_ref[...]
+    out_ref[length:, :] = (total[:, :width] + total[:, width:]).astype(jnp.bfloat16)
+
+
+def combined(table, rows, mixer_part, picks):
     return pl.pallas_call(
         functools.partial(combine_kernel, picks=picks),
-        out_shape=jax.ShapeDtypeStruct((table.shape[0], rows.shape[-1]), jnp.bfloat16),
-        in_specs=[VM] * 2,
+        out_shape=jax.ShapeDtypeStruct((mixer_part.shape[0] + table.shape[0], rows.shape[-1]), jnp.bfloat16),
+        in_specs=[VM] * 3,
         out_specs=VM,
         name="combine",
-    )(table, rows)
+    )(table, rows, mixer_part)
 
 
 def assemble_kernel(core_ref, mine_ref, other_ref, mixer_ref, routed_ref):
@@ -317,23 +303,15 @@
     column = lax.axis_index("p")
     length = mixer_rows.shape[0]
 
+    pack = jnp.concatenate([expert_gate[0], expert_up[0], narrow_view(expert_down[0], hidden_part)], axis=0)
+    pack_q = flipped(pack, "q")
+
     lead = 8
     before = lax.ppermute(mixer_rows[length - lead :], "ep", [(i, i + 1) for i in range(experts - 1)])
 
-    outgoing, table, pack = routed_slots(
-        quarter,
-        route_ids,
-        route_weights,
-        routed_rows,
-        routed_gain,
-        expert_gate[0],
-        expert_up[0],
-        narrow_view(expert_down[0], hidden_part),
-        experts,
-        capacity,
-        share,
-    )
-    pack_q = flipped(pack, "q")
+    outgoing, table = routed_slots(
+        quarter, route_ids, route_weights, routed_rows, routed_gain, experts, capacity, share
+    )
     slot_rows = lax.all_to_all(
         outgoing.reshape(experts, share, width), "ep", split_axis=0, concat_axis=0, tiled=True
     ).reshape(experts * share, width)
@@ -354,9 +332,8 @@
     back = lax.all_to_all(
         back.reshape(experts * parts, share, piece), ALL, split_axis=0, concat_axis=0, tiled=True
     )
-    routed_part = combined(table, back.reshape(experts, groups, capacity, piece), pick_count)
-
-    pieces = jnp.concatenate([mixer_part, routed_part], axis=0)
+    pieces = combined(table, back.reshape(experts, groups, capacity, piece), mixer_part, pick_count)
+
     mine = lax.all_gather(pieces, ("p", "q"), axis=0, tiled=False)
     other = flipped(mine, "c")
     return assembled(core, mine, other, length)

time: 215 us -> 165 us (0.77)
  Pallas kernels: 66.4 us -> 18.3 us
  waiting for transfers between devices: 40.7 us -> 37.4 us
    pallas_call x1, Pallas kernels: 51 us -> 3.02 us  [routed_slots(): pl.pallas_call(functools.partial(route_kernel, experts=experts, capacity=...]
    ppermute x4, waiting for transfers between devices: 15.3 us -> 12 us  [flipped(): return lax.ppermute(value, axis, [(0, 1), (1, 0)])]
  transfers between devices with their start and end apart: 11 -> 11, of which waited for: 6 -> 6; matrix products, arithmetic and copies ran while one was open for 0% -> 1% of each run, Pallas kernels for 4% -> 8%
where the time goes in v4:
time: 165 us; the launch traced here: 164 us
  starting transfers between devices  80.2 us (49%)
  waiting for transfers between devices  37.4 us (23%)
  blocking collectives  22.2 us (13%)
  Pallas kernels  18.3 us (11%)
  local copies, waits for them, and re-layouts  3.27 us (2%)
  other arithmetic  2.27 us (1%)
    ppermute x4, starting transfers between devices, flipped(): return lax.ppermute(value, axis, [(0, 1), (1, 0)])  24.5 us
    ppermute x4, waiting for transfers between devices, summed(): received = lax.ppermute(sent, axis, pairs)  24.4 us
    all_to_all x1, starting transfers between devices, on_device(): lax.all_to_all(back.reshape(experts * parts, share, piece), ALL, split_ax...  22.4 us
    all_gather x1, blocking collectives, on_device(): mine = lax.all_gather(pieces, ('p', 'q'), axis=0, tiled=False)  22.2 us
    ppermute x4, starting transfers between devices, summed(): received = lax.ppermute(sent, axis, pairs)  17 us
    all_to_all x1, starting transfers between devices, on_device(): lax.all_to_all(outgoing.reshape(experts, share, width), 'ep', split_axis=...  13 us
    ppermute x4, waiting for transfers between devices, flipped(): return lax.ppermute(value, axis, [(0, 1), (1, 0)])  12 us
    pallas_call x1, Pallas kernels, expert_ffn(): pl.pallas_call(ffn_kernel, out_shape=jax.ShapeDtypeStruct(x.shape, jnp.bf...  6.16 us
  transfers between devices with their start and end apart: 11, of which 6 were waited for; matrix products, arithmetic and copies ran while one was open for 1% of the time, Pallas kernels for 8%

profile of v4, /device:TPU:1, one launch (start us, length us, event | category | flops | bytes accessed | tf_op | source)
XLA Modules:
  0.0 164.5 jit_solution(999185219822952226)
XLA Ops:
  0.6 1.5 pad_maximum_fusion.a0
  2.1 4.0 %collective-permute-start.1 = (bf16[6144,128]{1,0:T(8,128)(2,1)S(1)}, bf16[6144,128]{1,0:T(8,128)(2,1)S(1)}, u32[]{:S(2)}, u32[]{:S(2)}) collective-permute-start(bf16[6144,128]{1,0:T(8,128)(2,1)S(1)} %pad_maximum_fusion.a0), channel_id=1, source_target_pairs={{0,2},{2,0},{1,3},{3,1},{4,6},{6,4},{5,7},{7,5},{8,10},{10,8},{9,1... | collective-permute-start | bytes 4718600 | tf_op jit(solution)/shard_map/ppermute | solution.py:17
  6.1 3.0 %route.1 = (bf16[256,2048]{1,0:T(8,128)(2,1)}, f32[256,128]{1,0:T(8,128)}) custom-call(s32[1]{0:T(128)} %bitcast.1.quarter_ref, s32[2,256]{1,0:T(2,128)} %bitcast.60, f32[2,256]{1,0:T(2,128)} %bitcast.61, bf16[256,2048]{1,0:T(8,128)(2,1)} %rows_ref.2, f32[1,2048]{1,0:T(1,128)} %bitcast.58), custom_call_target="tpu_custom_call" | custom-call | tf_op jit(solution)/shard_map/route/pallas_call | solution.py:70
  9.2 13.0 %all-to-all-start = ((bf16[32,8,2048]{2,1,0:T(8,128)(2,1)}), bf16[32,8,2048]{2,1,0:T(8,128)(2,1)}, u32[]{:S(2)}, u32[]{:S(2)}) async-start(bf16[32,8,2048]{2,1,0:T(8,128)(2,1)} %bitcast.51), calls=%async_computation | async-start | bytes 2097152 | tf_op jit(solution)/shard_map/all_to_all | solution.py:315
  22.2 3.1 %collective-permute-start = (bf16[6144,128]{1,0:T(8,128)(2,1)S(1)}, bf16[6144,128]{1,0:T(8,128)(2,1)}, u32[]{:S(2)}, u32[]{:S(2)}) collective-permute-start(bf16[6144,128]{1,0:T(8,128)(2,1)S(1)} %pad_maximum_fusion.a0), channel_id=1, source_target_pairs={{0,1},{1,0},{2,3},{3,2},{4,5},{5,4},{6,7},{7,6},{8,9},{9,8},{10,11... | collective-permute-start | bytes 4718600 | tf_op jit(solution)/shard_map/ppermute | solution.py:17
  25.3 10.1 %collective-permute-done.1.a2 = bf16[6144,128]{1,0:T(8,128)(2,1)S(1)} collective-permute-done((bf16[6144,128]{1,0:T(8,128)(2,1)S(1)}, bf16[6144,128]{1,0:T(8,128)(2,1)S(1)}, u32[]{:S(2)}, u32[]{:S(2)}) %collective-permute-start.1) | collective-permute-done | bytes 1572896 | tf_op jit(solution)/shard_map/ppermute | solution.py:17
  35.4 8.0 %collective-permute-start.2 = (bf16[6144,128]{1,0:T(8,128)(2,1)S(1)}, bf16[6144,128]{1,0:T(8,128)(2,1)}, u32[]{:S(2)}, u32[]{:S(2)}) collective-permute-start(bf16[6144,128]{1,0:T(8,128)(2,1)S(1)} %collective-permute-done.1.a2), channel_id=1, source_target_pairs={{0,1},{1,0},{2,3},{3,2},{4,5},{5,4},{6,7},{7,6},{8,9},{9,8},{10,11... | collective-permute-start | bytes 4718600 | tf_op jit(solution)/shard_map/ppermute | solution.py:17
  43.4 0.8 slice.21
  44.1 3.3 %collective-permute-start.3 = (bf16[8,2048]{1,0:T(8,128)(2,1)S(1)}, bf16[8,2048]{1,0:T(8,128)(2,1)S(1)}, u32[]{:S(2)}, u32[]{:S(2)}) collective-permute-start(bf16[8,2048]{1,0:T(8,128)(2,1)S(1)} %slice.21), channel_id=1, source_target_pairs={{0,16},{16,32},{32,48},{48,64},{64,80},{80,96},{96,112},{112,128},... | collective-permute-start | bytes 98312 | tf_op jit(solution)/shard_map/ppermute | solution.py:310
  47.4 1.0 collective-permute-done.3.before_ref
  48.4 0.6 copy-done.6
  49.0 3.5 %mixer.1 = (bf16[128,1024]{1,0:T(8,128)(2,1)}, bf16[128,1024]{1,0:T(8,128)(2,1)}) custom-call(s32[1]{0:T(128)} %bitcast.core_ref, bf16[8,2048]{1,0:T(8,128)(2,1)} %copy-done.6, bf16[128,2048]{1,0:T(8,128)(2,1)} %rows_ref.3, f32[1,2048]{1,0:T(1,128)} %bitcast.59, bf16[64,2048]{1,0:T(8,128)(2,1)} %bitcast.55, bf16[64,2048]{1,0:T(8,128)(2,1)} %bitcast.56, ...), custom_call_target="tpu_custom_call" | custom-call | tf_op jit(solution)/shard_map/mixer/pallas_call | solution.py:118
  52.5 2.8 %collective-permute-start.4 = (bf16[128,1024]{1,0:T(8,128)(2,1)}, bf16[128,1024]{1,0:T(8,128)(2,1)S(1)}, u32[]{:S(2)}, u32[]{:S(2)}) collective-permute-start(bf16[128,1024]{1,0:T(8,128)(2,1)} %get-tuple-element.9), channel_id=1, source_target_pairs={{0,1},{1,0},{2,3},{3,2},{4,5},{5,4},{6,7},{7,6},{8,9},{9,8},{10,11... | collective-permute-start | bytes 786440 | tf_op jit(solution)/shard_map/ppermute | solution.py:129
  55.3 6.2 %expert_ffn.1 = bf16[256,2048]{1,0:T(8,128)(2,1)} custom-call(bf16[256,2048]{1,0:T(8,128)(2,1)} %bitcast.6.x_hbm, bf16[6144,128]{1,0:T(8,128)(2,1)} %copy-done, bf16[6144,128]{1,0:T(8,128)(2,1)} %collective-permute-done.a1, bf16[6144,128]{1,0:T(8,128)(2,1)} %copy-done.1, bf16[6144,128]{1,0:T(8,128)(2,1)} %collective-permute-done.2.a3, ...), custom_call_target="tpu_custom_call" | custom-call | flops 1610612736 | bytes 8388608 | tf_op jit(solution)/shard_map/expert_ffn/pallas_call | solution.py:181
  61.5 0.0 copy-start.5
  61.5 22.4 %all-to-all-start.1 = ((bf16[512,8,128]{2,1,0:T(8,128)(2,1)}), bf16[512,8,128]{2,1,0:T(8,128)(2,1)S(1)}, u32[]{:S(2)}, u32[]{:S(2)}) async-start(bf16[512,8,128]{2,1,0:T(8,128)(2,1)} %bitcast.47), calls=%async_computation.1 | async-start | bytes 2097152 | tf_op jit(solution)/shard_map/all_to_all | solution.py:332
  84.0 0.1 add_convert_fusion
  84.1 3.3 %collective-permute-start.5 = (bf16[128,512]{1,0:T(8,128)(2,1)S(1)}, bf16[128,512]{1,0:T(8,128)(2,1)S(1)}, u32[]{:S(2)}, u32[]{:S(2)}) collective-permute-start(bf16[128,512]{1,0:T(8,128)(2,1)S(1)} %broadcast_select_fusion), channel_id=1, source_target_pairs={{0,2},{2,0},{1,3},{3,1},{4,6},{6,4},{5,7},{7,5},{8,10},{10,8},{9,1... | collective-permute-start | bytes 393224 | tf_op jit(solution)/shard_map/ppermute | solution.py:129
  87.3 20.2 %collective-permute-done.5 = bf16[128,512]{1,0:T(8,128)(2,1)S(1)} collective-permute-done((bf16[128,512]{1,0:T(8,128)(2,1)S(1)}, bf16[128,512]{1,0:T(8,128)(2,1)S(1)}, u32[]{:S(2)}, u32[]{:S(2)}) %collective-permute-start.5) | collective-permute-done | bytes 131104 | tf_op jit(solution)/shard_map/ppermute | solution.py:129
  107.5 0.1 add_convert_fusion.1
  107.6 6.5 %collective-permute-start.6 = (bf16[128,256]{1,0:T(8,128)(2,1)S(1)}, bf16[128,256]{1,0:T(8,128)(2,1)S(1)}, u32[]{:S(2)}, u32[]{:S(2)}) collective-permute-start(bf16[128,256]{1,0:T(8,128)(2,1)S(1)} %broadcast_select_fusion.1), channel_id=1, source_target_pairs={{0,8},{4,12},{8,0},{12,4},{1,9},{5,13},{9,1},{13,5},{2,10},{6,14},... | collective-permute-start | bytes 196616 | tf_op jit(solution)/shard_map/ppermute | solution.py:129
  114.2 2.6 %collective-permute-done.6 = bf16[128,256]{1,0:T(8,128)(2,1)S(1)} collective-permute-done((bf16[128,256]{1,0:T(8,128)(2,1)S(1)}, bf16[128,256]{1,0:T(8,128)(2,1)S(1)}, u32[]{:S(2)}, u32[]{:S(2)}) %collective-permute-start.6) | collective-permute-done | bytes 65568 | tf_op jit(solution)/shard_map/ppermute | solution.py:129
  116.9 4.4 %collective-permute-start.7 = (bf16[128,128]{1,0:T(8,128)(2,1)S(1)}, bf16[128,128]{1,0:T(8,128)(2,1)S(1)}, u32[]{:S(2)}, u32[]{:S(2)}) collective-permute-start(bf16[128,128]{1,0:T(8,128)(2,1)S(1)} %broadcast_select_fusion.2), channel_id=1, source_target_pairs={{0,4},{4,0},{8,12},{12,8},{1,5},{5,1},{9,13},{13,9},{2,6},{6,2},{1... | collective-permute-start | bytes 98312 | tf_op jit(solution)/shard_map/ppermute | solution.py:129
  121.3 1.6 collective-permute-done.7
  122.9 0.6 add_convert_fusion.3.mixer_ref
  123.5 1.0 copy-done.2
  124.5 2.8 %combine.1 = bf16[384,128]{1,0:T(8,128)(2,1)} custom-call(f32[256,128]{1,0:T(8,128)} %get-tuple-element.6.picks_ref, bf16[32,4,32,128]{3,2,1,0:T(8,128)(2,1)} %bitcast.48, bf16[128,128]{1,0:T(8,128)(2,1)} %add_convert_fusion.3.mixer_ref), custom_call_target="tpu_custom_call" | custom-call | tf_op jit(solution)/shard_map/combine/pallas_call | solution.py:234
  127.3 22.2 %all-gather = bf16[3072,128]{1,0:T(8,128)(2,1)S(1)} all-gather(bf16[384,128]{1,0:T(8,128)(2,1)} %combine.1), channel_id=2, replica_groups=mesh['ep'=32,'p'=4,'q'=2,'c'=2] {'p','q'}, dimensions={0}, use_global_device_ids=true | all-gather | bytes 884736 | tf_op jit(solution)/shard_map/all_gather | solution.py:337
  149.4 9.4 %collective-permute-start.8 = (bf16[8,384,128]{2,1,0:T(8,128)(2,1)S(1)}, bf16[8,384,128]{2,1,0:T(8,128)(2,1)S(1)}, u32[]{:S(2)}, u32[]{:S(2)}) collective-permute-start(bf16[8,384,128]{2,1,0:T(8,128)(2,1)S(1)} %bitcast.49), channel_id=1, source_target_pairs={{0,1},{1,0},{2,3},{3,2},{4,5},{5,4},{6,7},{7,6},{8,9},{9,8},{10,11... | collective-permute-start | bytes 2359304 | tf_op jit(solution)/shard_map/ppermute | solution.py:17
  158.8 1.9 %collective-permute-done.8.other_ref = bf16[8,384,128]{2,1,0:T(8,128)(2,1)S(1)} collective-permute-done((bf16[8,384,128]{2,1,0:T(8,128)(2,1)S(1)}, bf16[8,384,128]{2,1,0:T(8,128)(2,1)S(1)}, u32[]{:S(2)}, u32[]{:S(2)}) %collective-permute-start.8) | collective-permute-done | bytes 786464 | tf_op jit(solution)/shard_map/ppermute | solution.py:17
  160.7 0.9 copy-done.4
  161.6 2.8 %assemble.1 = (bf16[128,2048]{1,0:T(8,128)(2,1)}, bf16[256,2048]{1,0:T(8,128)(2,1)}) custom-call(s32[1]{0:T(128)} %bitcast.core_ref, bf16[8,384,128]{2,1,0:T(8,128)(2,1)} %bitcast.50, bf16[8,384,128]{2,1,0:T(8,128)(2,1)} %copy-done.4), custom_call_target="tpu_custom_call" | custom-call | tf_op jit(solution)/shard_map/assemble/pallas_call | solution.py:262
  (19 shorter events, 0.1 us)
Async XLA Ops:
  2.1 20.1 %copy-start = (bf16[6144,128]{1,0:T(8,128)(2,1)}, bf16[6144,128]{1,0:T(8,128)(2,1)S(1)}, u32[]{:S(2)}) copy-start(bf16[6144,128]{1,0:T(8,128)(2,1)S(1)} %pad_maximum_fusion.a0) | copy-start | bytes 4718596
  2.1 33.3 %collective-permute-start.1 = (bf16[6144,128]{1,0:T(8,128)(2,1)S(1)}, bf16[6144,128]{1,0:T(8,128)(2,1)S(1)}, u32[]{:S(2)}, u32[]{:S(2)}) collective-permute-start(bf16[6144,128]{1,0:T(8,128)(2,1)S(1)} %pad_maximum_fusion.a0), channel_id=1, source_target_pairs={{0,2},{2,0},{1,3},{3,1},{4,6},{6,4},{5,7},{7,5},{8,10},{10,8},{9,1... | collective-permute-start | bytes 4718600 | tf_op jit(solution)/shard_map/ppermute | solution.py:17
  9.2 46.1 %all-to-all-start = ((bf16[32,8,2048]{2,1,0:T(8,128)(2,1)}), bf16[32,8,2048]{2,1,0:T(8,128)(2,1)}, u32[]{:S(2)}, u32[]{:S(2)}) async-start(bf16[32,8,2048]{2,1,0:T(8,128)(2,1)} %bitcast.51), calls=%async_computation | async-start | bytes 2097152 | tf_op jit(solution)/shard_map/all_to_all | solution.py:315
  22.2 33.1 %collective-permute-start = (bf16[6144,128]{1,0:T(8,128)(2,1)S(1)}, bf16[6144,128]{1,0:T(8,128)(2,1)}, u32[]{:S(2)}, u32[]{:S(2)}) collective-permute-start(bf16[6144,128]{1,0:T(8,128)(2,1)S(1)} %pad_maximum_fusion.a0), channel_id=1, source_target_pairs={{0,1},{1,0},{2,3},{3,2},{4,5},{5,4},{6,7},{7,6},{8,9},{9,8},{10,11... | collective-permute-start | bytes 4718600 | tf_op jit(solution)/shard_map/ppermute | solution.py:17
  35.4 19.9 %copy-start.1 = (bf16[6144,128]{1,0:T(8,128)(2,1)}, bf16[6144,128]{1,0:T(8,128)(2,1)S(1)}, u32[]{:S(2)}) copy-start(bf16[6144,128]{1,0:T(8,128)(2,1)S(1)} %collective-permute-done.1.a2) | copy-start | bytes 4718596
  35.4 19.9 %collective-permute-start.2 = (bf16[6144,128]{1,0:T(8,128)(2,1)S(1)}, bf16[6144,128]{1,0:T(8,128)(2,1)}, u32[]{:S(2)}, u32[]{:S(2)}) collective-permute-start(bf16[6144,128]{1,0:T(8,128)(2,1)S(1)} %collective-permute-done.1.a2), channel_id=1, source_target_pairs={{0,1},{1,0},{2,3},{3,2},{4,5},{5,4},{6,7},{7,6},{8,9},{9,8},{10,11... | collective-permute-start | bytes 4718600 | tf_op jit(solution)/shard_map/ppermute | solution.py:17
  44.1 4.3 %collective-permute-start.3 = (bf16[8,2048]{1,0:T(8,128)(2,1)S(1)}, bf16[8,2048]{1,0:T(8,128)(2,1)S(1)}, u32[]{:S(2)}, u32[]{:S(2)}) collective-permute-start(bf16[8,2048]{1,0:T(8,128)(2,1)S(1)} %slice.21), channel_id=1, source_target_pairs={{0,16},{16,32},{32,48},{48,64},{64,80},{80,96},{96,112},{112,128},... | collective-permute-start | bytes 98312 | tf_op jit(solution)/shard_map/ppermute | solution.py:310
  48.4 0.6 copy-start.6
  52.5 31.4 %collective-permute-start.4 = (bf16[128,1024]{1,0:T(8,128)(2,1)}, bf16[128,1024]{1,0:T(8,128)(2,1)S(1)}, u32[]{:S(2)}, u32[]{:S(2)}) collective-permute-start(bf16[128,1024]{1,0:T(8,128)(2,1)} %get-tuple-element.9), channel_id=1, source_target_pairs={{0,1},{1,0},{2,3},{3,2},{4,5},{5,4},{6,7},{7,6},{8,9},{9,8},{10,11... | collective-permute-start | bytes 786440 | tf_op jit(solution)/shard_map/ppermute | solution.py:129
  61.5 22.5 %copy-start.5 = (bf16[128,1024]{1,0:T(8,128)(2,1)S(1)}, bf16[128,1024]{1,0:T(8,128)(2,1)}, u32[]{:S(2)}) copy-start(bf16[128,1024]{1,0:T(8,128)(2,1)} %get-tuple-element.8) | copy-start | bytes 786436
  61.5 62.0 %all-to-all-start.1 = ((bf16[512,8,128]{2,1,0:T(8,128)(2,1)}), bf16[512,8,128]{2,1,0:T(8,128)(2,1)S(1)}, u32[]{:S(2)}, u32[]{:S(2)}) async-start(bf16[512,8,128]{2,1,0:T(8,128)(2,1)} %bitcast.47), calls=%async_computation.1 | async-start | bytes 2097152 | tf_op jit(solution)/shard_map/all_to_all | solution.py:332
  84.1 23.5 %collective-permute-start.5 = (bf16[128,512]{1,0:T(8,128)(2,1)S(1)}, bf16[128,512]{1,0:T(8,128)(2,1)S(1)}, u32[]{:S(2)}, u32[]{:S(2)}) collective-permute-start(bf16[128,512]{1,0:T(8,128)(2,1)S(1)} %broadcast_select_fusion), channel_id=1, source_target_pairs={{0,2},{2,0},{1,3},{3,1},{4,6},{6,4},{5,7},{7,5},{8,10},{10,8},{9,1... | collective-permute-start | bytes 393224 | tf_op jit(solution)/shard_map/ppermute | solution.py:129
  107.6 9.2 %collective-permute-start.6 = (bf16[128,256]{1,0:T(8,128)(2,1)S(1)}, bf16[128,256]{1,0:T(8,128)(2,1)S(1)}, u32[]{:S(2)}, u32[]{:S(2)}) collective-permute-start(bf16[128,256]{1,0:T(8,128)(2,1)S(1)} %broadcast_select_fusion.1), channel_id=1, source_target_pairs={{0,8},{4,12},{8,0},{12,4},{1,9},{5,13},{9,1},{13,5},{2,10},{6,14},... | collective-permute-start | bytes 196616 | tf_op jit(solution)/shard_map/ppermute | solution.py:129
  116.9 6.0 %collective-permute-start.7 = (bf16[128,128]{1,0:T(8,128)(2,1)S(1)}, bf16[128,128]{1,0:T(8,128)(2,1)S(1)}, u32[]{:S(2)}, u32[]{:S(2)}) collective-permute-start(bf16[128,128]{1,0:T(8,128)(2,1)S(1)} %broadcast_select_fusion.2), channel_id=1, source_target_pairs={{0,4},{4,0},{8,12},{12,8},{1,5},{5,1},{9,13},{13,9},{2,6},{6,2},{1... | collective-permute-start | bytes 98312 | tf_op jit(solution)/shard_map/ppermute | solution.py:129
  123.5 1.0 copy-start.2
  149.4 11.3 %copy-start.3 = (bf16[3072,128]{1,0:T(8,128)(2,1)}, bf16[3072,128]{1,0:T(8,128)(2,1)S(1)}, u32[]{:S(2)}) copy-start(bf16[3072,128]{1,0:T(8,128)(2,1)S(1)} %all-gather) | copy-start | bytes 2359300
  149.4 11.3 %collective-permute-start.8 = (bf16[8,384,128]{2,1,0:T(8,128)(2,1)S(1)}, bf16[8,384,128]{2,1,0:T(8,128)(2,1)S(1)}, u32[]{:S(2)}, u32[]{:S(2)}) collective-permute-start(bf16[8,384,128]{2,1,0:T(8,128)(2,1)S(1)} %bitcast.49), channel_id=1, source_target_pairs={{0,1},{1,0},{2,3},{3,2},{4,5},{5,4},{6,7},{7,6},{8,9},{9,8},{10,11... | collective-permute-start | bytes 2359304 | tf_op jit(solution)/shard_map/ppermute | solution.py:17
  160.7 0.9 copy-start.4

commit v5 on v4

--- a/solution.py
+++ b/solution.py
@@ -207,7 +207,9 @@
     return value.reshape(-1, width // part, 8, part).transpose(0, 2, 1, 3).reshape(-1, width)
 
 
-def combine_kernel(picks_ref, rows_ref, mixer_ref, out_ref, *, picks):
+def combine_kernel(picks_ref, rows_hbm, main_ref, tail_ref, rows_ref, sem, *, picks):
+    copy = pltpu.make_async_copy(rows_hbm, rows_ref, sem)
+    copy.start()
     experts, groups, capacity, width = rows_ref.shape
     tokens = picks_ref.shape[0]
     slots = experts * capacity
@@ -218,6 +220,7 @@
         spread = jnp.where(column == key, picks_ref[:, picks + k : picks + k + 1], spread)
     high = spread.astype(jnp.bfloat16)
     low = (spread - high.astype(jnp.float32)).astype(jnp.bfloat16)
+    copy.wait()
     total = jnp.zeros((tokens, 2 * width), jnp.float32)
     for g in range(0, groups, 2):
         rows = jnp.concatenate(
@@ -225,50 +228,57 @@
         )
         total = total + jnp.dot(high, rows, preferred_element_type=jnp.float32)
         total = total + jnp.dot(low, rows, preferred_element_type=jnp.float32)
-    length = mixer_ref.shape[0]
-    out_ref[:length, :] = mixer_ref[...]
-    out_ref[length:, :] = (total[:, :width] + total[:, width:]).astype(jnp.bfloat16)
-
-
-def combined(table, rows, mixer_part, picks):
+    result = (total[:, :width] + total[:, width:]).astype(jnp.bfloat16)
+    head = main_ref.shape[0]
+    main_ref[...] = result[:head]
+    for i in range(tail_ref.shape[0]):
+        tail_ref[i] = result[head:]
+
+
+def combined(table, rows, picks, copies, tail):
+    tokens, width = table.shape[0], rows.shape[-1]
     return pl.pallas_call(
         functools.partial(combine_kernel, picks=picks),
-        out_shape=jax.ShapeDtypeStruct((mixer_part.shape[0] + table.shape[0], rows.shape[-1]), jnp.bfloat16),
-        in_specs=[VM] * 3,
+        out_shape=(
+            jax.ShapeDtypeStruct((tokens - tail, width), jnp.bfloat16),
+            jax.ShapeDtypeStruct((copies, tail, width), jnp.bfloat16),
+        ),
+        in_specs=[VM, HBM],
+        out_specs=(VM, VM),
+        scratch_shapes=[pltpu.VMEM(rows.shape, jnp.bfloat16), pltpu.SemaphoreType.DMA],
+        name="combine",
+    )(table, rows)
+
+
+def column_kernel(*refs, places):
+    *parts, out_ref, sems = refs
+    copies, at = [], 0
+    for part in parts:
+        count, rows, width = part.shape
+        for i in range(count):
+            copies.append(
+                pltpu.make_async_copy(
+                    part.at[i],
+                    out_ref.at[pl.ds(at, rows), pl.ds(places[i] * width, width)],
+                    sems.at[len(copies)],
+                )
+            )
+            copies[-1].start()
+        at += rows
+    for copy in copies:
+        copy.wait()
+
+
+def side_by_side(places, *parts):
+    count, _, width = parts[0].shape
+    return pl.pallas_call(
+        functools.partial(column_kernel, places=places),
+        out_shape=jax.ShapeDtypeStruct((sum(p.shape[1] for p in parts), count * width), jnp.bfloat16),
+        in_specs=[HBM] * len(parts),
         out_specs=VM,
-        name="combine",
-    )(table, rows, mixer_part)
-
-
-def assemble_kernel(core_ref, mine_ref, other_ref, mixer_ref, routed_ref):
-    count, _, piece = mine_ref.shape
-    length = mixer_ref.shape[0]
-    first = core_ref[0] == 0
-    for i in range(count):
-        mine, other = mine_ref[i], other_ref[i]
-        lower = jnp.where(first, mine, other)
-        upper = jnp.where(first, other, mine)
-        at = 2 * i * piece
-        routed_ref[:, at : at + piece] = lower[length:]
-        routed_ref[:, at + piece : at + 2 * piece] = upper[length:]
-        at = (i % 2 * (count // 2) + i // 2) * piece
-        mixer_ref[:, at : at + piece] = lower[:length]
-        at += count * piece
-        mixer_ref[:, at : at + piece] = upper[:length]
-
-
-def assembled(core, mine, other, length):
-    count, rows, piece = mine.shape
-    return pl.pallas_call(
-        assemble_kernel,
-        out_shape=(
-            jax.ShapeDtypeStruct((length, 2 * count * piece), jnp.bfloat16),
-            jax.ShapeDtypeStruct((rows - length, 2 * count * piece), jnp.bfloat16),
-        ),
-        in_specs=[pl.BlockSpec(memory_space=pltpu.SMEM), VM, VM],
-        out_specs=(VM, VM),
-        name="assemble",
-    )(core.reshape(1), mine, other)
+        scratch_shapes=[pltpu.SemaphoreType.DMA((count * len(parts),))],
+        name="side_by_side",
+    )(*parts)
 
 
 def on_device(
@@ -332,11 +342,13 @@
     back = lax.all_to_all(
         back.reshape(experts * parts, share, piece), ALL, split_axis=0, concat_axis=0, tiled=True
     )
-    pieces = combined(table, back.reshape(experts, groups, capacity, piece), mixer_part, pick_count)
-
-    mine = lax.all_gather(pieces, ("p", "q"), axis=0, tiled=False)
-    other = flipped(mine, "c")
-    return assembled(core, mine, other, length)
+    mixer_all = lax.all_gather(mixer_part, TP, axis=0, tiled=False)
+    mixer_whole = side_by_side([i % 2 * 8 + i // 2 % 2 * 4 + i // 4 for i in range(parts)], mixer_all)
+
+    main, tail = combined(table, back.reshape(experts, groups, capacity, piece), pick_count, parts, 8)
+    tail_all = lax.all_to_all(tail, TP, split_axis=0, concat_axis=0, tiled=True)
+    main_all = lax.all_gather(main, TP, axis=0, tiled=False)
+    return mixer_whole, side_by_side(list(range(parts)), main_all, tail_all)
 
 
 def solution(mesh):

time: 165 us -> 183 us (1.11)
  blocking collectives: 22.2 us -> 44.5 us
  starting transfers between devices: 80.2 us -> 75.9 us
  Pallas kernels: 18.3 us -> 20.6 us
  waiting for transfers between devices: 37.4 us -> 35.5 us
    all_gather x1 -> x2, blocking collectives: 22.2 us -> 44.5 us  [the longest x1 22.9 us: on_device(): mixer_all = lax.all_gather(mixer_part, TP, axis=0, tiled=False)]
    ppermute x4 -> x3, starting transfers between devices: 24.5 us -> 15.1 us  [flipped(): return lax.ppermute(value, axis, [(0, 1), (1, 0)])]
    all_to_all x0 -> x1, starting transfers between devices: none -> 5.04 us  [on_device(): tail_all = lax.all_to_all(tail, TP, split_axis=0, concat_axis=0, tiled=True)]
    ppermute x4 -> x3, waiting for transfers between devices: 12 us -> 10.1 us  [flipped(): return lax.ppermute(value, axis, [(0, 1), (1, 0)])]
    pallas_call x1 -> x2, Pallas kernels: 2.84 us -> 4.43 us  [side_by_side(): pl.pallas_call(functools.partial(column_kernel, places=places), out_shape...]
  transfers between devices with their start and end apart: 11 -> 11, of which waited for: 6 -> 5; matrix products, arithmetic and copies ran while one was open for 1% -> 1% of each run, Pallas kernels for 8% -> 8%
where the time goes in v5:
time: 183 us; the launch traced here: 182 us
  starting transfers between devices  75.9 us (41%)
  blocking collectives  44.5 us (24%)
  waiting for transfers between devices  35.5 us (19%)
  Pallas kernels  20.6 us (11%)
  local copies, waits for them, and re-layouts  2.97 us (2%)
    ppermute x4, waiting for transfers between devices, summed(): received = lax.ppermute(sent, axis, pairs)  24.4 us
    all_gather x1, blocking collectives, on_device(): mixer_all = lax.all_gather(mixer_part, TP, axis=0, tiled=False)  22.9 us
    all_to_all x1, starting transfers between devices, on_device(): lax.all_to_all(back.reshape(experts * parts, share, piece), ALL, split_ax...  22.4 us
    all_gather x1, blocking collectives, on_device(): main_all = lax.all_gather(main, TP, axis=0, tiled=False)  21.6 us
    ppermute x4, starting transfers between devices, summed(): received = lax.ppermute(sent, axis, pairs)  17 us
    ppermute x3, starting transfers between devices, flipped(): return lax.ppermute(value, axis, [(0, 1), (1, 0)])  15.1 us
    all_to_all x1, starting transfers between devices, on_device(): lax.all_to_all(outgoing.reshape(experts, share, width), 'ep', split_axis=...  13 us
    ppermute x3, waiting for transfers between devices, flipped(): return lax.ppermute(value, axis, [(0, 1), (1, 0)])  10.1 us
  transfers between devices with their start and end apart: 11, of which 5 were waited for; matrix products, arithmetic and copies ran while one was open for 1% of the time, Pallas kernels for 8%

profile of v5, /device:TPU:1, one launch (start us, length us, event | category | flops | bytes accessed | tf_op | source)
XLA Modules:
  0.0 182.0 jit_solution(15832727138627285273)
XLA Ops:
  0.6 1.5 pad_maximum_fusion.a0
  2.1 4.0 %collective-permute-start.6 = (bf16[6144,128]{1,0:T(8,128)(2,1)S(1)}, bf16[6144,128]{1,0:T(8,128)(2,1)S(1)}, u32[]{:S(2)}, u32[]{:S(2)}) collective-permute-start(bf16[6144,128]{1,0:T(8,128)(2,1)S(1)} %pad_maximum_fusion.a0), channel_id=1, source_target_pairs={{0,2},{2,0},{1,3},{3,1},{4,6},{6,4},{5,7},{7,5},{8,10},{10,8},{9,1... | collective-permute-start | bytes 4718600 | tf_op jit(solution)/shard_map/ppermute | solution.py:17
  6.1 3.0 %route.1 = (bf16[256,2048]{1,0:T(8,128)(2,1)}, f32[256,128]{1,0:T(8,128)}) custom-call(s32[1]{0:T(128)} %bitcast.6.quarter_ref, s32[2,256]{1,0:T(2,128)} %bitcast.61, f32[2,256]{1,0:T(2,128)} %bitcast.62, bf16[256,2048]{1,0:T(8,128)(2,1)} %rows_ref.3, f32[1,2048]{1,0:T(1,128)} %bitcast.59), custom_call_target="tpu_custom_call" | custom-call | tf_op jit(solution)/shard_map/route/pallas_call | solution.py:70
  9.2 13.0 %all-to-all-start = ((bf16[32,8,2048]{2,1,0:T(8,128)(2,1)}), bf16[32,8,2048]{2,1,0:T(8,128)(2,1)}, u32[]{:S(2)}, u32[]{:S(2)}) async-start(bf16[32,8,2048]{2,1,0:T(8,128)(2,1)} %bitcast.52), calls=%async_computation | async-start | bytes 2097152 | tf_op jit(solution)/shard_map/all_to_all | solution.py:325
  22.2 3.1 %collective-permute-start.5 = (bf16[6144,128]{1,0:T(8,128)(2,1)S(1)}, bf16[6144,128]{1,0:T(8,128)(2,1)}, u32[]{:S(2)}, u32[]{:S(2)}) collective-permute-start(bf16[6144,128]{1,0:T(8,128)(2,1)S(1)} %pad_maximum_fusion.a0), channel_id=1, source_target_pairs={{0,1},{1,0},{2,3},{3,2},{4,5},{5,4},{6,7},{7,6},{8,9},{9,8},{10,11... | collective-permute-start | bytes 4718600 | tf_op jit(solution)/shard_map/ppermute | solution.py:17
  25.3 10.1 %collective-permute-done.6.a2 = bf16[6144,128]{1,0:T(8,128)(2,1)S(1)} collective-permute-done((bf16[6144,128]{1,0:T(8,128)(2,1)S(1)}, bf16[6144,128]{1,0:T(8,128)(2,1)S(1)}, u32[]{:S(2)}, u32[]{:S(2)}) %collective-permute-start.6) | collective-permute-done | bytes 1572896 | tf_op jit(solution)/shard_map/ppermute | solution.py:17
  35.4 8.0 %collective-permute-start.7 = (bf16[6144,128]{1,0:T(8,128)(2,1)S(1)}, bf16[6144,128]{1,0:T(8,128)(2,1)}, u32[]{:S(2)}, u32[]{:S(2)}) collective-permute-start(bf16[6144,128]{1,0:T(8,128)(2,1)S(1)} %collective-permute-done.6.a2), channel_id=1, source_target_pairs={{0,1},{1,0},{2,3},{3,2},{4,5},{5,4},{6,7},{7,6},{8,9},{9,8},{10,11... | collective-permute-start | bytes 4718600 | tf_op jit(solution)/shard_map/ppermute | solution.py:17
  43.4 0.8 slice.21
  44.1 3.3 %collective-permute-start = (bf16[8,2048]{1,0:T(8,128)(2,1)S(1)}, bf16[8,2048]{1,0:T(8,128)(2,1)S(1)}, u32[]{:S(2)}, u32[]{:S(2)}) collective-permute-start(bf16[8,2048]{1,0:T(8,128)(2,1)S(1)} %slice.21), channel_id=1, source_target_pairs={{0,16},{16,32},{32,48},{48,64},{64,80},{80,96},{96,112},{112,128},... | collective-permute-start | bytes 98312 | tf_op jit(solution)/shard_map/ppermute | solution.py:320
  47.4 1.0 collective-permute-done.before_ref
  48.4 0.6 copy-done.5
  49.0 3.5 %mixer.1 = (bf16[128,1024]{1,0:T(8,128)(2,1)}, bf16[128,1024]{1,0:T(8,128)(2,1)}) custom-call(s32[1]{0:T(128)} %bitcast.core_ref, bf16[8,2048]{1,0:T(8,128)(2,1)} %copy-done.5, bf16[128,2048]{1,0:T(8,128)(2,1)} %rows_ref.2, f32[1,2048]{1,0:T(1,128)} %bitcast.60, bf16[64,2048]{1,0:T(8,128)(2,1)} %bitcast.56, bf16[64,2048]{1,0:T(8,128)(2,1)} %bitcast.57, ...), custom_call_target="tpu_custom_call" | custom-call | tf_op jit(solution)/shard_map/mixer/pallas_call | solution.py:118
  52.5 2.8 %collective-permute-start.1 = (bf16[128,1024]{1,0:T(8,128)(2,1)}, bf16[128,1024]{1,0:T(8,128)(2,1)S(1)}, u32[]{:S(2)}, u32[]{:S(2)}) collective-permute-start(bf16[128,1024]{1,0:T(8,128)(2,1)} %get-tuple-element.9), channel_id=1, source_target_pairs={{0,1},{1,0},{2,3},{3,2},{4,5},{5,4},{6,7},{7,6},{8,9},{9,8},{10,11... | collective-permute-start | bytes 786440 | tf_op jit(solution)/shard_map/ppermute | solution.py:129
  55.3 6.2 %expert_ffn.1 = bf16[256,2048]{1,0:T(8,128)(2,1)} custom-call(bf16[256,2048]{1,0:T(8,128)(2,1)} %bitcast.11.x_hbm, bf16[6144,128]{1,0:T(8,128)(2,1)} %copy-done, bf16[6144,128]{1,0:T(8,128)(2,1)} %collective-permute-done.5.a1, bf16[6144,128]{1,0:T(8,128)(2,1)} %copy-done.1, bf16[6144,128]{1,0:T(8,128)(2,1)} %collective-permute-done.7.a3, ...), custom_call_target="tpu_custom_call" | custom-call | flops 1610612736 | bytes 8388608 | tf_op jit(solution)/shard_map/expert_ffn/pallas_call | solution.py:181
  61.5 22.4 %all-to-all-start.1 = ((bf16[512,8,128]{2,1,0:T(8,128)(2,1)}), bf16[512,8,128]{2,1,0:T(8,128)(2,1)S(1)}, u32[]{:S(2)}, u32[]{:S(2)}) async-start(bf16[512,8,128]{2,1,0:T(8,128)(2,1)} %bitcast.48), calls=%async_computation.1 | async-start | bytes 2097152 | tf_op jit(solution)/shard_map/all_to_all | solution.py:342
  84.0 0.1 add_convert_fusion
  84.1 3.3 %collective-permute-start.2 = (bf16[128,512]{1,0:T(8,128)(2,1)S(1)}, bf16[128,512]{1,0:T(8,128)(2,1)S(1)}, u32[]{:S(2)}, u32[]{:S(2)}) collective-permute-start(bf16[128,512]{1,0:T(8,128)(2,1)S(1)} %broadcast_select_fusion), channel_id=1, source_target_pairs={{0,2},{2,0},{1,3},{3,1},{4,6},{6,4},{5,7},{7,5},{8,10},{10,8},{9,1... | collective-permute-start | bytes 393224 | tf_op jit(solution)/shard_map/ppermute | solution.py:129
  87.3 20.2 %collective-permute-done.2 = bf16[128,512]{1,0:T(8,128)(2,1)S(1)} collective-permute-done((bf16[128,512]{1,0:T(8,128)(2,1)S(1)}, bf16[128,512]{1,0:T(8,128)(2,1)S(1)}, u32[]{:S(2)}, u32[]{:S(2)}) %collective-permute-start.2) | collective-permute-done | bytes 131104 | tf_op jit(solution)/shard_map/ppermute | solution.py:129
  107.5 0.1 add_convert_fusion.1
  107.6 6.5 %collective-permute-start.3 = (bf16[128,256]{1,0:T(8,128)(2,1)S(1)}, bf16[128,256]{1,0:T(8,128)(2,1)S(1)}, u32[]{:S(2)}, u32[]{:S(2)}) collective-permute-start(bf16[128,256]{1,0:T(8,128)(2,1)S(1)} %broadcast_select_fusion.1), channel_id=1, source_target_pairs={{0,8},{4,12},{8,0},{12,4},{1,9},{5,13},{9,1},{13,5},{2,10},{6,14},... | collective-permute-start | bytes 196616 | tf_op jit(solution)/shard_map/ppermute | solution.py:129
  114.2 2.6 %collective-permute-done.3 = bf16[128,256]{1,0:T(8,128)(2,1)S(1)} collective-permute-done((bf16[128,256]{1,0:T(8,128)(2,1)S(1)}, bf16[128,256]{1,0:T(8,128)(2,1)S(1)}, u32[]{:S(2)}, u32[]{:S(2)}) %collective-permute-start.3) | collective-permute-done | bytes 65568 | tf_op jit(solution)/shard_map/ppermute | solution.py:129
  116.9 4.4 %collective-permute-start.4 = (bf16[128,128]{1,0:T(8,128)(2,1)S(1)}, bf16[128,128]{1,0:T(8,128)(2,1)S(1)}, u32[]{:S(2)}, u32[]{:S(2)}) collective-permute-start(bf16[128,128]{1,0:T(8,128)(2,1)S(1)} %broadcast_select_fusion.2), channel_id=1, source_target_pairs={{0,4},{4,0},{8,12},{12,8},{1,5},{5,1},{9,13},{13,9},{2,6},{6,2},{1... | collective-permute-start | bytes 98312 | tf_op jit(solution)/shard_map/ppermute | solution.py:129
  121.3 1.6 collective-permute-done.4
  122.9 22.9 %all-gather = bf16[2048,128]{1,0:T(8,128)(2,1)} all-gather(bf16[128,128]{1,0:T(8,128)(2,1)S(1)} %add_convert_fusion.3), channel_id=2, replica_groups=mesh['ep'=32,'p'=4,'q'=2,'c'=2] {'p','q','c'}, dimensions={0}, use_global_device_ids=true | all-gather | bytes 557056 | tf_op jit(solution)/shard_map/all_gather | solution.py:345
  145.8 1.9 %side_by_side.2 = bf16[128,2048]{1,0:T(8,128)(2,1)} custom-call(bf16[16,128,128]{2,1,0:T(8,128)(2,1)} %bitcast.51), custom_call_target="tpu_custom_call" | custom-call | tf_op jit(solution)/shard_map/side_by_side/pallas_call | solution.py:274
  147.7 0.0 copy-start.2
  147.7 1.0 copy-done.2
  148.7 3.5 %combine.1 = (bf16[248,128]{1,0:T(8,128)(2,1)}, bf16[16,8,128]{2,1,0:T(8,128)(2,1)}) custom-call(f32[256,128]{1,0:T(8,128)} %get-tuple-element.10.picks_ref, bf16[32,4,32,128]{3,2,1,0:T(8,128)(2,1)} %bitcast.49), custom_call_target="tpu_custom_call" | custom-call | tf_op jit(solution)/shard_map/combine/pallas_call | solution.py:240
  152.2 5.0 %all-to-all-start.2 = ((bf16[16,8,128]{2,1,0:T(8,128)(2,1)}), bf16[16,8,128]{2,1,0:T(8,128)(2,1)S(1)}, u32[]{:S(2)}, u32[]{:S(2)}) async-start(bf16[16,8,128]{2,1,0:T(8,128)(2,1)} %get-tuple-element.13), calls=%async_computation.2 | async-start | bytes 65536 | tf_op jit(solution)/shard_map/all_to_all | solution.py:349
  157.2 21.6 %all-gather.1 = bf16[3968,128]{1,0:T(8,128)(2,1)} all-gather(bf16[248,128]{1,0:T(8,128)(2,1)} %get-tuple-element.12), channel_id=3, replica_groups=mesh['ep'=32,'p'=4,'q'=2,'c'=2] {'p','q','c'}, dimensions={0}, use_global_device_ids=true | all-gather | bytes 1079296 | tf_op jit(solution)/shard_map/all_gather | solution.py:350
  178.9 0.6 copy-done.4
  179.5 2.5 %side_by_side.3 = bf16[256,2048]{1,0:T(8,128)(2,1)} custom-call(bf16[16,248,128]{2,1,0:T(8,128)(2,1)} %bitcast.50, bf16[16,8,128]{2,1,0:T(8,128)(2,1)} %copy-done.4), custom_call_target="tpu_custom_call" | custom-call | tf_op jit(solution)/shard_map/side_by_side/pallas_call | solution.py:274
  (19 shorter events, 0.1 us)
Async XLA Ops:
  2.1 20.1 %copy-start = (bf16[6144,128]{1,0:T(8,128)(2,1)}, bf16[6144,128]{1,0:T(8,128)(2,1)S(1)}, u32[]{:S(2)}) copy-start(bf16[6144,128]{1,0:T(8,128)(2,1)S(1)} %pad_maximum_fusion.a0) | copy-start | bytes 4718596
  2.1 33.3 %collective-permute-start.6 = (bf16[6144,128]{1,0:T(8,128)(2,1)S(1)}, bf16[6144,128]{1,0:T(8,128)(2,1)S(1)}, u32[]{:S(2)}, u32[]{:S(2)}) collective-permute-start(bf16[6144,128]{1,0:T(8,128)(2,1)S(1)} %pad_maximum_fusion.a0), channel_id=1, source_target_pairs={{0,2},{2,0},{1,3},{3,1},{4,6},{6,4},{5,7},{7,5},{8,10},{10,8},{9,1... | collective-permute-start | bytes 4718600 | tf_op jit(solution)/shard_map/ppermute | solution.py:17
  9.2 46.1 %all-to-all-start = ((bf16[32,8,2048]{2,1,0:T(8,128)(2,1)}), bf16[32,8,2048]{2,1,0:T(8,128)(2,1)}, u32[]{:S(2)}, u32[]{:S(2)}) async-start(bf16[32,8,2048]{2,1,0:T(8,128)(2,1)} %bitcast.52), calls=%async_computation | async-start | bytes 2097152 | tf_op jit(solution)/shard_map/all_to_all | solution.py:325
  22.2 33.1 %collective-permute-start.5 = (bf16[6144,128]{1,0:T(8,128)(2,1)S(1)}, bf16[6144,128]{1,0:T(8,128)(2,1)}, u32[]{:S(2)}, u32[]{:S(2)}) collective-permute-start(bf16[6144,128]{1,0:T(8,128)(2,1)S(1)} %pad_maximum_fusion.a0), channel_id=1, source_target_pairs={{0,1},{1,0},{2,3},{3,2},{4,5},{5,4},{6,7},{7,6},{8,9},{9,8},{10,11... | collective-permute-start | bytes 4718600 | tf_op jit(solution)/shard_map/ppermute | solution.py:17
  35.4 19.9 %copy-start.1 = (bf16[6144,128]{1,0:T(8,128)(2,1)}, bf16[6144,128]{1,0:T(8,128)(2,1)S(1)}, u32[]{:S(2)}) copy-start(bf16[6144,128]{1,0:T(8,128)(2,1)S(1)} %collective-permute-done.6.a2) | copy-start | bytes 4718596
  35.4 19.9 %collective-permute-start.7 = (bf16[6144,128]{1,0:T(8,128)(2,1)S(1)}, bf16[6144,128]{1,0:T(8,128)(2,1)}, u32[]{:S(2)}, u32[]{:S(2)}) collective-permute-start(bf16[6144,128]{1,0:T(8,128)(2,1)S(1)} %collective-permute-done.6.a2), channel_id=1, source_target_pairs={{0,1},{1,0},{2,3},{3,2},{4,5},{5,4},{6,7},{7,6},{8,9},{9,8},{10,11... | collective-permute-start | bytes 4718600 | tf_op jit(solution)/shard_map/ppermute | solution.py:17
  44.1 4.3 %collective-permute-start = (bf16[8,2048]{1,0:T(8,128)(2,1)S(1)}, bf16[8,2048]{1,0:T(8,128)(2,1)S(1)}, u32[]{:S(2)}, u32[]{:S(2)}) collective-permute-start(bf16[8,2048]{1,0:T(8,128)(2,1)S(1)} %slice.21), channel_id=1, source_target_pairs={{0,16},{16,32},{32,48},{48,64},{64,80},{80,96},{96,112},{112,128},... | collective-permute-start | bytes 98312 | tf_op jit(solution)/shard_map/ppermute | solution.py:320
  48.4 0.6 copy-start.5
  52.5 31.4 %collective-permute-start.1 = (bf16[128,1024]{1,0:T(8,128)(2,1)}, bf16[128,1024]{1,0:T(8,128)(2,1)S(1)}, u32[]{:S(2)}, u32[]{:S(2)}) collective-permute-start(bf16[128,1024]{1,0:T(8,128)(2,1)} %get-tuple-element.9), channel_id=1, source_target_pairs={{0,1},{1,0},{2,3},{3,2},{4,5},{5,4},{6,7},{7,6},{8,9},{9,8},{10,11... | collective-permute-start | bytes 786440 | tf_op jit(solution)/shard_map/ppermute | solution.py:129
  61.5 22.5 %copy-start.3 = (bf16[128,1024]{1,0:T(8,128)(2,1)S(1)}, bf16[128,1024]{1,0:T(8,128)(2,1)}, u32[]{:S(2)}) copy-start(bf16[128,1024]{1,0:T(8,128)(2,1)} %get-tuple-element.8) | copy-start | bytes 786436
  61.5 86.2 %all-to-all-start.1 = ((bf16[512,8,128]{2,1,0:T(8,128)(2,1)}), bf16[512,8,128]{2,1,0:T(8,128)(2,1)S(1)}, u32[]{:S(2)}, u32[]{:S(2)}) async-start(bf16[512,8,128]{2,1,0:T(8,128)(2,1)} %bitcast.48), calls=%async_computation.1 | async-start | bytes 2097152 | tf_op jit(solution)/shard_map/all_to_all | solution.py:342
  84.1 23.5 %collective-permute-start.2 = (bf16[128,512]{1,0:T(8,128)(2,1)S(1)}, bf16[128,512]{1,0:T(8,128)(2,1)S(1)}, u32[]{:S(2)}, u32[]{:S(2)}) collective-permute-start(bf16[128,512]{1,0:T(8,128)(2,1)S(1)} %broadcast_select_fusion), channel_id=1, source_target_pairs={{0,2},{2,0},{1,3},{3,1},{4,6},{6,4},{5,7},{7,5},{8,10},{10,8},{9,1... | collective-permute-start | bytes 393224 | tf_op jit(solution)/shard_map/ppermute | solution.py:129
  107.6 9.2 %collective-permute-start.3 = (bf16[128,256]{1,0:T(8,128)(2,1)S(1)}, bf16[128,256]{1,0:T(8,128)(2,1)S(1)}, u32[]{:S(2)}, u32[]{:S(2)}) collective-permute-start(bf16[128,256]{1,0:T(8,128)(2,1)S(1)} %broadcast_select_fusion.1), channel_id=1, source_target_pairs={{0,8},{4,12},{8,0},{12,4},{1,9},{5,13},{9,1},{13,5},{2,10},{6,14},... | collective-permute-start | bytes 196616 | tf_op jit(solution)/shard_map/ppermute | solution.py:129
  116.9 6.0 %collective-permute-start.4 = (bf16[128,128]{1,0:T(8,128)(2,1)S(1)}, bf16[128,128]{1,0:T(8,128)(2,1)S(1)}, u32[]{:S(2)}, u32[]{:S(2)}) collective-permute-start(bf16[128,128]{1,0:T(8,128)(2,1)S(1)} %broadcast_select_fusion.2), channel_id=1, source_target_pairs={{0,4},{4,0},{8,12},{12,8},{1,5},{5,1},{9,13},{13,9},{2,6},{6,2},{1... | collective-permute-start | bytes 98312 | tf_op jit(solution)/shard_map/ppermute | solution.py:129
  147.7 1.0 copy-start.2
  152.2 26.7 %all-to-all-start.2 = ((bf16[16,8,128]{2,1,0:T(8,128)(2,1)}), bf16[16,8,128]{2,1,0:T(8,128)(2,1)S(1)}, u32[]{:S(2)}, u32[]{:S(2)}) async-start(bf16[16,8,128]{2,1,0:T(8,128)(2,1)} %get-tuple-element.13), calls=%async_computation.2 | async-start | bytes 65536 | tf_op jit(solution)/shard_map/all_to_all | solution.py:349
  178.9 0.6 copy-start.4

commit v6 on v4

--- a/solution.py
+++ b/solution.py
@@ -108,13 +108,16 @@
     left = jnp.dot(gated, out_w_ref[:, :middle], preferred_element_type=jnp.float32).astype(jnp.bfloat16)
     right = jnp.dot(gated, out_w_ref[:, middle:], preferred_element_type=jnp.float32).astype(jnp.bfloat16)
     first = core_ref[0] == 0
-    keep_ref[...] = jnp.where(first, left, right)
-    send_ref[...] = jnp.where(first, right, left)
-
-
-def mixer_terms(core, before, rows, gain, inner, gate_in, gate_out, taps, out_weight):
+    piece = keep_ref.shape[2]
+    for i in range(keep_ref.shape[0]):
+        a, b = left[:, i * piece : (i + 1) * piece], right[:, i * piece : (i + 1) * piece]
+        keep_ref[i] = jnp.where(first, a, b)
+        send_ref[i] = jnp.where(first, b, a)
+
+
+def mixer_terms(core, before, rows, gain, inner, gate_in, gate_out, taps, out_weight, blocks):
     length, width = rows.shape
-    half = jax.ShapeDtypeStruct((length, width // 2), jnp.bfloat16)
+    half = jax.ShapeDtypeStruct((blocks, length, width // (2 * blocks)), jnp.bfloat16)
     return pl.pallas_call(
         mixer_kernel,
         out_shape=(half, half),
@@ -131,9 +134,28 @@
 
 
 def halves(value, first):
-    middle = value.shape[1] // 2
-    left, right = value[:, :middle], value[:, middle:]
+    middle = value.shape[0] // 2
+    left, right = value[:middle], value[middle:]
     return jnp.where(first, left, right), jnp.where(first, right, left)
+
+
+def spread_kernel(me_ref, kept_ref, received_ref, *out_refs):
+    count = kept_ref.shape[0]
+    for step, out_ref in enumerate(out_refs):
+        block = lax.rem(me_ref[0] + step, count)
+        total = kept_ref[block].astype(jnp.float32) + received_ref[block].astype(jnp.float32)
+        out_ref[...] = total.astype(jnp.bfloat16)
+
+
+def spread_blocks(me, kept, received):
+    count = kept.shape[0]
+    return pl.pallas_call(
+        spread_kernel,
+        out_shape=tuple(jax.ShapeDtypeStruct(kept.shape[1:], jnp.bfloat16) for _ in range(count)),
+        in_specs=[pl.BlockSpec(memory_space=pltpu.SMEM), VM, VM],
+        out_specs=(VM,) * count,
+        name="spread_blocks",
+    )(me.reshape(1), kept, received)
 
 
 def ffn_kernel(x_hbm, a0, a1, a2, a3, b0, b1, b2, b3, out_ref, x_ref, gu_ref, down_ref, hid_ref, sems):
@@ -240,35 +262,42 @@
     )(table, rows, mixer_part)
 
 
-def assemble_kernel(core_ref, mine_ref, other_ref, mixer_ref, routed_ref):
-    count, _, piece = mine_ref.shape
-    length = mixer_ref.shape[0]
-    first = core_ref[0] == 0
+def place_kernel(core_ref, parts_ref, *refs, length, flip):
+    mixer_ref, routed_ref, sems = refs[-3:]
+    count, rows, piece = parts_ref.shape
+    core = 1 - core_ref[0] if flip else core_ref[0]
+    copies = []
     for i in range(count):
-        mine, other = mine_ref[i], other_ref[i]
-        lower = jnp.where(first, mine, other)
-        upper = jnp.where(first, other, mine)
-        at = 2 * i * piece
-        routed_ref[:, at : at + piece] = lower[length:]
-        routed_ref[:, at + piece : at + 2 * piece] = upper[length:]
-        at = (i % 2 * (count // 2) + i // 2) * piece
-        mixer_ref[:, at : at + piece] = lower[:length]
-        at += count * piece
-        mixer_ref[:, at : at + piece] = upper[:length]
-
-
-def assembled(core, mine, other, length):
-    count, rows, piece = mine.shape
-    return pl.pallas_call(
-        assemble_kernel,
+        at = pl.multiple_of((2 * i + core) * piece, piece)
+        copies.append((length, rows - length, routed_ref, at))
+        at = pl.multiple_of((core * count + i % 2 * (count // 2) + i // 2) * piece, piece)
+        copies.append((0, length, mixer_ref, at))
+    copies = [
+        pltpu.make_async_copy(
+            parts_ref.at[n // 2, pl.ds(start, size), :], target.at[:, pl.ds(at, piece)], sems.at[n]
+        )
+        for n, (start, size, target, at) in enumerate(copies)
+    ]
+    for copy in copies:
+        copy.start()
+    for copy in copies:
+        copy.wait()
+
+
+def placed(core, parts, length, wholes=()):
+    count, rows, piece = parts.shape
+    return pl.pallas_call(
+        functools.partial(place_kernel, length=length, flip=bool(wholes)),
         out_shape=(
             jax.ShapeDtypeStruct((length, 2 * count * piece), jnp.bfloat16),
             jax.ShapeDtypeStruct((rows - length, 2 * count * piece), jnp.bfloat16),
         ),
-        in_specs=[pl.BlockSpec(memory_space=pltpu.SMEM), VM, VM],
-        out_specs=(VM, VM),
-        name="assemble",
-    )(core.reshape(1), mine, other)
+        in_specs=[pl.BlockSpec(memory_space=pltpu.SMEM), VM] + [HBM] * len(wholes),
+        out_specs=(HBM, HBM),
+        input_output_aliases={2: 0, 3: 1} if wholes else {},
+        scratch_shapes=[pltpu.SemaphoreType.DMA((2 * count,))],
+        name="placed",
+    )(core.reshape(1), parts, *wholes)
 
 
 def on_device(
@@ -319,13 +348,18 @@
     pack_qc = flipped(pack_q, "c")
 
     keep, send = mixer_terms(
-        core, before, mixer_rows, mixer_gain, inner_weight, gate_in_weight, gate_out_weight, conv_taps, mixer_out_weight
+        core, before, mixer_rows, mixer_gain, inner_weight, gate_in_weight, gate_out_weight, conv_taps, mixer_out_weight, parts // 2
     )
     swap = [(0, 1), (1, 0)]
     mixer_part = summed(keep, send, "c", swap)
-    mixer_part = summed(*halves(mixer_part, side == 0), "q", swap)
-    mixer_part = summed(*halves(mixer_part, column < 2), "p", [(i, i ^ 2) for i in range(groups)])
-    mixer_part = summed(*halves(mixer_part, column % 2 == 0), "p", [(i, i ^ 1) for i in range(groups)])
+    kept, sent = halves(mixer_part, side == 0)
+    received = lax.ppermute(sent, "q", swap)
+    blocks = spread_blocks(column, kept, received)
+    total = blocks[0].astype(jnp.float32)
+    for step in range(1, groups):
+        block = lax.ppermute(blocks[step], "p", [(i, (i + step) % groups) for i in range(groups)])
+        total = total + block.astype(jnp.float32)
+    mixer_part = total.astype(jnp.bfloat16)
 
     results = expert_ffn(slot_rows, (pack, pack_c, pack_q, pack_qc), sharers * hidden_part)
     back = results.reshape(experts, share, parts, piece).transpose(0, 2, 1, 3)
@@ -336,7 +370,8 @@
 
     mine = lax.all_gather(pieces, ("p", "q"), axis=0, tiled=False)
     other = flipped(mine, "c")
-    return assembled(core, mine, other, length)
+    wholes = placed(core, mine, length)
+    return placed(core, other, length, wholes)
 
 
 def solution(mesh):

time: 165 us -> 171 us (1.036)
  the two profiles are of different devices: /device:TPU:1 before, /device:TPU:385 now
where the time goes in v6:
time: 171 us; the launch traced here: 170 us
  starting transfers between devices  73.7 us (43%)
  waiting for transfers between devices  44.9 us (26%)
  Pallas kernels  21.3 us (12%)
  blocking collectives  20.9 us (12%)
  other arithmetic  4.54 us (3%)
  local copies, waits for them, and re-layouts  3.86 us (2%)
    ppermute x4, waiting for transfers between devices, flipped(): return lax.ppermute(value, axis, [(0, 1), (1, 0)])  23.2 us
    all_gather x1, blocking collectives, on_device(): mine = lax.all_gather(pieces, ('p', 'q'), axis=0, tiled=False)  20.9 us
    ppermute x4, starting transfers between devices, flipped(): return lax.ppermute(value, axis, [(0, 1), (1, 0)])  19.5 us
    all_to_all x1, starting transfers between devices, on_device(): lax.all_to_all(back.reshape(experts * parts, share, piece), ALL, split_ax...  18.8 us
    ppermute x3, starting transfers between devices, on_device(): lax.ppermute(blocks[step], 'p', [(i, (i + step) % groups) for i in range(...  15.5 us
    ppermute x1, waiting for transfers between devices, on_device(): lax.ppermute(mixer_rows[length - lead:], 'ep', [(i, i + 1) for i in range...  13.8 us
    all_to_all x1, starting transfers between devices, on_device(): lax.all_to_all(outgoing.reshape(experts, share, width), 'ep', split_axis=...  7.57 us
    ppermute x1, starting transfers between devices, on_device(): received = lax.ppermute(sent, 'q', swap)  6.55 us
  transfers between devices with their start and end apart: 12, of which 7 were waited for; matrix products, arithmetic and copies ran while one was open for 2% of the time, Pallas kernels for 6%

profile of v6, /device:TPU:385, one launch (start us, length us, event | category | flops | bytes accessed | tf_op | source)
XLA Modules:
  0.0 170.0 jit_solution(4290978218090815720)
XLA Ops:
  0.6 1.5 pad_maximum_fusion.a0
  2.1 3.2 %collective-permute-start.1 = (bf16[6144,128]{1,0:T(8,128)(2,1)S(1)}, bf16[6144,128]{1,0:T(8,128)(2,1)S(1)}, u32[]{:S(2)}, u32[]{:S(2)}) collective-permute-start(bf16[6144,128]{1,0:T(8,128)(2,1)S(1)} %pad_maximum_fusion.a0), channel_id=1, source_target_pairs={{0,2},{2,0},{1,3},{3,1},{4,6},{6,4},{5,7},{7,5},{8,10},{10,8},{9,1... | collective-permute-start | bytes 4718600 | tf_op jit(solution)/shard_map/ppermute | solution.py:17
  5.3 3.0 %route.1 = (bf16[256,2048]{1,0:T(8,128)(2,1)}, f32[256,128]{1,0:T(8,128)}) custom-call(s32[1]{0:T(128)} %bitcast.1.quarter_ref, s32[2,256]{1,0:T(2,128)} %bitcast.61, f32[2,256]{1,0:T(2,128)} %bitcast.62, bf16[256,2048]{1,0:T(8,128)(2,1)} %rows_ref.2, f32[1,2048]{1,0:T(1,128)} %bitcast.59), custom_call_target="tpu_custom_call" | custom-call | tf_op jit(solution)/shard_map/route/pallas_call | solution.py:70
  8.3 7.6 %all-to-all-start = ((bf16[32,8,2048]{2,1,0:T(8,128)(2,1)}), bf16[32,8,2048]{2,1,0:T(8,128)(2,1)}, u32[]{:S(2)}, u32[]{:S(2)}) async-start(bf16[32,8,2048]{2,1,0:T(8,128)(2,1)} %bitcast.52), calls=%async_computation | async-start | bytes 2097152 | tf_op jit(solution)/shard_map/all_to_all | solution.py:344
  15.9 3.4 %collective-permute-start = (bf16[6144,128]{1,0:T(8,128)(2,1)S(1)}, bf16[6144,128]{1,0:T(8,128)(2,1)}, u32[]{:S(2)}, u32[]{:S(2)}) collective-permute-start(bf16[6144,128]{1,0:T(8,128)(2,1)S(1)} %pad_maximum_fusion.a0), channel_id=1, source_target_pairs={{0,1},{1,0},{2,3},{3,2},{4,5},{5,4},{6,7},{7,6},{8,9},{9,8},{10,11... | collective-permute-start | bytes 4718600 | tf_op jit(solution)/shard_map/ppermute | solution.py:17
  19.4 20.0 %collective-permute-done.1.a2 = bf16[6144,128]{1,0:T(8,128)(2,1)S(1)} collective-permute-done((bf16[6144,128]{1,0:T(8,128)(2,1)S(1)}, bf16[6144,128]{1,0:T(8,128)(2,1)S(1)}, u32[]{:S(2)}, u32[]{:S(2)}) %collective-permute-start.1) | collective-permute-done | bytes 1572896 | tf_op jit(solution)/shard_map/ppermute | solution.py:17
  39.4 3.3 %collective-permute-start.2 = (bf16[6144,128]{1,0:T(8,128)(2,1)S(1)}, bf16[6144,128]{1,0:T(8,128)(2,1)}, u32[]{:S(2)}, u32[]{:S(2)}) collective-permute-start(bf16[6144,128]{1,0:T(8,128)(2,1)S(1)} %collective-permute-done.1.a2), channel_id=1, source_target_pairs={{0,1},{1,0},{2,3},{3,2},{4,5},{5,4},{6,7},{7,6},{8,9},{9,8},{10,11... | collective-permute-start | bytes 4718600 | tf_op jit(solution)/shard_map/ppermute | solution.py:17
  42.7 3.1 %collective-permute-done.2.a3 = bf16[6144,128]{1,0:T(8,128)(2,1)} collective-permute-done((bf16[6144,128]{1,0:T(8,128)(2,1)S(1)}, bf16[6144,128]{1,0:T(8,128)(2,1)}, u32[]{:S(2)}, u32[]{:S(2)}) %collective-permute-start.2) | collective-permute-done | bytes 1572896 | tf_op jit(solution)/shard_map/ppermute | solution.py:17
  45.9 6.1 %expert_ffn.1 = bf16[256,2048]{1,0:T(8,128)(2,1)} custom-call(bf16[256,2048]{1,0:T(8,128)(2,1)} %bitcast.6.x_hbm, bf16[6144,128]{1,0:T(8,128)(2,1)} %copy-done, bf16[6144,128]{1,0:T(8,128)(2,1)} %collective-permute-done.a1, bf16[6144,128]{1,0:T(8,128)(2,1)} %copy-done.1, bf16[6144,128]{1,0:T(8,128)(2,1)} %collective-permute-done.2.a3, ...), custom_call_target="tpu_custom_call" | custom-call | flops 1610612736 | bytes 8388608 | tf_op jit(solution)/shard_map/expert_ffn/pallas_call | solution.py:203
  52.0 18.8 %all-to-all-start.1 = ((bf16[512,8,128]{2,1,0:T(8,128)(2,1)}), bf16[512,8,128]{2,1,0:T(8,128)(2,1)S(1)}, u32[]{:S(2)}, u32[]{:S(2)}) async-start(bf16[512,8,128]{2,1,0:T(8,128)(2,1)} %bitcast.48), calls=%async_computation.1 | async-start | bytes 2097152 | tf_op jit(solution)/shard_map/all_to_all | solution.py:366
  70.9 0.8 slice.9
  71.6 3.1 %collective-permute-start.3 = (bf16[8,2048]{1,0:T(8,128)(2,1)S(1)}, bf16[8,2048]{1,0:T(8,128)(2,1)S(1)}, u32[]{:S(2)}, u32[]{:S(2)}) collective-permute-start(bf16[8,2048]{1,0:T(8,128)(2,1)S(1)} %slice.9), channel_id=1, source_target_pairs={{0,16},{16,32},{32,48},{48,64},{64,80},{80,96},{96,112},{112,128},... | collective-permute-start | bytes 98312 | tf_op jit(solution)/shard_map/ppermute | solution.py:339
  74.7 13.8 %collective-permute-done.3.before_ref = bf16[8,2048]{1,0:T(8,128)(2,1)S(1)} collective-permute-done((bf16[8,2048]{1,0:T(8,128)(2,1)S(1)}, bf16[8,2048]{1,0:T(8,128)(2,1)S(1)}, u32[]{:S(2)}, u32[]{:S(2)}) %collective-permute-start.3) | collective-permute-done | bytes 32800 | tf_op jit(solution)/shard_map/ppermute | solution.py:339
  89.1 3.5 %mixer.1 = (bf16[8,128,128]{2,1,0:T(8,128)(2,1)}, bf16[8,128,128]{2,1,0:T(8,128)(2,1)}) custom-call(s32[1]{0:T(128)} %bitcast.core_ref, bf16[8,2048]{1,0:T(8,128)(2,1)} %copy-done.6, bf16[128,2048]{1,0:T(8,128)(2,1)} %rows_ref.3, f32[1,2048]{1,0:T(1,128)} %bitcast.60, bf16[64,2048]{1,0:T(8,128)(2,1)} %bitcast.56, bf16[64,2048]{1,0:T(8,128)(2,1)} %bitcast.57, ...), custom_call_target="tpu_custom_call" | custom-call | tf_op jit(solution)/shard_map/mixer/pallas_call | solution.py:121
  92.6 2.5 %collective-permute-start.4 = (bf16[8,128,128]{2,1,0:T(8,128)(2,1)}, bf16[8,128,128]{2,1,0:T(8,128)(2,1)S(1)}, u32[]{:S(2)}, u32[]{:S(2)}) collective-permute-start(bf16[8,128,128]{2,1,0:T(8,128)(2,1)} %get-tuple-element.15), channel_id=1, source_target_pairs={{0,1},{1,0},{2,3},{3,2},{4,5},{5,4},{6,7},{7,6},{8,9},{9,8},{10,11... | collective-permute-start | bytes 786440 | tf_op jit(solution)/shard_map/ppermute | solution.py:132
  95.2 1.3 collective-permute-done.4
  96.5 1.0 add_convert_fusion
  98.2 6.5 %collective-permute-start.5 = (bf16[4,128,128]{2,1,0:T(8,128)(2,1)S(1)}, bf16[4,128,128]{2,1,0:T(8,128)(2,1)S(1)}, u32[]{:S(2)}, u32[]{:S(2)}) collective-permute-start(bf16[4,128,128]{2,1,0:T(8,128)(2,1)S(1)} %get-tuple-element.22), channel_id=1, source_target_pairs={{0,2},{2,0},{1,3},{3,1},{4,6},{6,4},{5,7},{7,5},{8,10},{10,8},{9,1... | collective-permute-start | bytes 393224 | tf_op jit(solution)/shard_map/ppermute | solution.py:356
  104.8 3.5 %collective-permute-done.5.received_ref = bf16[4,128,128]{2,1,0:T(8,128)(2,1)S(1)} collective-permute-done((bf16[4,128,128]{2,1,0:T(8,128)(2,1)S(1)}, bf16[4,128,128]{2,1,0:T(8,128)(2,1)S(1)}, u32[]{:S(2)}, u32[]{:S(2)}) %collective-permute-start.5) | collective-permute-done | bytes 131104 | tf_op jit(solution)/shard_map/ppermute | solution.py:356
  108.9 1.6 spread_blocks.1
  110.5 7.2 %collective-permute-start.8 = (bf16[128,128]{1,0:T(8,128)(2,1)}, bf16[128,128]{1,0:T(8,128)(2,1)S(1)}, u32[]{:S(2)}, u32[]{:S(2)}) collective-permute-start(bf16[128,128]{1,0:T(8,128)(2,1)} %get-tuple-element.19), channel_id=1, source_target_pairs={{0,12},{4,0},{8,4},{12,8},{1,13},{5,1},{9,5},{13,9},{2,14},{6,2},{... | collective-permute-start | bytes 98312 | tf_op jit(solution)/shard_map/ppermute | solution.py:360
  117.7 4.1 %collective-permute-start.7 = (bf16[128,128]{1,0:T(8,128)(2,1)}, bf16[128,128]{1,0:T(8,128)(2,1)S(1)}, u32[]{:S(2)}, u32[]{:S(2)}) collective-permute-start(bf16[128,128]{1,0:T(8,128)(2,1)} %get-tuple-element.18), channel_id=1, source_target_pairs={{0,8},{4,12},{8,0},{12,4},{1,9},{5,13},{9,1},{13,5},{2,10},{6,14},... | collective-permute-start | bytes 98312 | tf_op jit(solution)/shard_map/ppermute | solution.py:360
  121.8 4.3 %collective-permute-start.6 = (bf16[128,128]{1,0:T(8,128)(2,1)}, bf16[128,128]{1,0:T(8,128)(2,1)S(1)}, u32[]{:S(2)}, u32[]{:S(2)}) collective-permute-start(bf16[128,128]{1,0:T(8,128)(2,1)} %get-tuple-element.17), channel_id=1, source_target_pairs={{0,4},{4,8},{8,12},{12,0},{1,5},{5,9},{9,13},{13,1},{2,6},{6,10},{... | collective-permute-start | bytes 98312 | tf_op jit(solution)/shard_map/ppermute | solution.py:360
  126.5 2.7 %collective-permute-done.6 = bf16[128,128]{1,0:T(8,128)(2,1)S(1)} collective-permute-done((bf16[128,128]{1,0:T(8,128)(2,1)}, bf16[128,128]{1,0:T(8,128)(2,1)S(1)}, u32[]{:S(2)}, u32[]{:S(2)}) %collective-permute-start.6) | collective-permute-done | bytes 32800 | tf_op jit(solution)/shard_map/ppermute | solution.py:360
  129.2 1.4 add_convert_fusion.1.mixer_ref
  130.6 1.0 copy-done.2
  131.6 2.8 %combine.1 = bf16[384,128]{1,0:T(8,128)(2,1)} custom-call(f32[256,128]{1,0:T(8,128)} %get-tuple-element.12.picks_ref, bf16[32,4,32,128]{3,2,1,0:T(8,128)(2,1)} %bitcast.49, bf16[128,128]{1,0:T(8,128)(2,1)} %add_convert_fusion.1.mixer_ref), custom_call_target="tpu_custom_call" | custom-call | tf_op jit(solution)/shard_map/combine/pallas_call | solution.py:256
  134.3 20.9 %all-gather = bf16[3072,128]{1,0:T(8,128)(2,1)S(1)} all-gather(bf16[384,128]{1,0:T(8,128)(2,1)} %combine.1), channel_id=2, replica_groups=mesh['ep'=32,'p'=4,'q'=2,'c'=2] {'p','q'}, dimensions={0}, use_global_device_ids=true | all-gather | bytes 884736 | tf_op jit(solution)/shard_map/all_gather | solution.py:371
  155.2 9.6 %collective-permute-start.9 = (bf16[8,384,128]{2,1,0:T(8,128)(2,1)S(1)}, bf16[8,384,128]{2,1,0:T(8,128)(2,1)S(1)}, u32[]{:S(2)}, u32[]{:S(2)}) collective-permute-start(bf16[8,384,128]{2,1,0:T(8,128)(2,1)S(1)} %bitcast.50), channel_id=1, source_target_pairs={{0,1},{1,0},{2,3},{3,2},{4,5},{5,4},{6,7},{7,6},{8,9},{9,8},{10,11... | collective-permute-start | bytes 2359304 | tf_op jit(solution)/shard_map/ppermute | solution.py:17
  164.9 2.1 %placed.2 = (bf16[128,2048]{1,0:T(8,128)(2,1)}, bf16[256,2048]{1,0:T(8,128)(2,1)}) custom-call(s32[1]{0:T(128)} %bitcast.core_ref, bf16[8,384,128]{2,1,0:T(8,128)(2,1)} %bitcast.51), custom_call_target="tpu_custom_call" | custom-call | tf_op jit(solution)/shard_map/placed/pallas_call | solution.py:289
  167.0 0.9 copy-done.4
  167.9 2.1 %placed.3 = (bf16[128,2048]{1,0:T(8,128)(2,1)}, bf16[256,2048]{1,0:T(8,128)(2,1)}) custom-call(s32[1]{0:T(128)} %bitcast.core_ref, bf16[8,384,128]{2,1,0:T(8,128)(2,1)} %copy-done.4, bf16[128,2048]{1,0:T(8,128)(2,1)} %get-tuple-element.20.refs_0_, bf16[256,2048]{1,0:T(8,128)(2,1)} %get-tuple-element.21.refs_1_), custom_call_target="tpu_custom_call", output_to_operand_aliasing={{0}: (2, {}), {1}: (3, {})} | custom-call | tf_op jit(solution)/shard_map/placed/pallas_call | solution.py:289
  (19 shorter events, 2.4 us)
Async XLA Ops:
  2.1 13.8 %copy-start = (bf16[6144,128]{1,0:T(8,128)(2,1)}, bf16[6144,128]{1,0:T(8,128)(2,1)S(1)}, u32[]{:S(2)}) copy-start(bf16[6144,128]{1,0:T(8,128)(2,1)S(1)} %pad_maximum_fusion.a0) | copy-start | bytes 4718596
  2.1 37.3 %collective-permute-start.1 = (bf16[6144,128]{1,0:T(8,128)(2,1)S(1)}, bf16[6144,128]{1,0:T(8,128)(2,1)S(1)}, u32[]{:S(2)}, u32[]{:S(2)}) collective-permute-start(bf16[6144,128]{1,0:T(8,128)(2,1)S(1)} %pad_maximum_fusion.a0), channel_id=1, source_target_pairs={{0,2},{2,0},{1,3},{3,1},{4,6},{6,4},{5,7},{7,5},{8,10},{10,8},{9,1... | collective-permute-start | bytes 4718600 | tf_op jit(solution)/shard_map/ppermute | solution.py:17
  8.3 34.4 %all-to-all-start = ((bf16[32,8,2048]{2,1,0:T(8,128)(2,1)}), bf16[32,8,2048]{2,1,0:T(8,128)(2,1)}, u32[]{:S(2)}, u32[]{:S(2)}) async-start(bf16[32,8,2048]{2,1,0:T(8,128)(2,1)} %bitcast.52), calls=%async_computation | async-start | bytes 2097152 | tf_op jit(solution)/shard_map/all_to_all | solution.py:344
  15.9 26.8 %collective-permute-start = (bf16[6144,128]{1,0:T(8,128)(2,1)S(1)}, bf16[6144,128]{1,0:T(8,128)(2,1)}, u32[]{:S(2)}, u32[]{:S(2)}) collective-permute-start(bf16[6144,128]{1,0:T(8,128)(2,1)S(1)} %pad_maximum_fusion.a0), channel_id=1, source_target_pairs={{0,1},{1,0},{2,3},{3,2},{4,5},{5,4},{6,7},{7,6},{8,9},{9,8},{10,11... | collective-permute-start | bytes 4718600 | tf_op jit(solution)/shard_map/ppermute | solution.py:17
  39.4 6.5 %copy-start.1 = (bf16[6144,128]{1,0:T(8,128)(2,1)}, bf16[6144,128]{1,0:T(8,128)(2,1)S(1)}, u32[]{:S(2)}) copy-start(bf16[6144,128]{1,0:T(8,128)(2,1)S(1)} %collective-permute-done.1.a2) | copy-start | bytes 4718596
  39.4 6.5 %collective-permute-start.2 = (bf16[6144,128]{1,0:T(8,128)(2,1)S(1)}, bf16[6144,128]{1,0:T(8,128)(2,1)}, u32[]{:S(2)}, u32[]{:S(2)}) collective-permute-start(bf16[6144,128]{1,0:T(8,128)(2,1)S(1)} %collective-permute-done.1.a2), channel_id=1, source_target_pairs={{0,1},{1,0},{2,3},{3,2},{4,5},{5,4},{6,7},{7,6},{8,9},{9,8},{10,11... | collective-permute-start | bytes 4718600 | tf_op jit(solution)/shard_map/ppermute | solution.py:17
  52.0 78.6 %all-to-all-start.1 = ((bf16[512,8,128]{2,1,0:T(8,128)(2,1)}), bf16[512,8,128]{2,1,0:T(8,128)(2,1)S(1)}, u32[]{:S(2)}, u32[]{:S(2)}) async-start(bf16[512,8,128]{2,1,0:T(8,128)(2,1)} %bitcast.48), calls=%async_computation.1 | async-start | bytes 2097152 | tf_op jit(solution)/shard_map/all_to_all | solution.py:366
  71.6 16.9 %collective-permute-start.3 = (bf16[8,2048]{1,0:T(8,128)(2,1)S(1)}, bf16[8,2048]{1,0:T(8,128)(2,1)S(1)}, u32[]{:S(2)}, u32[]{:S(2)}) collective-permute-start(bf16[8,2048]{1,0:T(8,128)(2,1)S(1)} %slice.9), channel_id=1, source_target_pairs={{0,16},{16,32},{32,48},{48,64},{64,80},{80,96},{96,112},{112,128},... | collective-permute-start | bytes 98312 | tf_op jit(solution)/shard_map/ppermute | solution.py:339
  88.5 0.6 copy-start.6
  92.6 3.9 %collective-permute-start.4 = (bf16[8,128,128]{2,1,0:T(8,128)(2,1)}, bf16[8,128,128]{2,1,0:T(8,128)(2,1)S(1)}, u32[]{:S(2)}, u32[]{:S(2)}) collective-permute-start(bf16[8,128,128]{2,1,0:T(8,128)(2,1)} %get-tuple-element.15), channel_id=1, source_target_pairs={{0,1},{1,0},{2,3},{3,2},{4,5},{5,4},{6,7},{7,6},{8,9},{9,8},{10,11... | collective-permute-start | bytes 786440 | tf_op jit(solution)/shard_map/ppermute | solution.py:132
  98.2 10.0 %collective-permute-start.5 = (bf16[4,128,128]{2,1,0:T(8,128)(2,1)S(1)}, bf16[4,128,128]{2,1,0:T(8,128)(2,1)S(1)}, u32[]{:S(2)}, u32[]{:S(2)}) collective-permute-start(bf16[4,128,128]{2,1,0:T(8,128)(2,1)S(1)} %get-tuple-element.22), channel_id=1, source_target_pairs={{0,2},{2,0},{1,3},{3,1},{4,6},{6,4},{5,7},{7,5},{8,10},{10,8},{9,1... | collective-permute-start | bytes 393224 | tf_op jit(solution)/shard_map/ppermute | solution.py:356
  108.3 0.6 copy-start.5
  110.5 15.6 %collective-permute-start.8 = (bf16[128,128]{1,0:T(8,128)(2,1)}, bf16[128,128]{1,0:T(8,128)(2,1)S(1)}, u32[]{:S(2)}, u32[]{:S(2)}) collective-permute-start(bf16[128,128]{1,0:T(8,128)(2,1)} %get-tuple-element.19), channel_id=1, source_target_pairs={{0,12},{4,0},{8,4},{12,8},{1,13},{5,1},{9,5},{13,9},{2,14},{6,2},{... | collective-permute-start | bytes 98312 | tf_op jit(solution)/shard_map/ppermute | solution.py:360
  117.7 8.8 %collective-permute-start.7 = (bf16[128,128]{1,0:T(8,128)(2,1)}, bf16[128,128]{1,0:T(8,128)(2,1)S(1)}, u32[]{:S(2)}, u32[]{:S(2)}) collective-permute-start(bf16[128,128]{1,0:T(8,128)(2,1)} %get-tuple-element.18), channel_id=1, source_target_pairs={{0,8},{4,12},{8,0},{12,4},{1,9},{5,13},{9,1},{13,5},{2,10},{6,14},... | collective-permute-start | bytes 98312 | tf_op jit(solution)/shard_map/ppermute | solution.py:360
  121.8 7.4 %collective-permute-start.6 = (bf16[128,128]{1,0:T(8,128)(2,1)}, bf16[128,128]{1,0:T(8,128)(2,1)S(1)}, u32[]{:S(2)}, u32[]{:S(2)}) collective-permute-start(bf16[128,128]{1,0:T(8,128)(2,1)} %get-tuple-element.17), channel_id=1, source_target_pairs={{0,4},{4,8},{8,12},{12,0},{1,5},{5,9},{9,13},{13,1},{2,6},{6,10},{... | collective-permute-start | bytes 98312 | tf_op jit(solution)/shard_map/ppermute | solution.py:360
  130.6 1.0 copy-start.2
  155.2 9.6 %copy-start.3 = (bf16[3072,128]{1,0:T(8,128)(2,1)}, bf16[3072,128]{1,0:T(8,128)(2,1)S(1)}, u32[]{:S(2)}) copy-start(bf16[3072,128]{1,0:T(8,128)(2,1)S(1)} %all-gather) | copy-start | bytes 2359300
  155.2 11.8 %collective-permute-start.9 = (bf16[8,384,128]{2,1,0:T(8,128)(2,1)S(1)}, bf16[8,384,128]{2,1,0:T(8,128)(2,1)S(1)}, u32[]{:S(2)}, u32[]{:S(2)}) collective-permute-start(bf16[8,384,128]{2,1,0:T(8,128)(2,1)S(1)} %bitcast.50), channel_id=1, source_target_pairs={{0,1},{1,0},{2,3},{3,2},{4,5},{5,4},{6,7},{7,6},{8,9},{9,8},{10,11... | collective-permute-start | bytes 2359304 | tf_op jit(solution)/shard_map/ppermute | solution.py:17
  167.0 0.9 copy-start.4

commit v7 on v6

--- a/solution.py
+++ b/solution.py
@@ -23,13 +23,16 @@
     weights_ref,
     rows_ref,
     gain_ref,
+    last_ref,
     out_ref,
     picks_ref,
+    halo_ref,
     *,
     experts,
     capacity,
     share,
 ):
+    halo_ref[...] = last_ref[...]
     picks, tokens = ids_ref.shape
     slots = out_ref.shape[0]
     expert = lax.broadcasted_iota(jnp.int32, (experts, tokens), 0)
@@ -65,18 +68,27 @@
     ).astype(jnp.bfloat16)
 
 
-def routed_slots(quarter, ids, weights, rows, gain, experts, capacity, share):
+def routed_slots(quarter, ids, weights, rows, gain, mixer_rows, lead, experts, capacity, share):
     tokens, width = rows.shape
     return pl.pallas_call(
         functools.partial(route_kernel, experts=experts, capacity=capacity, share=share),
         out_shape=(
             jax.ShapeDtypeStruct((experts * share, width), jnp.bfloat16),
             jax.ShapeDtypeStruct((tokens, 128), jnp.float32),
+            jax.ShapeDtypeStruct((lead, width), jnp.bfloat16),
         ),
-        in_specs=[pl.BlockSpec(memory_space=pltpu.SMEM), VM, VM, VM, VM],
-        out_specs=(VM, VM),
+        grid=(1,),
+        in_specs=[
+            pl.BlockSpec(memory_space=pltpu.SMEM),
+            VM,
+            VM,
+            VM,
+            VM,
+            pl.BlockSpec((lead, width), lambda i: (mixer_rows.shape[0] // lead - 1, 0)),
+        ],
+        out_specs=(VM, VM, VM),
         name="route",
-    )(quarter.reshape(1), ids.T, weights.T, rows, gain.reshape(1, -1))
+    )(quarter.reshape(1), ids.T, weights.T, rows, gain.reshape(1, -1), mixer_rows)
 
 
 def mixer_kernel(
@@ -164,7 +176,7 @@
     lead = b0.shape[0] - part
     x_copy = pltpu.make_async_copy(x_hbm, x_ref, sems.at[0])
     x_copy.start()
-    copies = []
+    weights, downs = [], []
     for i, (a, b) in enumerate(((a0, b0), (a1, b1), (a2, b2), (a3, b3))):
         gate = pltpu.make_async_copy(
             a.at[pl.ds(0, width), :], gu_ref.at[i, :, pl.ds(0, part)], sems.at[3 * i + 1]
@@ -175,19 +187,22 @@
         down = pltpu.make_async_copy(
             b.at[pl.ds(lead, part), :], down_ref.at[pl.ds(i * part, part), :], sems.at[3 * i + 3]
         )
-        gate.start()
-        up.start()
-        copies.append((gate, up, down))
-    for _, _, down in copies:
-        down.start()
+        weights.append((gate, up))
+        downs.append(down)
+    later = weights[2:] + [downs]
+    for copy in weights[0] + weights[1]:
+        copy.start()
     x_copy.wait()
-    for i, (gate, up, _) in enumerate(copies):
-        gate.wait()
-        up.wait()
+    for i, slices in enumerate(weights):
+        for copy in slices:
+            copy.wait()
+        if i < len(later):
+            for copy in later[i]:
+                copy.start()
         acts = jnp.dot(x_ref[...], gu_ref[i], preferred_element_type=jnp.float32)
         g = acts[:, :part]
         hid_ref[:, i * part : (i + 1) * part] = (g / (1.0 + jnp.exp(-g)) * acts[:, part:]).astype(jnp.bfloat16)
-    for _, _, down in copies:
+    for down in downs:
         down.wait()
     cols = 512
     for n in range(0, width, cols):
@@ -229,37 +244,38 @@
     return value.reshape(-1, width // part, 8, part).transpose(0, 2, 1, 3).reshape(-1, width)
 
 
-def combine_kernel(picks_ref, rows_ref, mixer_ref, out_ref, *, picks):
-    experts, groups, capacity, width = rows_ref.shape
+def combine_kernel(core_ref, picks_ref, rows_ref, keep_ref, send_ref, *, picks, share, capacity):
+    experts, groups, pair, width = rows_ref.shape
     tokens = picks_ref.shape[0]
-    slots = experts * capacity
-    column = lax.broadcasted_iota(jnp.int32, (tokens, slots), 1)
+    slots = experts * pair
+    core = core_ref[0]
+    slot = lax.broadcasted_iota(jnp.int32, (tokens, slots), 1)
+    column = slot // pair * capacity + slot % pair // share * (2 * share) + slot % share + core * share
     spread = jnp.zeros((tokens, slots), jnp.float32)
     for k in range(picks):
         key = picks_ref[:, k : k + 1].astype(jnp.int32)
         spread = jnp.where(column == key, picks_ref[:, picks + k : picks + k + 1], spread)
     high = spread.astype(jnp.bfloat16)
     low = (spread - high.astype(jnp.float32)).astype(jnp.bfloat16)
-    total = jnp.zeros((tokens, 2 * width), jnp.float32)
-    for g in range(0, groups, 2):
-        rows = jnp.concatenate(
-            [rows_ref[:, g].reshape(slots, width), rows_ref[:, g + 1].reshape(slots, width)], axis=1
-        )
+    total = jnp.zeros((tokens, width), jnp.float32)
+    for g in range(groups):
+        rows = rows_ref[:, g].reshape(slots, width)
         total = total + jnp.dot(high, rows, preferred_element_type=jnp.float32)
         total = total + jnp.dot(low, rows, preferred_element_type=jnp.float32)
-    length = mixer_ref.shape[0]
-    out_ref[:length, :] = mixer_ref[...]
-    out_ref[length:, :] = (total[:, :width] + total[:, width:]).astype(jnp.bfloat16)
-
-
-def combined(table, rows, mixer_part, picks):
-    return pl.pallas_call(
-        functools.partial(combine_kernel, picks=picks),
-        out_shape=jax.ShapeDtypeStruct((mixer_part.shape[0] + table.shape[0], rows.shape[-1]), jnp.bfloat16),
-        in_specs=[VM] * 3,
-        out_specs=VM,
+    left, right = total[:, : width // 2], total[:, width // 2 :]
+    keep_ref[...] = jnp.where(core == 0, left, right)
+    send_ref[...] = jnp.where(core == 0, right, left).astype(jnp.bfloat16)
+
+
+def combined(core, table, rows, picks, share, capacity):
+    half = (table.shape[0], rows.shape[-1] // 2)
+    return pl.pallas_call(
+        functools.partial(combine_kernel, picks=picks, share=share, capacity=capacity),
+        out_shape=(jax.ShapeDtypeStruct(half, jnp.float32), jax.ShapeDtypeStruct(half, jnp.bfloat16)),
+        in_specs=[pl.BlockSpec(memory_space=pltpu.SMEM), VM, VM],
+        out_specs=(VM, VM),
         name="combine",
-    )(table, rows, mixer_part)
+    )(core.reshape(1), table, rows)
 
 
 def place_kernel(core_ref, parts_ref, *refs, length, flip):
@@ -335,12 +351,10 @@
     pack = jnp.concatenate([expert_gate[0], expert_up[0], narrow_view(expert_down[0], hidden_part)], axis=0)
     pack_q = flipped(pack, "q")
 
-    lead = 8
-    before = lax.ppermute(mixer_rows[length - lead :], "ep", [(i, i + 1) for i in range(experts - 1)])
-
-    outgoing, table = routed_slots(
-        quarter, route_ids, route_weights, routed_rows, routed_gain, experts, capacity, share
-    )
+    outgoing, table, last_rows = routed_slots(
+        quarter, route_ids, route_weights, routed_rows, routed_gain, mixer_rows, 8, experts, capacity, share
+    )
+    before = lax.ppermute(last_rows, "ep", [(i, i + 1) for i in range(experts - 1)])
     slot_rows = lax.all_to_all(
         outgoing.reshape(experts, share, width), "ep", split_axis=0, concat_axis=0, tiled=True
     ).reshape(experts * share, width)
@@ -362,12 +376,18 @@
     mixer_part = total.astype(jnp.bfloat16)
 
     results = expert_ffn(slot_rows, (pack, pack_c, pack_q, pack_qc), sharers * hidden_part)
-    back = results.reshape(experts, share, parts, piece).transpose(0, 2, 1, 3)
+    chips = parts // 2
+    back = results.reshape(experts, share, chips, 2 * piece).transpose(0, 2, 1, 3)
     back = lax.all_to_all(
-        back.reshape(experts * parts, share, piece), ALL, split_axis=0, concat_axis=0, tiled=True
-    )
-    pieces = combined(table, back.reshape(experts, groups, capacity, piece), mixer_part, pick_count)
-
+        back.reshape(experts * chips, share, 2 * piece), ALL[:3], split_axis=0, concat_axis=0, tiled=True
+    )
+    kept, sent = combined(
+        core, table, back.reshape(experts, groups, 2 * share, 2 * piece), pick_count, share, capacity
+    )
+    received = flipped(sent, "c")
+    routed_part = (kept + received.astype(jnp.float32)).astype(jnp.bfloat16)
+
+    pieces = jnp.concatenate([mixer_part, routed_part], axis=0)
     mine = lax.all_gather(pieces, ("p", "q"), axis=0, tiled=False)
     other = flipped(mine, "c")
     wholes = placed(core, mine, length)

time: 171 us -> 173 us (1.012)
  the two profiles are of different devices: /device:TPU:385 before, /device:TPU:193 now
where the time goes in v7:
time: 173 us; the launch traced here: 172 us
  starting transfers between devices  86.1 us (50%)
  waiting for transfers between devices  34.6 us (20%)
  Pallas kernels  21.6 us (12%)
  blocking collectives  20.8 us (12%)
  other arithmetic  4.87 us (3%)
  local copies, waits for them, and re-layouts  3.15 us (2%)
    ppermute x5, starting transfers between devices, flipped(): return lax.ppermute(value, axis, [(0, 1), (1, 0)])  21.4 us
    all_gather x1, blocking collectives, on_device(): mine = lax.all_gather(pieces, ('p', 'q'), axis=0, tiled=False)  20.8 us
    ppermute x3, starting transfers between devices, on_device(): lax.ppermute(blocks[step], 'p', [(i, (i + step) % groups) for i in range(...  20.5 us
    ppermute x5, waiting for transfers between devices, flipped(): return lax.ppermute(value, axis, [(0, 1), (1, 0)])  19 us
    all_to_all x1, starting transfers between devices, on_device(): lax.all_to_all(back.reshape(experts * chips, share, 2 * piece), ALL[:3],...  18.7 us
    all_to_all x1, starting transfers between devices, on_device(): lax.all_to_all(outgoing.reshape(experts, share, width), 'ep', split_axis=...  10.3 us
    ppermute x1, waiting for transfers between devices, on_device(): lax.ppermute(last_rows, 'ep', [(i, i + 1) for i in range(experts - 1)])  9 us
    ppermute x1, starting transfers between devices, summed(): received = lax.ppermute(sent, axis, pairs)  6.4 us
  transfers between devices with their start and end apart: 13, of which 7 were waited for; matrix products, arithmetic and copies ran while one was open for 1% of the time, Pallas kernels for 8%

profile of v7, /device:TPU:193, one launch (start us, length us, event | category | flops | bytes accessed | tf_op | source)
XLA Modules:
  0.0 172.1 jit_solution(14525750936512966840)
XLA Ops:
  0.6 1.5 pad_maximum_fusion.a0
  2.1 3.2 %collective-permute-start.7 = (bf16[6144,128]{1,0:T(8,128)(2,1)S(1)}, bf16[6144,128]{1,0:T(8,128)(2,1)S(1)}, u32[]{:S(2)}, u32[]{:S(2)}) collective-permute-start(bf16[6144,128]{1,0:T(8,128)(2,1)S(1)} %pad_maximum_fusion.a0), channel_id=1, source_target_pairs={{0,2},{2,0},{1,3},{3,1},{4,6},{6,4},{5,7},{7,5},{8,10},{10,8},{9,1... | collective-permute-start | bytes 4718600 | tf_op jit(solution)/shard_map/ppermute | solution.py:17
  5.3 3.0 %route.1 = (bf16[256,2048]{1,0:T(8,128)(2,1)}, f32[256,128]{1,0:T(8,128)}, bf16[8,2048]{1,0:T(8,128)(2,1)}) custom-call(s32[1]{0:T(128)} %bitcast.2.quarter_ref, s32[2,256]{1,0:T(2,128)} %bitcast.61, f32[2,256]{1,0:T(2,128)} %bitcast.62, bf16[256,2048]{1,0:T(8,128)(2,1)} %rows_ref.2, f32[1,2048]{1,0:T(1,128)} %bitcast.59, bf16[128,2048]{1,0:T(8,128)(2,1)} %rows_ref.3), custom_call_target="tpu_custom_call" | custom-call | tf_op jit(solution)/shard_map/route/pallas_call | solution.py:73
  8.4 10.3 %all-to-all-start = ((bf16[32,8,2048]{2,1,0:T(8,128)(2,1)}), bf16[32,8,2048]{2,1,0:T(8,128)(2,1)}, u32[]{:S(2)}, u32[]{:S(2)}) async-start(bf16[32,8,2048]{2,1,0:T(8,128)(2,1)} %bitcast.52), calls=%async_computation | async-start | bytes 2097152 | tf_op jit(solution)/shard_map/all_to_all | solution.py:358
  18.6 3.4 %collective-permute-start.6 = (bf16[6144,128]{1,0:T(8,128)(2,1)S(1)}, bf16[6144,128]{1,0:T(8,128)(2,1)}, u32[]{:S(2)}, u32[]{:S(2)}) collective-permute-start(bf16[6144,128]{1,0:T(8,128)(2,1)S(1)} %pad_maximum_fusion.a0), channel_id=1, source_target_pairs={{0,1},{1,0},{2,3},{3,2},{4,5},{5,4},{6,7},{7,6},{8,9},{9,8},{10,11... | collective-permute-start | bytes 4718600 | tf_op jit(solution)/shard_map/ppermute | solution.py:17
  22.1 17.3 %collective-permute-done.7.a2 = bf16[6144,128]{1,0:T(8,128)(2,1)S(1)} collective-permute-done((bf16[6144,128]{1,0:T(8,128)(2,1)S(1)}, bf16[6144,128]{1,0:T(8,128)(2,1)S(1)}, u32[]{:S(2)}, u32[]{:S(2)}) %collective-permute-start.7) | collective-permute-done | bytes 1572896 | tf_op jit(solution)/shard_map/ppermute | solution.py:17
  39.4 3.3 %collective-permute-start.8 = (bf16[6144,128]{1,0:T(8,128)(2,1)S(1)}, bf16[6144,128]{1,0:T(8,128)(2,1)}, u32[]{:S(2)}, u32[]{:S(2)}) collective-permute-start(bf16[6144,128]{1,0:T(8,128)(2,1)S(1)} %collective-permute-done.7.a2), channel_id=1, source_target_pairs={{0,1},{1,0},{2,3},{3,2},{4,5},{5,4},{6,7},{7,6},{8,9},{9,8},{10,11... | collective-permute-start | bytes 4718600 | tf_op jit(solution)/shard_map/ppermute | solution.py:17
  42.7 1.7 all-to-all-done
  44.4 1.4 collective-permute-done.8.a3
  45.9 6.3 %expert_ffn.1 = bf16[256,2048]{1,0:T(8,128)(2,1)} custom-call(bf16[256,2048]{1,0:T(8,128)(2,1)} %bitcast.11.x_hbm, bf16[6144,128]{1,0:T(8,128)(2,1)} %copy-done, bf16[6144,128]{1,0:T(8,128)(2,1)} %collective-permute-done.6.a1, bf16[6144,128]{1,0:T(8,128)(2,1)} %copy-done.1, bf16[6144,128]{1,0:T(8,128)(2,1)} %collective-permute-done.8.a3, ...), custom_call_target="tpu_custom_call" | custom-call | flops 1610612736 | bytes 8388608 | tf_op jit(solution)/shard_map/expert_ffn/pallas_call | solution.py:218
  52.2 18.7 %all-to-all-start.1 = ((bf16[256,8,256]{2,1,0:T(8,128)(2,1)}), bf16[256,8,256]{2,1,0:T(8,128)(2,1)S(1)}, u32[]{:S(2)}, u32[]{:S(2)}) async-start(bf16[256,8,256]{2,1,0:T(8,128)(2,1)} %bitcast.48), calls=%async_computation.1 | async-start | bytes 2097152 | tf_op jit(solution)/shard_map/all_to_all | solution.py:381
  70.9 3.1 %collective-permute-start = (bf16[8,2048]{1,0:T(8,128)(2,1)S(1)}, bf16[8,2048]{1,0:T(8,128)(2,1)S(1)}, u32[]{:S(2)}, u32[]{:S(2)}) collective-permute-start(bf16[8,2048]{1,0:T(8,128)(2,1)S(1)} %copy-done.7), channel_id=1, source_target_pairs={{0,16},{16,32},{32,48},{48,64},{64,80},{80,96},{96,112},{112,128},... | collective-permute-start | bytes 98312 | tf_op jit(solution)/shard_map/ppermute | solution.py:357
  74.1 9.0 %collective-permute-done.before_ref = bf16[8,2048]{1,0:T(8,128)(2,1)S(1)} collective-permute-done((bf16[8,2048]{1,0:T(8,128)(2,1)S(1)}, bf16[8,2048]{1,0:T(8,128)(2,1)S(1)}, u32[]{:S(2)}, u32[]{:S(2)}) %collective-permute-start) | collective-permute-done | bytes 32800 | tf_op jit(solution)/shard_map/ppermute | solution.py:357
  83.7 3.5 %mixer.1 = (bf16[8,128,128]{2,1,0:T(8,128)(2,1)}, bf16[8,128,128]{2,1,0:T(8,128)(2,1)}) custom-call(s32[1]{0:T(128)} %bitcast.core_ref, bf16[8,2048]{1,0:T(8,128)(2,1)} %copy-done.6, bf16[128,2048]{1,0:T(8,128)(2,1)} %rows_ref.3, f32[1,2048]{1,0:T(1,128)} %bitcast.60, bf16[64,2048]{1,0:T(8,128)(2,1)} %bitcast.56, bf16[64,2048]{1,0:T(8,128)(2,1)} %bitcast.57, ...), custom_call_target="tpu_custom_call" | custom-call | tf_op jit(solution)/shard_map/mixer/pallas_call | solution.py:133
  87.2 6.4 %collective-permute-start.1 = (bf16[8,128,128]{2,1,0:T(8,128)(2,1)}, bf16[8,128,128]{2,1,0:T(8,128)(2,1)S(1)}, u32[]{:S(2)}, u32[]{:S(2)}) collective-permute-start(bf16[8,128,128]{2,1,0:T(8,128)(2,1)} %get-tuple-element.17), channel_id=1, source_target_pairs={{0,1},{1,0},{2,3},{3,2},{4,5},{5,4},{6,7},{7,6},{8,9},{9,8},{10,11... | collective-permute-start | bytes 786440 | tf_op jit(solution)/shard_map/ppermute | solution.py:144
  93.6 1.3 collective-permute-done.1
  95.0 1.0 add_convert_fusion
  96.7 5.7 %collective-permute-start.2 = (bf16[4,128,128]{2,1,0:T(8,128)(2,1)S(1)}, bf16[4,128,128]{2,1,0:T(8,128)(2,1)S(1)}, u32[]{:S(2)}, u32[]{:S(2)}) collective-permute-start(bf16[4,128,128]{2,1,0:T(8,128)(2,1)S(1)} %get-tuple-element.28), channel_id=1, source_target_pairs={{0,2},{2,0},{1,3},{3,1},{4,6},{6,4},{5,7},{7,5},{8,10},{10,8},{9,1... | collective-permute-start | bytes 393224 | tf_op jit(solution)/shard_map/ppermute | solution.py:370
  102.4 3.5 %collective-permute-done.2.received_ref = bf16[4,128,128]{2,1,0:T(8,128)(2,1)S(1)} collective-permute-done((bf16[4,128,128]{2,1,0:T(8,128)(2,1)S(1)}, bf16[4,128,128]{2,1,0:T(8,128)(2,1)S(1)}, u32[]{:S(2)}, u32[]{:S(2)}) %collective-permute-start.2) | collective-permute-done | bytes 131104 | tf_op jit(solution)/shard_map/ppermute | solution.py:370
  106.6 1.6 spread_blocks.1
  108.2 5.0 %collective-permute-start.3 = (bf16[128,128]{1,0:T(8,128)(2,1)}, bf16[128,128]{1,0:T(8,128)(2,1)S(1)}, u32[]{:S(2)}, u32[]{:S(2)}) collective-permute-start(bf16[128,128]{1,0:T(8,128)(2,1)} %get-tuple-element.19), channel_id=1, source_target_pairs={{0,4},{4,8},{8,12},{12,0},{1,5},{5,9},{9,13},{13,1},{2,6},{6,10},{... | collective-permute-start | bytes 98312 | tf_op jit(solution)/shard_map/ppermute | solution.py:374
  113.2 10.0 %collective-permute-start.4 = (bf16[128,128]{1,0:T(8,128)(2,1)}, bf16[128,128]{1,0:T(8,128)(2,1)S(1)}, u32[]{:S(2)}, u32[]{:S(2)}) collective-permute-start(bf16[128,128]{1,0:T(8,128)(2,1)} %get-tuple-element.20), channel_id=1, source_target_pairs={{0,8},{4,12},{8,0},{12,4},{1,9},{5,13},{9,1},{13,5},{2,10},{6,14},... | collective-permute-start | bytes 98312 | tf_op jit(solution)/shard_map/ppermute | solution.py:374
  123.2 5.5 %collective-permute-start.5 = (bf16[128,128]{1,0:T(8,128)(2,1)}, bf16[128,128]{1,0:T(8,128)(2,1)S(1)}, u32[]{:S(2)}, u32[]{:S(2)}) collective-permute-start(bf16[128,128]{1,0:T(8,128)(2,1)} %get-tuple-element.21), channel_id=1, source_target_pairs={{0,12},{4,0},{8,4},{12,8},{1,13},{5,1},{9,5},{13,9},{2,14},{6,2},{... | collective-permute-start | bytes 98312 | tf_op jit(solution)/shard_map/ppermute | solution.py:374
  128.7 1.0 copy-done.2
  129.7 2.9 %combine.1 = (f32[256,128]{1,0:T(8,128)}, bf16[256,128]{1,0:T(8,128)(2,1)}) custom-call(s32[1]{0:T(128)} %bitcast.core_ref, f32[256,128]{1,0:T(8,128)} %get-tuple-element.22.picks_ref, bf16[32,4,16,256]{3,2,1,0:T(8,128)(2,1)} %bitcast.49), custom_call_target="tpu_custom_call" | custom-call | tf_op jit(solution)/shard_map/combine/pallas_call | solution.py:272
  132.5 4.0 %collective-permute-start.9 = (bf16[256,128]{1,0:T(8,128)(2,1)}, bf16[256,128]{1,0:T(8,128)(2,1)S(1)}, u32[]{:S(2)}, u32[]{:S(2)}) collective-permute-start(bf16[256,128]{1,0:T(8,128)(2,1)} %get-tuple-element.25), channel_id=1, source_target_pairs={{0,1},{1,0},{2,3},{3,2},{4,5},{5,4},{6,7},{7,6},{8,9},{9,8},{10,11... | collective-permute-start | bytes 196616 | tf_op jit(solution)/shard_map/ppermute | solution.py:17
  137.6 0.9 add_convert_fusion.1
  138.6 20.8 %all-gather = bf16[3072,128]{1,0:T(8,128)(2,1)S(1)} all-gather(bf16[384,128]{1,0:T(8,128)(2,1)S(1)} %pad_maximum_fusion.1), channel_id=2, replica_groups=mesh['ep'=32,'p'=4,'q'=2,'c'=2] {'p','q'}, dimensions={0}, use_global_device_ids=true | all-gather | bytes 884736 | tf_op jit(solution)/shard_map/all_gather | solution.py:391
  159.4 7.5 %collective-permute-start.10 = (bf16[8,384,128]{2,1,0:T(8,128)(2,1)S(1)}, bf16[8,384,128]{2,1,0:T(8,128)(2,1)S(1)}, u32[]{:S(2)}, u32[]{:S(2)}) collective-permute-start(bf16[8,384,128]{2,1,0:T(8,128)(2,1)S(1)} %bitcast.50), channel_id=1, source_target_pairs={{0,1},{1,0},{2,3},{3,2},{4,5},{5,4},{6,7},{7,6},{8,9},{9,8},{10,11... | collective-permute-start | bytes 2359304 | tf_op jit(solution)/shard_map/ppermute | solution.py:17
  166.9 2.1 %placed.2 = (bf16[128,2048]{1,0:T(8,128)(2,1)}, bf16[256,2048]{1,0:T(8,128)(2,1)}) custom-call(s32[1]{0:T(128)} %bitcast.core_ref, bf16[8,384,128]{2,1,0:T(8,128)(2,1)} %bitcast.51), custom_call_target="tpu_custom_call" | custom-call | tf_op jit(solution)/shard_map/placed/pallas_call | solution.py:305
  169.1 0.9 copy-done.4
  169.9 2.1 %placed.3 = (bf16[128,2048]{1,0:T(8,128)(2,1)}, bf16[256,2048]{1,0:T(8,128)(2,1)}) custom-call(s32[1]{0:T(128)} %bitcast.core_ref, bf16[8,384,128]{2,1,0:T(8,128)(2,1)} %copy-done.4, bf16[128,2048]{1,0:T(8,128)(2,1)} %get-tuple-element.26.refs_0_, bf16[256,2048]{1,0:T(8,128)(2,1)} %get-tuple-element.27.refs_1_), custom_call_target="tpu_custom_call", output_to_operand_aliasing={{0}: (2, {}), {1}: (3, {})} | custom-call | tf_op jit(solution)/shard_map/placed/pallas_call | solution.py:305
  (24 shorter events, 3.1 us)
Async XLA Ops:
  2.1 16.5 %copy-start = (bf16[6144,128]{1,0:T(8,128)(2,1)}, bf16[6144,128]{1,0:T(8,128)(2,1)S(1)}, u32[]{:S(2)}) copy-start(bf16[6144,128]{1,0:T(8,128)(2,1)S(1)} %pad_maximum_fusion.a0) | copy-start | bytes 4718596
  2.1 37.3 %collective-permute-start.7 = (bf16[6144,128]{1,0:T(8,128)(2,1)S(1)}, bf16[6144,128]{1,0:T(8,128)(2,1)S(1)}, u32[]{:S(2)}, u32[]{:S(2)}) collective-permute-start(bf16[6144,128]{1,0:T(8,128)(2,1)S(1)} %pad_maximum_fusion.a0), channel_id=1, source_target_pairs={{0,2},{2,0},{1,3},{3,1},{4,6},{6,4},{5,7},{7,5},{8,10},{10,8},{9,1... | collective-permute-start | bytes 4718600 | tf_op jit(solution)/shard_map/ppermute | solution.py:17
  8.4 36.1 %all-to-all-start = ((bf16[32,8,2048]{2,1,0:T(8,128)(2,1)}), bf16[32,8,2048]{2,1,0:T(8,128)(2,1)}, u32[]{:S(2)}, u32[]{:S(2)}) async-start(bf16[32,8,2048]{2,1,0:T(8,128)(2,1)} %bitcast.52), calls=%async_computation | async-start | bytes 2097152 | tf_op jit(solution)/shard_map/all_to_all | solution.py:358
  18.6 24.1 %collective-permute-start.6 = (bf16[6144,128]{1,0:T(8,128)(2,1)S(1)}, bf16[6144,128]{1,0:T(8,128)(2,1)}, u32[]{:S(2)}, u32[]{:S(2)}) collective-permute-start(bf16[6144,128]{1,0:T(8,128)(2,1)S(1)} %pad_maximum_fusion.a0), channel_id=1, source_target_pairs={{0,1},{1,0},{2,3},{3,2},{4,5},{5,4},{6,7},{7,6},{8,9},{9,8},{10,11... | collective-permute-start | bytes 4718600 | tf_op jit(solution)/shard_map/ppermute | solution.py:17
  39.4 6.5 %copy-start.1 = (bf16[6144,128]{1,0:T(8,128)(2,1)}, bf16[6144,128]{1,0:T(8,128)(2,1)S(1)}, u32[]{:S(2)}) copy-start(bf16[6144,128]{1,0:T(8,128)(2,1)S(1)} %collective-permute-done.7.a2) | copy-start | bytes 4718596
  39.4 6.5 %collective-permute-start.8 = (bf16[6144,128]{1,0:T(8,128)(2,1)S(1)}, bf16[6144,128]{1,0:T(8,128)(2,1)}, u32[]{:S(2)}, u32[]{:S(2)}) collective-permute-start(bf16[6144,128]{1,0:T(8,128)(2,1)S(1)} %collective-permute-done.7.a2), channel_id=1, source_target_pairs={{0,1},{1,0},{2,3},{3,2},{4,5},{5,4},{6,7},{7,6},{8,9},{9,8},{10,11... | collective-permute-start | bytes 4718600 | tf_op jit(solution)/shard_map/ppermute | solution.py:17
  52.2 18.7 %copy-start.7 = (bf16[8,2048]{1,0:T(8,128)(2,1)S(1)}, bf16[8,2048]{1,0:T(8,128)(2,1)}, u32[]{:S(2)}) copy-start(bf16[8,2048]{1,0:T(8,128)(2,1)} %get-tuple-element.15) | copy-start | bytes 98308
  52.2 76.5 %all-to-all-start.1 = ((bf16[256,8,256]{2,1,0:T(8,128)(2,1)}), bf16[256,8,256]{2,1,0:T(8,128)(2,1)S(1)}, u32[]{:S(2)}, u32[]{:S(2)}) async-start(bf16[256,8,256]{2,1,0:T(8,128)(2,1)} %bitcast.48), calls=%async_computation.1 | async-start | bytes 2097152 | tf_op jit(solution)/shard_map/all_to_all | solution.py:381
  70.9 12.2 %collective-permute-start = (bf16[8,2048]{1,0:T(8,128)(2,1)S(1)}, bf16[8,2048]{1,0:T(8,128)(2,1)S(1)}, u32[]{:S(2)}, u32[]{:S(2)}) collective-permute-start(bf16[8,2048]{1,0:T(8,128)(2,1)S(1)} %copy-done.7), channel_id=1, source_target_pairs={{0,16},{16,32},{32,48},{48,64},{64,80},{80,96},{96,112},{112,128},... | collective-permute-start | bytes 98312 | tf_op jit(solution)/shard_map/ppermute | solution.py:357
  83.1 0.6 copy-start.6
  87.2 7.8 %collective-permute-start.1 = (bf16[8,128,128]{2,1,0:T(8,128)(2,1)}, bf16[8,128,128]{2,1,0:T(8,128)(2,1)S(1)}, u32[]{:S(2)}, u32[]{:S(2)}) collective-permute-start(bf16[8,128,128]{2,1,0:T(8,128)(2,1)} %get-tuple-element.17), channel_id=1, source_target_pairs={{0,1},{1,0},{2,3},{3,2},{4,5},{5,4},{6,7},{7,6},{8,9},{9,8},{10,11... | collective-permute-start | bytes 786440 | tf_op jit(solution)/shard_map/ppermute | solution.py:144
  96.7 9.2 %collective-permute-start.2 = (bf16[4,128,128]{2,1,0:T(8,128)(2,1)S(1)}, bf16[4,128,128]{2,1,0:T(8,128)(2,1)S(1)}, u32[]{:S(2)}, u32[]{:S(2)}) collective-permute-start(bf16[4,128,128]{2,1,0:T(8,128)(2,1)S(1)} %get-tuple-element.28), channel_id=1, source_target_pairs={{0,2},{2,0},{1,3},{3,1},{4,6},{6,4},{5,7},{7,5},{8,10},{10,8},{9,1... | collective-permute-start | bytes 393224 | tf_op jit(solution)/shard_map/ppermute | solution.py:370
  105.9 0.7 copy-start.5
  108.2 28.3 %collective-permute-start.3 = (bf16[128,128]{1,0:T(8,128)(2,1)}, bf16[128,128]{1,0:T(8,128)(2,1)S(1)}, u32[]{:S(2)}, u32[]{:S(2)}) collective-permute-start(bf16[128,128]{1,0:T(8,128)(2,1)} %get-tuple-element.19), channel_id=1, source_target_pairs={{0,4},{4,8},{8,12},{12,0},{1,5},{5,9},{9,13},{13,1},{2,6},{6,10},{... | collective-permute-start | bytes 98312 | tf_op jit(solution)/shard_map/ppermute | solution.py:374
  113.2 23.4 %collective-permute-start.4 = (bf16[128,128]{1,0:T(8,128)(2,1)}, bf16[128,128]{1,0:T(8,128)(2,1)S(1)}, u32[]{:S(2)}, u32[]{:S(2)}) collective-permute-start(bf16[128,128]{1,0:T(8,128)(2,1)} %get-tuple-element.20), channel_id=1, source_target_pairs={{0,8},{4,12},{8,0},{12,4},{1,9},{5,13},{9,1},{13,5},{2,10},{6,14},... | collective-permute-start | bytes 98312 | tf_op jit(solution)/shard_map/ppermute | solution.py:374
  123.2 13.3 %collective-permute-start.5 = (bf16[128,128]{1,0:T(8,128)(2,1)}, bf16[128,128]{1,0:T(8,128)(2,1)S(1)}, u32[]{:S(2)}, u32[]{:S(2)}) collective-permute-start(bf16[128,128]{1,0:T(8,128)(2,1)} %get-tuple-element.21), channel_id=1, source_target_pairs={{0,12},{4,0},{8,4},{12,8},{1,13},{5,1},{9,5},{13,9},{2,14},{6,2},{... | collective-permute-start | bytes 98312 | tf_op jit(solution)/shard_map/ppermute | solution.py:374
  128.7 1.0 copy-start.2
  132.5 5.1 %collective-permute-start.9 = (bf16[256,128]{1,0:T(8,128)(2,1)}, bf16[256,128]{1,0:T(8,128)(2,1)S(1)}, u32[]{:S(2)}, u32[]{:S(2)}) collective-permute-start(bf16[256,128]{1,0:T(8,128)(2,1)} %get-tuple-element.25), channel_id=1, source_target_pairs={{0,1},{1,0},{2,3},{3,2},{4,5},{5,4},{6,7},{7,6},{8,9},{9,8},{10,11... | collective-permute-start | bytes 196616 | tf_op jit(solution)/shard_map/ppermute | solution.py:17
  159.4 7.5 %copy-start.3 = (bf16[3072,128]{1,0:T(8,128)(2,1)}, bf16[3072,128]{1,0:T(8,128)(2,1)S(1)}, u32[]{:S(2)}) copy-start(bf16[3072,128]{1,0:T(8,128)(2,1)S(1)} %all-gather) | copy-start | bytes 2359300
  159.4 9.6 %collective-permute-start.10 = (bf16[8,384,128]{2,1,0:T(8,128)(2,1)S(1)}, bf16[8,384,128]{2,1,0:T(8,128)(2,1)S(1)}, u32[]{:S(2)}, u32[]{:S(2)}) collective-permute-start(bf16[8,384,128]{2,1,0:T(8,128)(2,1)S(1)} %bitcast.50), channel_id=1, source_target_pairs={{0,1},{1,0},{2,3},{3,2},{4,5},{5,4},{6,7},{7,6},{8,9},{9,8},{10,11... | collective-permute-start | bytes 2359304 | tf_op jit(solution)/shard_map/ppermute | solution.py:17
  169.0 0.9 copy-start.4

commit v8 on v6

--- a/solution.py
+++ b/solution.py
@@ -23,13 +23,16 @@
     weights_ref,
     rows_ref,
     gain_ref,
+    last_ref,
     out_ref,
     picks_ref,
+    halo_ref,
     *,
     experts,
     capacity,
     share,
 ):
+    halo_ref[...] = last_ref[...]
     picks, tokens = ids_ref.shape
     slots = out_ref.shape[0]
     expert = lax.broadcasted_iota(jnp.int32, (experts, tokens), 0)
@@ -65,18 +68,27 @@
     ).astype(jnp.bfloat16)
 
 
-def routed_slots(quarter, ids, weights, rows, gain, experts, capacity, share):
+def routed_slots(quarter, ids, weights, rows, gain, mixer_rows, lead, experts, capacity, share):
     tokens, width = rows.shape
     return pl.pallas_call(
         functools.partial(route_kernel, experts=experts, capacity=capacity, share=share),
         out_shape=(
             jax.ShapeDtypeStruct((experts * share, width), jnp.bfloat16),
             jax.ShapeDtypeStruct((tokens, 128), jnp.float32),
+            jax.ShapeDtypeStruct((lead, width), jnp.bfloat16),
         ),
-        in_specs=[pl.BlockSpec(memory_space=pltpu.SMEM), VM, VM, VM, VM],
-        out_specs=(VM, VM),
+        grid=(1,),
+        in_specs=[
+            pl.BlockSpec(memory_space=pltpu.SMEM),
+            VM,
+            VM,
+            VM,
+            VM,
+            pl.BlockSpec((lead, width), lambda i: (mixer_rows.shape[0] // lead - 1, 0)),
+        ],
+        out_specs=(VM, VM, VM),
         name="route",
-    )(quarter.reshape(1), ids.T, weights.T, rows, gain.reshape(1, -1))
+    )(quarter.reshape(1), ids.T, weights.T, rows, gain.reshape(1, -1), mixer_rows)
 
 
 def mixer_kernel(
@@ -335,12 +347,10 @@
     pack = jnp.concatenate([expert_gate[0], expert_up[0], narrow_view(expert_down[0], hidden_part)], axis=0)
     pack_q = flipped(pack, "q")
 
-    lead = 8
-    before = lax.ppermute(mixer_rows[length - lead :], "ep", [(i, i + 1) for i in range(experts - 1)])
-
-    outgoing, table = routed_slots(
-        quarter, route_ids, route_weights, routed_rows, routed_gain, experts, capacity, share
+    outgoing, table, last_rows = routed_slots(
+        quarter, route_ids, route_weights, routed_rows, routed_gain, mixer_rows, 8, experts, capacity, share
     )
+    before = lax.ppermute(last_rows, "ep", [(i, i + 1) for i in range(experts - 1)])
     slot_rows = lax.all_to_all(
         outgoing.reshape(experts, share, width), "ep", split_axis=0, concat_axis=0, tiled=True
     ).reshape(experts * share, width)

time: 171 us -> 173 us (1.012)
  starting transfers between devices: 73.7 us -> 76.1 us
  transfers between devices with their start and end apart: 12 -> 12, of which waited for: 7 -> 6; matrix products, arithmetic and copies ran while one was open for 2% -> 2% of each run, Pallas kernels for 6% -> 6%
where the time goes in v8:
time: 173 us; the launch traced here: 172 us
  starting transfers between devices  76.1 us (44%)
  waiting for transfers between devices  44 us (25%)
  blocking collectives  21.7 us (13%)
  Pallas kernels  21.4 us (12%)
  other arithmetic  4.55 us (3%)
  local copies, waits for them, and re-layouts  3.13 us (2%)
    ppermute x4, waiting for transfers between devices, flipped(): return lax.ppermute(value, axis, [(0, 1), (1, 0)])  23.1 us
    all_gather x1, blocking collectives, on_device(): mine = lax.all_gather(pieces, ('p', 'q'), axis=0, tiled=False)  21.7 us
    ppermute x4, starting transfers between devices, flipped(): return lax.ppermute(value, axis, [(0, 1), (1, 0)])  20.7 us
    all_to_all x1, starting transfers between devices, on_device(): lax.all_to_all(back.reshape(experts * parts, share, piece), ALL, split_ax...  18.8 us
    ppermute x3, starting transfers between devices, on_device(): lax.ppermute(blocks[step], 'p', [(i, (i + step) % groups) for i in range(...  16.8 us
    ppermute x1, waiting for transfers between devices, on_device(): lax.ppermute(last_rows, 'ep', [(i, i + 1) for i in range(experts - 1)])  14.5 us
    all_to_all x1, starting transfers between devices, on_device(): lax.all_to_all(outgoing.reshape(experts, share, width), 'ep', split_axis=...  7.58 us
    ppermute x1, starting transfers between devices, on_device(): received = lax.ppermute(sent, 'q', swap)  6.53 us
  transfers between devices with their start and end apart: 12, of which 6 were waited for; matrix products, arithmetic and copies ran while one was open for 2% of the time, Pallas kernels for 6%

profile of v8, /device:TPU:385, one launch (start us, length us, event | category | flops | bytes accessed | tf_op | source)
XLA Modules:
  0.0 171.7 jit_solution(12296628966898723126)
XLA Ops:
  0.6 1.5 pad_maximum_fusion.a0
  2.1 3.2 %collective-permute-start.1 = (bf16[6144,128]{1,0:T(8,128)(2,1)S(1)}, bf16[6144,128]{1,0:T(8,128)(2,1)S(1)}, u32[]{:S(2)}, u32[]{:S(2)}) collective-permute-start(bf16[6144,128]{1,0:T(8,128)(2,1)S(1)} %pad_maximum_fusion.a0), channel_id=1, source_target_pairs={{0,2},{2,0},{1,3},{3,1},{4,6},{6,4},{5,7},{7,5},{8,10},{10,8},{9,1... | collective-permute-start | bytes 4718600 | tf_op jit(solution)/shard_map/ppermute | solution.py:17
  5.3 3.0 %route.1 = (bf16[256,2048]{1,0:T(8,128)(2,1)}, f32[256,128]{1,0:T(8,128)}, bf16[8,2048]{1,0:T(8,128)(2,1)}) custom-call(s32[1]{0:T(128)} %bitcast.1.quarter_ref, s32[2,256]{1,0:T(2,128)} %bitcast.61, f32[2,256]{1,0:T(2,128)} %bitcast.62, bf16[256,2048]{1,0:T(8,128)(2,1)} %rows_ref.2, f32[1,2048]{1,0:T(1,128)} %bitcast.59, bf16[128,2048]{1,0:T(8,128)(2,1)} %rows_ref.3), custom_call_target="tpu_custom_call" | custom-call | tf_op jit(solution)/shard_map/route/pallas_call | solution.py:73
  8.4 7.6 %all-to-all-start = ((bf16[32,8,2048]{2,1,0:T(8,128)(2,1)}), bf16[32,8,2048]{2,1,0:T(8,128)(2,1)}, u32[]{:S(2)}, u32[]{:S(2)}) async-start(bf16[32,8,2048]{2,1,0:T(8,128)(2,1)} %bitcast.52), calls=%async_computation | async-start | bytes 2097152 | tf_op jit(solution)/shard_map/all_to_all | solution.py:354
  16.0 3.4 %collective-permute-start = (bf16[6144,128]{1,0:T(8,128)(2,1)S(1)}, bf16[6144,128]{1,0:T(8,128)(2,1)}, u32[]{:S(2)}, u32[]{:S(2)}) collective-permute-start(bf16[6144,128]{1,0:T(8,128)(2,1)S(1)} %pad_maximum_fusion.a0), channel_id=1, source_target_pairs={{0,1},{1,0},{2,3},{3,2},{4,5},{5,4},{6,7},{7,6},{8,9},{9,8},{10,11... | collective-permute-start | bytes 4718600 | tf_op jit(solution)/shard_map/ppermute | solution.py:17
  19.4 20.0 %collective-permute-done.1.a2 = bf16[6144,128]{1,0:T(8,128)(2,1)S(1)} collective-permute-done((bf16[6144,128]{1,0:T(8,128)(2,1)S(1)}, bf16[6144,128]{1,0:T(8,128)(2,1)S(1)}, u32[]{:S(2)}, u32[]{:S(2)}) %collective-permute-start.1) | collective-permute-done | bytes 1572896 | tf_op jit(solution)/shard_map/ppermute | solution.py:17
  39.4 3.3 %collective-permute-start.2 = (bf16[6144,128]{1,0:T(8,128)(2,1)S(1)}, bf16[6144,128]{1,0:T(8,128)(2,1)}, u32[]{:S(2)}, u32[]{:S(2)}) collective-permute-start(bf16[6144,128]{1,0:T(8,128)(2,1)S(1)} %collective-permute-done.1.a2), channel_id=1, source_target_pairs={{0,1},{1,0},{2,3},{3,2},{4,5},{5,4},{6,7},{7,6},{8,9},{9,8},{10,11... | collective-permute-start | bytes 4718600 | tf_op jit(solution)/shard_map/ppermute | solution.py:17
  42.7 3.1 %collective-permute-done.2.a3 = bf16[6144,128]{1,0:T(8,128)(2,1)} collective-permute-done((bf16[6144,128]{1,0:T(8,128)(2,1)S(1)}, bf16[6144,128]{1,0:T(8,128)(2,1)}, u32[]{:S(2)}, u32[]{:S(2)}) %collective-permute-start.2) | collective-permute-done | bytes 1572896 | tf_op jit(solution)/shard_map/ppermute | solution.py:17
  45.9 6.1 %expert_ffn.1 = bf16[256,2048]{1,0:T(8,128)(2,1)} custom-call(bf16[256,2048]{1,0:T(8,128)(2,1)} %bitcast.6.x_hbm, bf16[6144,128]{1,0:T(8,128)(2,1)} %copy-done, bf16[6144,128]{1,0:T(8,128)(2,1)} %collective-permute-done.a1, bf16[6144,128]{1,0:T(8,128)(2,1)} %copy-done.1, bf16[6144,128]{1,0:T(8,128)(2,1)} %collective-permute-done.2.a3, ...), custom_call_target="tpu_custom_call" | custom-call | flops 1610612736 | bytes 8388608 | tf_op jit(solution)/shard_map/expert_ffn/pallas_call | solution.py:215
  52.0 18.8 %all-to-all-start.1 = ((bf16[512,8,128]{2,1,0:T(8,128)(2,1)}), bf16[512,8,128]{2,1,0:T(8,128)(2,1)S(1)}, u32[]{:S(2)}, u32[]{:S(2)}) async-start(bf16[512,8,128]{2,1,0:T(8,128)(2,1)} %bitcast.48), calls=%async_computation.1 | async-start | bytes 2097152 | tf_op jit(solution)/shard_map/all_to_all | solution.py:376
  70.9 3.1 %collective-permute-start.3 = (bf16[8,2048]{1,0:T(8,128)(2,1)S(1)}, bf16[8,2048]{1,0:T(8,128)(2,1)S(1)}, u32[]{:S(2)}, u32[]{:S(2)}) collective-permute-start(bf16[8,2048]{1,0:T(8,128)(2,1)S(1)} %copy-done.7), channel_id=1, source_target_pairs={{0,16},{16,32},{32,48},{48,64},{64,80},{80,96},{96,112},{112,128},... | collective-permute-start | bytes 98312 | tf_op jit(solution)/shard_map/ppermute | solution.py:353
  74.0 14.5 %collective-permute-done.3.before_ref = bf16[8,2048]{1,0:T(8,128)(2,1)S(1)} collective-permute-done((bf16[8,2048]{1,0:T(8,128)(2,1)S(1)}, bf16[8,2048]{1,0:T(8,128)(2,1)S(1)}, u32[]{:S(2)}, u32[]{:S(2)}) %collective-permute-start.3) | collective-permute-done | bytes 32800 | tf_op jit(solution)/shard_map/ppermute | solution.py:353
  89.1 3.5 %mixer.1 = (bf16[8,128,128]{2,1,0:T(8,128)(2,1)}, bf16[8,128,128]{2,1,0:T(8,128)(2,1)}) custom-call(s32[1]{0:T(128)} %bitcast.core_ref, bf16[8,2048]{1,0:T(8,128)(2,1)} %copy-done.6, bf16[128,2048]{1,0:T(8,128)(2,1)} %rows_ref.3, f32[1,2048]{1,0:T(1,128)} %bitcast.60, bf16[64,2048]{1,0:T(8,128)(2,1)} %bitcast.56, bf16[64,2048]{1,0:T(8,128)(2,1)} %bitcast.57, ...), custom_call_target="tpu_custom_call" | custom-call | tf_op jit(solution)/shard_map/mixer/pallas_call | solution.py:133
  92.6 2.5 %collective-permute-start.4 = (bf16[8,128,128]{2,1,0:T(8,128)(2,1)}, bf16[8,128,128]{2,1,0:T(8,128)(2,1)S(1)}, u32[]{:S(2)}, u32[]{:S(2)}) collective-permute-start(bf16[8,128,128]{2,1,0:T(8,128)(2,1)} %get-tuple-element.17), channel_id=1, source_target_pairs={{0,1},{1,0},{2,3},{3,2},{4,5},{5,4},{6,7},{7,6},{8,9},{9,8},{10,11... | collective-permute-start | bytes 786440 | tf_op jit(solution)/shard_map/ppermute | solution.py:144
  95.2 1.3 collective-permute-done.4
  96.5 1.0 add_convert_fusion
  97.5 0.7 broadcast_select_fusion
  98.2 6.5 %collective-permute-start.5 = (bf16[4,128,128]{2,1,0:T(8,128)(2,1)S(1)}, bf16[4,128,128]{2,1,0:T(8,128)(2,1)S(1)}, u32[]{:S(2)}, u32[]{:S(2)}) collective-permute-start(bf16[4,128,128]{2,1,0:T(8,128)(2,1)S(1)} %get-tuple-element.24), channel_id=1, source_target_pairs={{0,2},{2,0},{1,3},{3,1},{4,6},{6,4},{5,7},{7,5},{8,10},{10,8},{9,1... | collective-permute-start | bytes 393224 | tf_op jit(solution)/shard_map/ppermute | solution.py:366
  104.8 3.5 %collective-permute-done.5.received_ref = bf16[4,128,128]{2,1,0:T(8,128)(2,1)S(1)} collective-permute-done((bf16[4,128,128]{2,1,0:T(8,128)(2,1)S(1)}, bf16[4,128,128]{2,1,0:T(8,128)(2,1)S(1)}, u32[]{:S(2)}, u32[]{:S(2)}) %collective-permute-start.5) | collective-permute-done | bytes 131104 | tf_op jit(solution)/shard_map/ppermute | solution.py:366
  108.9 1.6 spread_blocks.1
  110.5 4.9 %collective-permute-start.6 = (bf16[128,128]{1,0:T(8,128)(2,1)}, bf16[128,128]{1,0:T(8,128)(2,1)S(1)}, u32[]{:S(2)}, u32[]{:S(2)}) collective-permute-start(bf16[128,128]{1,0:T(8,128)(2,1)} %get-tuple-element.19), channel_id=1, source_target_pairs={{0,4},{4,8},{8,12},{12,0},{1,5},{5,9},{9,13},{13,1},{2,6},{6,10},{... | collective-permute-start | bytes 98312 | tf_op jit(solution)/shard_map/ppermute | solution.py:370
  115.5 6.4 %collective-permute-start.7 = (bf16[128,128]{1,0:T(8,128)(2,1)}, bf16[128,128]{1,0:T(8,128)(2,1)S(1)}, u32[]{:S(2)}, u32[]{:S(2)}) collective-permute-start(bf16[128,128]{1,0:T(8,128)(2,1)} %get-tuple-element.20), channel_id=1, source_target_pairs={{0,8},{4,12},{8,0},{12,4},{1,9},{5,13},{9,1},{13,5},{2,10},{6,14},... | collective-permute-start | bytes 98312 | tf_op jit(solution)/shard_map/ppermute | solution.py:370
  121.8 5.5 %collective-permute-start.8 = (bf16[128,128]{1,0:T(8,128)(2,1)}, bf16[128,128]{1,0:T(8,128)(2,1)S(1)}, u32[]{:S(2)}, u32[]{:S(2)}) collective-permute-start(bf16[128,128]{1,0:T(8,128)(2,1)} %get-tuple-element.21), channel_id=1, source_target_pairs={{0,12},{4,0},{8,4},{12,8},{1,13},{5,1},{9,5},{13,9},{2,14},{6,2},{... | collective-permute-start | bytes 98312 | tf_op jit(solution)/shard_map/ppermute | solution.py:370
  127.3 1.5 collective-permute-done.8
  128.9 1.4 add_convert_fusion.1.mixer_ref
  130.3 1.0 copy-done.2
  131.2 2.8 %combine.1 = bf16[384,128]{1,0:T(8,128)(2,1)} custom-call(f32[256,128]{1,0:T(8,128)} %get-tuple-element.13.picks_ref, bf16[32,4,32,128]{3,2,1,0:T(8,128)(2,1)} %bitcast.49, bf16[128,128]{1,0:T(8,128)(2,1)} %add_convert_fusion.1.mixer_ref), custom_call_target="tpu_custom_call" | custom-call | tf_op jit(solution)/shard_map/combine/pallas_call | solution.py:268
  134.0 21.7 %all-gather = bf16[3072,128]{1,0:T(8,128)(2,1)S(1)} all-gather(bf16[384,128]{1,0:T(8,128)(2,1)} %combine.1), channel_id=2, replica_groups=mesh['ep'=32,'p'=4,'q'=2,'c'=2] {'p','q'}, dimensions={0}, use_global_device_ids=true | all-gather | bytes 884736 | tf_op jit(solution)/shard_map/all_gather | solution.py:381
  155.8 10.8 %collective-permute-start.9 = (bf16[8,384,128]{2,1,0:T(8,128)(2,1)S(1)}, bf16[8,384,128]{2,1,0:T(8,128)(2,1)S(1)}, u32[]{:S(2)}, u32[]{:S(2)}) collective-permute-start(bf16[8,384,128]{2,1,0:T(8,128)(2,1)S(1)} %bitcast.50), channel_id=1, source_target_pairs={{0,1},{1,0},{2,3},{3,2},{4,5},{5,4},{6,7},{7,6},{8,9},{9,8},{10,11... | collective-permute-start | bytes 2359304 | tf_op jit(solution)/shard_map/ppermute | solution.py:17
  166.6 2.1 %placed.2 = (bf16[128,2048]{1,0:T(8,128)(2,1)}, bf16[256,2048]{1,0:T(8,128)(2,1)}) custom-call(s32[1]{0:T(128)} %bitcast.core_ref, bf16[8,384,128]{2,1,0:T(8,128)(2,1)} %bitcast.51), custom_call_target="tpu_custom_call" | custom-call | tf_op jit(solution)/shard_map/placed/pallas_call | solution.py:301
  168.7 0.9 copy-done.4
  169.6 2.1 %placed.3 = (bf16[128,2048]{1,0:T(8,128)(2,1)}, bf16[256,2048]{1,0:T(8,128)(2,1)}) custom-call(s32[1]{0:T(128)} %bitcast.core_ref, bf16[8,384,128]{2,1,0:T(8,128)(2,1)} %copy-done.4, bf16[128,2048]{1,0:T(8,128)(2,1)} %get-tuple-element.22.refs_0_, bf16[256,2048]{1,0:T(8,128)(2,1)} %get-tuple-element.23.refs_1_), custom_call_target="tpu_custom_call", output_to_operand_aliasing={{0}: (2, {}), {1}: (3, {})} | custom-call | tf_op jit(solution)/shard_map/placed/pallas_call | solution.py:301
  (20 shorter events, 1.3 us)
Async XLA Ops:
  2.1 13.9 %copy-start = (bf16[6144,128]{1,0:T(8,128)(2,1)}, bf16[6144,128]{1,0:T(8,128)(2,1)S(1)}, u32[]{:S(2)}) copy-start(bf16[6144,128]{1,0:T(8,128)(2,1)S(1)} %pad_maximum_fusion.a0) | copy-start | bytes 4718596
  2.1 37.3 %collective-permute-start.1 = (bf16[6144,128]{1,0:T(8,128)(2,1)S(1)}, bf16[6144,128]{1,0:T(8,128)(2,1)S(1)}, u32[]{:S(2)}, u32[]{:S(2)}) collective-permute-start(bf16[6144,128]{1,0:T(8,128)(2,1)S(1)} %pad_maximum_fusion.a0), channel_id=1, source_target_pairs={{0,2},{2,0},{1,3},{3,1},{4,6},{6,4},{5,7},{7,5},{8,10},{10,8},{9,1... | collective-permute-start | bytes 4718600 | tf_op jit(solution)/shard_map/ppermute | solution.py:17
  8.4 34.4 %all-to-all-start = ((bf16[32,8,2048]{2,1,0:T(8,128)(2,1)}), bf16[32,8,2048]{2,1,0:T(8,128)(2,1)}, u32[]{:S(2)}, u32[]{:S(2)}) async-start(bf16[32,8,2048]{2,1,0:T(8,128)(2,1)} %bitcast.52), calls=%async_computation | async-start | bytes 2097152 | tf_op jit(solution)/shard_map/all_to_all | solution.py:354
  16.0 26.8 %collective-permute-start = (bf16[6144,128]{1,0:T(8,128)(2,1)S(1)}, bf16[6144,128]{1,0:T(8,128)(2,1)}, u32[]{:S(2)}, u32[]{:S(2)}) collective-permute-start(bf16[6144,128]{1,0:T(8,128)(2,1)S(1)} %pad_maximum_fusion.a0), channel_id=1, source_target_pairs={{0,1},{1,0},{2,3},{3,2},{4,5},{5,4},{6,7},{7,6},{8,9},{9,8},{10,11... | collective-permute-start | bytes 4718600 | tf_op jit(solution)/shard_map/ppermute | solution.py:17
  39.4 6.5 %copy-start.1 = (bf16[6144,128]{1,0:T(8,128)(2,1)}, bf16[6144,128]{1,0:T(8,128)(2,1)S(1)}, u32[]{:S(2)}) copy-start(bf16[6144,128]{1,0:T(8,128)(2,1)S(1)} %collective-permute-done.1.a2) | copy-start | bytes 4718596
  39.4 6.5 %collective-permute-start.2 = (bf16[6144,128]{1,0:T(8,128)(2,1)S(1)}, bf16[6144,128]{1,0:T(8,128)(2,1)}, u32[]{:S(2)}, u32[]{:S(2)}) collective-permute-start(bf16[6144,128]{1,0:T(8,128)(2,1)S(1)} %collective-permute-done.1.a2), channel_id=1, source_target_pairs={{0,1},{1,0},{2,3},{3,2},{4,5},{5,4},{6,7},{7,6},{8,9},{9,8},{10,11... | collective-permute-start | bytes 4718600 | tf_op jit(solution)/shard_map/ppermute | solution.py:17
  52.0 18.9 %copy-start.7 = (bf16[8,2048]{1,0:T(8,128)(2,1)S(1)}, bf16[8,2048]{1,0:T(8,128)(2,1)}, u32[]{:S(2)}) copy-start(bf16[8,2048]{1,0:T(8,128)(2,1)} %get-tuple-element.15) | copy-start | bytes 98308
  52.0 78.2 %all-to-all-start.1 = ((bf16[512,8,128]{2,1,0:T(8,128)(2,1)}), bf16[512,8,128]{2,1,0:T(8,128)(2,1)S(1)}, u32[]{:S(2)}, u32[]{:S(2)}) async-start(bf16[512,8,128]{2,1,0:T(8,128)(2,1)} %bitcast.48), calls=%async_computation.1 | async-start | bytes 2097152 | tf_op jit(solution)/shard_map/all_to_all | solution.py:376
  70.9 17.6 %collective-permute-start.3 = (bf16[8,2048]{1,0:T(8,128)(2,1)S(1)}, bf16[8,2048]{1,0:T(8,128)(2,1)S(1)}, u32[]{:S(2)}, u32[]{:S(2)}) collective-permute-start(bf16[8,2048]{1,0:T(8,128)(2,1)S(1)} %copy-done.7), channel_id=1, source_target_pairs={{0,16},{16,32},{32,48},{48,64},{64,80},{80,96},{96,112},{112,128},... | collective-permute-start | bytes 98312 | tf_op jit(solution)/shard_map/ppermute | solution.py:353
  88.5 0.6 copy-start.6
  92.6 3.9 %collective-permute-start.4 = (bf16[8,128,128]{2,1,0:T(8,128)(2,1)}, bf16[8,128,128]{2,1,0:T(8,128)(2,1)S(1)}, u32[]{:S(2)}, u32[]{:S(2)}) collective-permute-start(bf16[8,128,128]{2,1,0:T(8,128)(2,1)} %get-tuple-element.17), channel_id=1, source_target_pairs={{0,1},{1,0},{2,3},{3,2},{4,5},{5,4},{6,7},{7,6},{8,9},{9,8},{10,11... | collective-permute-start | bytes 786440 | tf_op jit(solution)/shard_map/ppermute | solution.py:144
  98.2 10.0 %collective-permute-start.5 = (bf16[4,128,128]{2,1,0:T(8,128)(2,1)S(1)}, bf16[4,128,128]{2,1,0:T(8,128)(2,1)S(1)}, u32[]{:S(2)}, u32[]{:S(2)}) collective-permute-start(bf16[4,128,128]{2,1,0:T(8,128)(2,1)S(1)} %get-tuple-element.24), channel_id=1, source_target_pairs={{0,2},{2,0},{1,3},{3,1},{4,6},{6,4},{5,7},{7,5},{8,10},{10,8},{9,1... | collective-permute-start | bytes 393224 | tf_op jit(solution)/shard_map/ppermute | solution.py:366
  108.3 0.7 copy-start.5
  110.5 16.8 %collective-permute-start.6 = (bf16[128,128]{1,0:T(8,128)(2,1)}, bf16[128,128]{1,0:T(8,128)(2,1)S(1)}, u32[]{:S(2)}, u32[]{:S(2)}) collective-permute-start(bf16[128,128]{1,0:T(8,128)(2,1)} %get-tuple-element.19), channel_id=1, source_target_pairs={{0,4},{4,8},{8,12},{12,0},{1,5},{5,9},{9,13},{13,1},{2,6},{6,10},{... | collective-permute-start | bytes 98312 | tf_op jit(solution)/shard_map/ppermute | solution.py:370
  115.5 11.9 %collective-permute-start.7 = (bf16[128,128]{1,0:T(8,128)(2,1)}, bf16[128,128]{1,0:T(8,128)(2,1)S(1)}, u32[]{:S(2)}, u32[]{:S(2)}) collective-permute-start(bf16[128,128]{1,0:T(8,128)(2,1)} %get-tuple-element.20), channel_id=1, source_target_pairs={{0,8},{4,12},{8,0},{12,4},{1,9},{5,13},{9,1},{13,5},{2,10},{6,14},... | collective-permute-start | bytes 98312 | tf_op jit(solution)/shard_map/ppermute | solution.py:370
  121.8 7.0 %collective-permute-start.8 = (bf16[128,128]{1,0:T(8,128)(2,1)}, bf16[128,128]{1,0:T(8,128)(2,1)S(1)}, u32[]{:S(2)}, u32[]{:S(2)}) collective-permute-start(bf16[128,128]{1,0:T(8,128)(2,1)} %get-tuple-element.21), channel_id=1, source_target_pairs={{0,12},{4,0},{8,4},{12,8},{1,13},{5,1},{9,5},{13,9},{2,14},{6,2},{... | collective-permute-start | bytes 98312 | tf_op jit(solution)/shard_map/ppermute | solution.py:370
  130.3 1.0 copy-start.2
  155.8 10.8 %copy-start.3 = (bf16[3072,128]{1,0:T(8,128)(2,1)}, bf16[3072,128]{1,0:T(8,128)(2,1)S(1)}, u32[]{:S(2)}) copy-start(bf16[3072,128]{1,0:T(8,128)(2,1)S(1)} %all-gather) | copy-start | bytes 2359300
  155.8 12.9 %collective-permute-start.9 = (bf16[8,384,128]{2,1,0:T(8,128)(2,1)S(1)}, bf16[8,384,128]{2,1,0:T(8,128)(2,1)S(1)}, u32[]{:S(2)}, u32[]{:S(2)}) collective-permute-start(bf16[8,384,128]{2,1,0:T(8,128)(2,1)S(1)} %bitcast.50), channel_id=1, source_target_pairs={{0,1},{1,0},{2,3},{3,2},{4,5},{5,4},{6,7},{7,6},{8,9},{9,8},{10,11... | collective-permute-start | bytes 2359304 | tf_op jit(solution)/shard_map/ppermute | solution.py:17
  168.7 0.9 copy-start.4
